TPU v7x, 512 devices: a whole 4x8x8 slice. The times are simulated.
512 devices in a mesh: tp: 64 (over z, y), dp: 8 (over x, core).
Axes of the slice: x: 4, y: 8, z: 8, core: 2. Of those that a mesh axis runs over, the one named last changes fastest.
Arguments:
- hidden: bfloat16 [64, 4096], P(None, 'dp'), may hold values from -6 to 6
- norm_gain: float32 [2, 4096], P(None, 'dp'), may hold values from 0.1 to 1.9
- gate_weight: bfloat16 [2, 4096, 8192], P(None, 'dp', 'tp'), may hold values from -0.09375 to 0.09375
- inner_weight: bfloat16 [2, 4096, 8192], P(None, 'dp', 'tp'), may hold values from -0.09375 to 0.09375
- write_weight: bfloat16 [2, 4096, 2048], P(None, 'dp', 'tp'), may hold values from -0.09375 to 0.09375
- read_weight: bfloat16 [2, 4096, 2048], P(None, 'dp', 'tp'), may hold values from -0.09375 to 0.09375
- step_weight: bfloat16 [2, 4096, 128], P(None, 'dp'), may hold values from -0.09375 to 0.09375
- conv_inner: bfloat16 [2, 4, 8192], P(None, None, 'tp'), may hold values from -3 to 3
- conv_write: bfloat16 [2, 4, 2048], P(None, None, 'tp'), may hold values from -3 to 3
- conv_read: bfloat16 [2, 4, 2048], P(None, None, 'tp'), may hold values from -3 to 3
- step_bias: float32 [2, 128], P(None, 'tp'), may hold values from -4 to -1
- decay_log: float32 [2, 128], P(None, 'tp'), may hold values from -3 to 0.5
- skip_gain: float32 [2, 128], P(None, 'tp'), may hold values from 0.1 to 1.9
- group_gain: float32 [2, 8192], P(None, 'tp'), may hold values from 0.1 to 1.9
- out_weight: bfloat16 [2, 8192, 4096], P(None, 'tp', 'dp'), may hold values from -0.4 to 0.4
- state_inner: bfloat16 [2, 64, 3, 8192], P(None, 'dp', None, 'tp'), may hold values from -6 to 6
- state_write: bfloat16 [2, 64, 3, 2048], P(None, 'dp', None, 'tp'), may hold values from -6 to 6
- state_read: bfloat16 [2, 64, 3, 2048], P(None, 'dp', None, 'tp'), may hold values from -6 to 6
- recurrent: float32 [2, 64, 128, 64, 128], P(None, 'dp', 'tp'), may hold values from -1.2 to 1.2, as said below
Outputs:
- out_hidden: bfloat16 [64, 4096], P(None, 'dp')
- next_inner: bfloat16 [2, 64, 3, 8192], P(None, 'dp', None, 'tp')
- next_write: bfloat16 [2, 64, 3, 2048], P(None, 'dp', None, 'tp')
- next_read: bfloat16 [2, 64, 3, 2048], P(None, 'dp', None, 'tp')
- next_recurrent: float32 [2, 64, 128, 64, 128], P(None, 'dp', 'tp')
Inputs may be any that keep to these rules, and one draw needn't show every extreme that they name: recurrent states of order a tenth, with scales that differ between heads.
All inputs are finite; a program needn't handle non-finite values.
Results may differ from a plain program's by a relative error of at most 0.025.
Values may be sent and summed in bfloat16 or wider, within the bound.
No kernel may reach another device: no remote copies, remote signals or barrier semaphores. Data moves between devices by JAX's collectives and lax.ppermute only.
A program may use at most 64 MiB of HBM per device.

v0:
```python
import jax
import jax.numpy as jnp
from jax import lax
from jax.sharding import Mesh
from jax.sharding import PartitionSpec as P

D = 4096
HEADS = 128
GROUPS = 16
DP = ("dp_0", "dp_1")
TP = ("tp_0", "tp_1")
TP_DP = ("tp_0", "tp_1", "dp_0", "dp_1")


eps = 1e-06


def cut_along(shard, dim, size):
    before, after = (shard.shape[:dim], shard.shape[dim + 1 :])
    return jnp.moveaxis(shard.reshape(*before, size, -1, *after), dim, 0)


def summed_on_arrival(shard, axis, dim):
    size = lax.axis_size(axis)
    pieces = lax.all_to_all(cut_along(shard, dim, size), axis, 0, 0, tiled=True)
    return jnp.sum(pieces.astype(jnp.float32), axis=0)


def side_by_side(arrays, axis, dim, along):
    widths = [a.shape[along] for a in arrays]
    both = jnp.concatenate(arrays, axis=along)
    result = summed_on_arrival(both, axis, dim)
    return tuple(jnp.split(result, [sum(widths[:k]) for k in range(1, len(widths))], axis=along))


def gather_turned(arrays, axis, dims):
    turned = [jnp.moveaxis(a, dim, 0) for a, dim in zip(arrays, dims)]
    both = jnp.concatenate([t.reshape(len(t), -1) for t in turned], axis=1)
    result, at, gathered = (lax.all_gather(both, axis, axis=0, tiled=True), 0, [])
    for t, dim in zip(turned, dims):
        share = result[:, at : at + t[0].size].reshape(-1, *t.shape[1:])
        gathered.append(jnp.moveaxis(share, 0, dim))
        at += t[0].size
    return tuple(gathered)


def over_axes(shard, axes):
    for axis in axes:
        shard = lax.psum(shard, axis)
    return shard


def copy_for_each(shard, axis):
    size = lax.axis_size(axis)
    return lax.all_to_all(
        jnp.broadcast_to(shard[None], (size, *shard.shape)), axis, 0, 0, tiled=True
    )


def laid_out(pieces, dim):
    lengths = list(pieces.shape[1:])
    lengths[dim] *= pieces.shape[0]
    return jnp.moveaxis(pieces, 0, dim).reshape(lengths)


def collect(shard, axis, dim):
    pieces = copy_for_each(shard, axis)
    return laid_out(pieces, dim)


def summed_on_arrival_2(shard, axis, dim):
    pieces = cut_along(shard, dim, lax.axis_size(axis))
    arrived = lax.all_to_all(pieces, axis, split_axis=0, concat_axis=0, tiled=True)
    return arrived.sum(axis=0)


def taken_together(shard, axis):
    return copy_for_each(shard, axis).sum(axis=0)


def convolve(state, fresh_row, kernel):
    window = jnp.concatenate([state, fresh_row[:, None, :]], axis=1)
    summed = jnp.sum(window.astype(jnp.float32) * kernel.astype(jnp.float32)[None], axis=1)
    return (jax.nn.silu(summed), window[:, 1:])


def mixer_block(normed, number, weights):
    (
        gate_weight,
        inner_weight,
        write_weight,
        read_weight,
        step_weight,
        conv_inner,
        conv_write,
        conv_read,
        step_bias,
        decay_log,
        skip_gain,
        group_gain,
        out_weight,
        state_inner,
        state_write,
        state_read,
        recurrent,
    ) = weights

    def partial_of(weight):
        return jnp.dot(normed, weight[number], preferred_element_type=jnp.float32).astype(
            jnp.bfloat16
        )

    summed = side_by_side(
        (
            partial_of(gate_weight),
            partial_of(inner_weight),
            partial_of(write_weight),
            partial_of(read_weight),
            partial_of(step_weight),
        ),
        DP,
        0,
        1,
    )
    gate_raw, inner_raw, write_raw, read_raw, step_raw = [
        member.astype(jnp.bfloat16) for member in summed
    ]
    inner_act, next_inner = convolve(state_inner[number], inner_raw, conv_inner[number])
    write_act, next_write = convolve(state_write[number], write_raw, conv_write[number])
    read_act, next_read = convolve(state_read[number], read_raw, conv_read[number])
    write_all, read_all = gather_turned(
        (write_act.astype(jnp.bfloat16), read_act.astype(jnp.bfloat16)), TP, (1, 1)
    )
    heads_here = step_bias.shape[1]
    head_dim = recurrent.shape[3]
    state_dim = recurrent.shape[4]
    rows_here = inner_act.shape[0]
    first_head = lax.axis_index(TP) * heads_here
    group_index = first_head // (HEADS // GROUPS)
    write_grid = write_all.reshape(rows_here, state_dim, GROUPS)
    read_grid = read_all.reshape(rows_here, state_dim, GROUPS)
    write_vec = lax.dynamic_slice_in_dim(write_grid, group_index, 1, 2)[:, :, 0].astype(jnp.float32)
    read_vec = lax.dynamic_slice_in_dim(read_grid, group_index, 1, 2)[:, :, 0].astype(jnp.float32)
    step_own = lax.dynamic_slice_in_dim(step_raw, first_head, heads_here, 1)
    step_size = jax.nn.softplus(step_own.astype(jnp.float32) + step_bias[number][None, :])
    retain = jnp.exp(-step_size * jnp.exp(decay_log[number])[None, :])
    inner_heads = inner_act.reshape(rows_here, heads_here, head_dim)
    updated = (
        retain[:, :, None, None] * recurrent[number]
        + (step_size[:, :, None] * inner_heads)[:, :, :, None] * write_vec[:, None, None, :]
    )
    readout = jnp.einsum("bhpn,bn->bhp", updated, read_vec, precision=lax.Precision.HIGHEST)
    readout = readout + skip_gain[number][None, :, None] * inner_heads
    gated_out = readout.reshape(rows_here, heads_here * head_dim) * jax.nn.silu(
        gate_raw.astype(jnp.float32)
    )
    selector = (jnp.arange(GROUPS) == group_index).astype(jnp.float32)
    totals = over_axes(jnp.sum(gated_out * gated_out, axis=1)[:, None] * selector[None, :], TP)
    group_sum = jnp.sum(totals * selector[None, :], axis=1, keepdims=True)
    group_factor = lax.rsqrt(group_sum / (HEADS // GROUPS * head_dim) + eps)
    group_normed = (gated_out * group_factor * group_gain[number][None, :]).astype(jnp.bfloat16)
    branch = jnp.dot(
        collect(group_normed, DP, 0), out_weight[number], preferred_element_type=jnp.float32
    )
    return (branch, (next_inner, next_write, next_read, updated))


def columns_over(branch):
    return summed_on_arrival_2(branch, TP, 1)


def local(
    hidden,
    norm_gain,
    gate_weight,
    inner_weight,
    write_weight,
    read_weight,
    step_weight,
    conv_inner,
    conv_write,
    conv_read,
    step_bias,
    decay_log,
    skip_gain,
    group_gain,
    out_weight,
    state_inner,
    state_write,
    state_read,
    recurrent,
):
    weights = (
        gate_weight,
        inner_weight,
        write_weight,
        read_weight,
        step_weight,
        conv_inner,
        conv_write,
        conv_read,
        step_bias,
        decay_log,
        skip_gain,
        group_gain,
        out_weight,
        state_inner,
        state_write,
        state_read,
        recurrent,
    )
    wide_in = hidden.astype(jnp.float32)
    squares = taken_together(jnp.sum(wide_in * wide_in, axis=1, keepdims=True), DP)
    normed = (wide_in * lax.rsqrt(squares / D + eps) * norm_gain[0][None, :]).astype(jnp.bfloat16)
    branch, first_states = mixer_block(normed, 0, weights)
    slice_width = hidden.shape[1] // lax.axis_size(TP)
    offset = lax.axis_index(TP) * slice_width
    own_cols = lax.dynamic_slice_in_dim(wide_in, offset, slice_width, 1)
    middle = (own_cols + columns_over(branch)).astype(jnp.bfloat16).astype(jnp.float32)
    squares = over_axes(jnp.sum(middle * middle, axis=1, keepdims=True), TP_DP)
    gain_slice = lax.dynamic_slice_in_dim(norm_gain[1], offset, slice_width, 0)
    normed_part = (middle * lax.rsqrt(squares / D + eps) * gain_slice[None, :]).astype(jnp.bfloat16)
    normed = collect(normed_part, TP, 1)
    branch, second_states = mixer_block(normed, 1, weights)
    result = collect((middle + columns_over(branch)).astype(jnp.bfloat16), TP, 1)
    stacked = [jnp.stack([earlier, later]) for earlier, later in zip(first_states, second_states)]
    return (result, stacked[0], stacked[1], stacked[2], stacked[3])


def solution(mesh):
    finer = Mesh(mesh.devices.reshape(8, 8, 4, 2), ("tp_0", "tp_1", "dp_0", "dp_1"))
    placed = (
        P(None, DP),
        P(None, DP),
        P(None, DP, TP),
        P(None, DP, TP),
        P(None, DP, TP),
        P(None, DP, TP),
        P(None, DP, None),
        P(None, None, TP),
        P(None, None, TP),
        P(None, None, TP),
        P(None, TP),
        P(None, TP),
        P(None, TP),
        P(None, TP),
        P(None, TP, DP),
        P(None, DP, None, TP),
        P(None, DP, None, TP),
        P(None, DP, None, TP),
        P(None, DP, TP, None, None),
    )
    return jax.shard_map(
        local,
        mesh=finer,
        in_specs=placed,
        out_specs=(
            P(None, DP),
            P(None, DP, None, TP),
            P(None, DP, None, TP),
            P(None, DP, None, TP),
            P(None, DP, TP, None, None),
        ),
        check_vma=False,
    )
```

profile of v0, /device:TPU:2, one launch (start us, length us, event | category | flops | bytes accessed | tf_op | source)
XLA Modules:
  0.0 351.2 jit_solution(7885808371134442058)
XLA Ops:
  0.6 1.0 copy.87
  2.3 9.2 %all-to-all-start = ((f32[8,64,1]{1,2,0:T(1,128)}), f32[8,64,1]{1,2,0:T(1,128)S(1)}, u32[]{:S(2)}, u32[]{:S(2)}) async-start(f32[8,64,1]{1,2,0:T(1,128)} %broadcast_in_dim.24), calls=%async_computation | async-start | bytes 8192 | tf_op jit(solution)/shard_map/all_to_all | solution.py:55
  11.6 0.7 copy-done.12
  12.3 0.7 copy-done.13
  13.0 0.6 copy-done.8
  13.7 1.6 all-to-all-done
  17.7 0.6 copy-done.4
  18.6 0.7 concatenate.30
  19.4 4.7 %all-to-all-start.1 = ((bf16[8,8,448]{2,1,0:T(8,128)(2,1)}), bf16[8,8,448]{2,1,0:T(8,128)(2,1)S(1)}, u32[]{:S(2)}, u32[]{:S(2)}) async-start(bf16[8,8,448]{2,1,0:T(8,128)(2,1)} %bitcast.6), calls=%async_computation.1 | async-start | bytes 131072 | tf_op jit(solution)/shard_map/all_to_all | solution.py:25
  24.1 4.2 %all-to-all-done.1 = bf16[8,8,448]{2,1,0:T(8,128)(2,1)S(1)} async-done(((bf16[8,8,448]{2,1,0:T(8,128)(2,1)}), bf16[8,8,448]{2,1,0:T(8,128)(2,1)S(1)}, u32[]{:S(2)}, u32[]{:S(2)}) %all-to-all-start.1) | async-done | bytes 57376 | tf_op jit(solution)/shard_map/all_to_all | solution.py:25
  28.6 52.7 %all-gather = bf16[64,32,16]{1,2,0:T(8,128)(2,1)S(1)} all-gather(bf16[1,32,16]{1,2,0:T(8,128)(2,1)S(1)} %maximum_bitcast_fusion), channel_id=1, replica_groups=mesh['tp_0'=8,'tp_1'=8,'dp_0'=4,'dp_1'=2] {'tp_0','tp_1'}, dimensions={0}, use_global_device_ids=true | all-gather | bytes 66560 | tf_op jit(solution)/shard_map/all_gather | solution.py:39
  82.8 0.8 fusion.4
  84.0 15.9 %psum.56 = f32[8,16]{1,0:T(8,128)S(1)} all-reduce(f32[8,16]{1,0:T(8,128)S(1)} %broadcast_multiply_fusion.3), channel_id=1, replica_groups=mesh['tp_0'=8,'tp_1'=8,'dp_0'=4,'dp_1'=2] {'tp_0'}, use_global_device_ids=true, to_apply=%region_7.8 | all-reduce | flops 128 | bytes 1024 | tf_op jit(solution)/shard_map/psum | solution.py:49
  99.9 15.6 %psum.57 = f32[8,16]{1,0:T(8,128)S(1)} all-reduce(f32[8,16]{1,0:T(8,128)S(1)} %psum.56), channel_id=1, replica_groups=mesh['tp_0'=8,'tp_1'=8,'dp_0'=4,'dp_1'=2] {'tp_1'}, use_global_device_ids=true, to_apply=%region_8.9 | all-reduce | flops 128 | bytes 1024 | tf_op jit(solution)/shard_map/psum | solution.py:49
  115.7 0.6 broadcast_in_dim.28
  116.3 4.7 %all-to-all-start.2 = ((bf16[8,8,128]{2,1,0:T(8,128)(2,1)}), bf16[8,8,128]{2,1,0:T(8,128)(2,1)S(1)}, u32[]{:S(2)}, u32[]{:S(2)}) async-start(bf16[8,8,128]{2,1,0:T(8,128)(2,1)} %broadcast_in_dim.28), calls=%async_computation.2 | async-start | bytes 32768 | tf_op jit(solution)/shard_map/all_to_all | solution.py:55
  121.1 3.8 %all-to-all-done.2 = bf16[8,8,128]{2,1,0:T(8,128)(2,1)S(1)} async-done(((bf16[8,8,128]{2,1,0:T(8,128)(2,1)}), bf16[8,8,128]{2,1,0:T(8,128)(2,1)S(1)}, u32[]{:S(2)}, u32[]{:S(2)}) %all-to-all-start.2) | async-done | bytes 16416 | tf_op jit(solution)/shard_map/all_to_all | solution.py:55
  125.3 0.8 reshape.185
  126.2 7.3 %all-to-all-start.3 = ((f32[64,1,512]{2,1,0:T(1,128)}), f32[64,1,512]{2,1,0:T(1,128)S(1)}, u32[]{:S(2)}, u32[]{:S(2)}) async-start(f32[64,1,512]{2,1,0:T(1,128)} %reshape.185), calls=%async_computation.3 | async-start | bytes 262144 | tf_op jit(solution)/shard_map/all_to_all | solution.py:73
  133.6 12.6 %all-to-all-done.3 = f32[64,1,512]{2,1,0:T(1,128)S(1)} async-done(((f32[64,1,512]{2,1,0:T(1,128)}), f32[64,1,512]{2,1,0:T(1,128)S(1)}, u32[]{:S(2)}, u32[]{:S(2)}) %all-to-all-start.3) | async-done | bytes 131104 | tf_op jit(solution)/shard_map/all_to_all | solution.py:73
  146.8 1.0 reduce.11
  148.0 14.8 %psum.58 = f32[64,1]{0,1:T(1,128)S(1)} all-reduce(f32[64,1]{0,1:T(1,128)S(1)} %bitcast.277), channel_id=1, replica_groups=mesh['tp_0'=8,'tp_1'=8,'dp_0'=4,'dp_1'=2] {'tp_0'}, use_global_device_ids=true, to_apply=%region_12.13 | all-reduce | flops 64 | bytes 512 | tf_op jit(solution)/shard_map/psum | solution.py:49
  162.7 14.9 %psum.59 = f32[64,1]{0,1:T(1,128)S(1)} all-reduce(f32[64,1]{0,1:T(1,128)S(1)} %psum.58), channel_id=1, replica_groups=mesh['tp_0'=8,'tp_1'=8,'dp_0'=4,'dp_1'=2] {'tp_1'}, use_global_device_ids=true, to_apply=%region_13.14 | all-reduce | flops 64 | bytes 512 | tf_op jit(solution)/shard_map/psum | solution.py:49
  177.6 9.2 %psum.60 = f32[64,1]{0,1:T(1,128)S(1)} all-reduce(f32[64,1]{0,1:T(1,128)S(1)} %psum.59), channel_id=1, replica_groups=mesh['tp_0'=8,'tp_1'=8,'dp_0'=4,'dp_1'=2] {'dp_0'}, use_global_device_ids=true, to_apply=%region_14.15 | all-reduce | flops 64 | bytes 512 | tf_op jit(solution)/shard_map/psum | solution.py:49
  186.8 2.5 psum.61
  189.3 0.8 reshape.187
  190.1 7.4 %all-to-all-start.4 = ((bf16[64,2,256]{2,1,0:T(2,128)(2,1)}), bf16[64,2,256]{2,1,0:T(2,128)(2,1)S(1)}, u32[]{:S(2)}, u32[]{:S(2)}) async-start(bf16[64,2,256]{2,1,0:T(2,128)(2,1)} %reshape.187), calls=%async_computation.4 | async-start | bytes 131072 | tf_op jit(solution)/shard_map/all_to_all | solution.py:55
  197.7 12.1 %all-to-all-done.4 = bf16[64,2,256]{2,1,0:T(2,128)(2,1)S(1)} async-done(((bf16[64,2,256]{2,1,0:T(2,128)(2,1)}), bf16[64,2,256]{2,1,0:T(2,128)(2,1)S(1)}, u32[]{:S(2)}, u32[]{:S(2)}) %all-to-all-start.4) | async-done | bytes 65568 | tf_op jit(solution)/shard_map/all_to_all | solution.py:55
  211.0 0.7 concatenate.35
  211.8 4.4 %all-to-all-start.5 = ((bf16[8,8,448]{2,1,0:T(8,128)(2,1)}), bf16[8,8,448]{2,1,0:T(8,128)(2,1)S(1)}, u32[]{:S(2)}, u32[]{:S(2)}) async-start(bf16[8,8,448]{2,1,0:T(8,128)(2,1)} %bitcast.45), calls=%async_computation.5 | async-start | bytes 131072 | tf_op jit(solution)/shard_map/all_to_all | solution.py:25
  216.2 4.2 %all-to-all-done.5 = bf16[8,8,448]{2,1,0:T(8,128)(2,1)S(1)} async-done(((bf16[8,8,448]{2,1,0:T(8,128)(2,1)}), bf16[8,8,448]{2,1,0:T(8,128)(2,1)S(1)}, u32[]{:S(2)}, u32[]{:S(2)}) %all-to-all-start.5) | async-done | bytes 57376 | tf_op jit(solution)/shard_map/all_to_all | solution.py:25
  220.7 46.9 %all-gather.1 = bf16[64,32,16]{1,2,0:T(8,128)(2,1)S(1)} all-gather(bf16[1,32,16]{1,2,0:T(8,128)(2,1)S(1)} %maximum_bitcast_fusion.1), channel_id=1, replica_groups=mesh['tp_0'=8,'tp_1'=8,'dp_0'=4,'dp_1'=2] {'tp_0','tp_1'}, dimensions={0}, use_global_device_ids=true | all-gather | bytes 66560 | tf_op jit(solution)/shard_map/all_gather | solution.py:39
  269.2 0.8 fusion.1
  270.3 16.7 %psum.62 = f32[8,16]{1,0:T(8,128)S(1)} all-reduce(f32[8,16]{1,0:T(8,128)S(1)} %broadcast_multiply_fusion.2), channel_id=1, replica_groups=mesh['tp_0'=8,'tp_1'=8,'dp_0'=4,'dp_1'=2] {'tp_0'}, use_global_device_ids=true, to_apply=%region_21.22 | all-reduce | flops 128 | bytes 1024 | tf_op jit(solution)/shard_map/psum | solution.py:49
  287.0 14.8 %psum.63 = f32[8,16]{1,0:T(8,128)S(1)} all-reduce(f32[8,16]{1,0:T(8,128)S(1)} %psum.62), channel_id=1, replica_groups=mesh['tp_0'=8,'tp_1'=8,'dp_0'=4,'dp_1'=2] {'tp_1'}, use_global_device_ids=true, to_apply=%region_22.23 | all-reduce | flops 128 | bytes 1024 | tf_op jit(solution)/shard_map/psum | solution.py:49
  302.1 0.6 broadcast_in_dim.34
  302.7 4.7 %all-to-all-start.6 = ((bf16[8,8,128]{2,1,0:T(8,128)(2,1)}), bf16[8,8,128]{2,1,0:T(8,128)(2,1)S(1)}, u32[]{:S(2)}, u32[]{:S(2)}) async-start(bf16[8,8,128]{2,1,0:T(8,128)(2,1)} %broadcast_in_dim.34), calls=%async_computation.6 | async-start | bytes 32768 | tf_op jit(solution)/shard_map/all_to_all | solution.py:55
  307.4 0.6 pad_maximum_fusion.2
  309.2 2.1 all-to-all-done.6
  311.7 0.8 reshape.189
  312.5 6.2 %all-to-all-start.7 = ((f32[64,1,512]{2,1,0:T(1,128)}), f32[64,1,512]{2,1,0:T(1,128)S(1)}, u32[]{:S(2)}, u32[]{:S(2)}) async-start(f32[64,1,512]{2,1,0:T(1,128)} %reshape.189), calls=%async_computation.7 | async-start | bytes 262144 | tf_op jit(solution)/shard_map/all_to_all | solution.py:73
  319.1 12.3 %all-to-all-done.7 = f32[64,1,512]{2,1,0:T(1,128)S(1)} async-done(((f32[64,1,512]{2,1,0:T(1,128)}), f32[64,1,512]{2,1,0:T(1,128)S(1)}, u32[]{:S(2)}, u32[]{:S(2)}) %all-to-all-start.7) | async-done | bytes 131104 | tf_op jit(solution)/shard_map/all_to_all | solution.py:73
  331.4 1.0 reduce.12
  332.7 0.8 reshape.191
  333.4 4.6 %all-to-all-start.8 = ((bf16[64,2,256]{2,1,0:T(2,128)(2,1)}), bf16[64,2,256]{2,1,0:T(2,128)(2,1)S(1)}, u32[]{:S(2)}, u32[]{:S(2)}) async-start(bf16[64,2,256]{2,1,0:T(2,128)(2,1)} %reshape.191), calls=%async_computation.8 | async-start | bytes 131072 | tf_op jit(solution)/shard_map/all_to_all | solution.py:55
  338.1 1.0 pad_maximum_fusion
  339.1 11.2 %all-to-all-done.8 = bf16[64,2,256]{2,1,0:T(2,128)(2,1)S(1)} async-done(((bf16[64,2,256]{2,1,0:T(2,128)(2,1)}), bf16[64,2,256]{2,1,0:T(2,128)(2,1)S(1)}, u32[]{:S(2)}, u32[]{:S(2)}) %all-to-all-start.8) | async-done | bytes 65568 | tf_op jit(solution)/shard_map/all_to_all | solution.py:55
  350.5 0.7 copy.102
  (145 shorter events, 13.3 us)
Async XLA Ops:
  2.3 9.2 %copy-start.14 = (f32[2,2]{1,0:T(2,128)S(1)}, f32[2,2]{1,0:T(2,128)}, u32[]{:S(2)}) copy-start(f32[2,2]{1,0:T(2,128)} %param.31) | copy-start | bytes 52
  2.3 9.2 %copy-start.10 = (f32[2,512]{1,0:T(2,128)S(1)}, f32[2,512]{1,0:T(2,128)}, u32[]{:S(2)}) copy-start(f32[2,512]{1,0:T(2,128)} %param.20) | copy-start | bytes 12292
  2.3 9.3 %copy-start.11 = (bf16[2,4,128]{2,1,0:T(4,128)(2,1)S(1)}, bf16[2,4,128]{2,1,0:T(4,128)(2,1)}, u32[]{:S(2)}) copy-start(bf16[2,4,128]{2,1,0:T(4,128)(2,1)} %param.26) | copy-start | bytes 6148
  2.3 13.0 %all-to-all-start = ((f32[8,64,1]{1,2,0:T(1,128)}), f32[8,64,1]{1,2,0:T(1,128)S(1)}, u32[]{:S(2)}, u32[]{:S(2)}) async-start(f32[8,64,1]{1,2,0:T(1,128)} %broadcast_in_dim.24), calls=%async_computation | async-start | bytes 8192 | tf_op jit(solution)/shard_map/all_to_all | solution.py:55
  11.5 1.4 copy-start.7
  11.6 0.7 copy-start.12
  12.3 0.7 copy-start.13
  12.9 0.7 copy-start.8
  12.9 0.7 copy-start.9
  12.9 0.7 copy-start.16
  12.9 0.7 copy-start.17
  13.0 0.7 copy-start.15
  13.0 2.4 copy-start.6
  15.3 0.8 copy-start.5
  15.3 1.2 copy-start.3
  16.4 1.0 copy-start.2
  17.4 0.9 copy-start.4
  19.4 8.9 %all-to-all-start.1 = ((bf16[8,8,448]{2,1,0:T(8,128)(2,1)}), bf16[8,8,448]{2,1,0:T(8,128)(2,1)S(1)}, u32[]{:S(2)}, u32[]{:S(2)}) async-start(bf16[8,8,448]{2,1,0:T(8,128)(2,1)} %bitcast.6), calls=%async_computation.1 | async-start | bytes 131072 | tf_op jit(solution)/shard_map/all_to_all | solution.py:25
  81.3 1.5 copy-start
  82.8 38.2 %copy-start.1 = (bf16[2,128,512]{2,1,0:T(8,128)(2,1)S(1)}, bf16[2,128,512]{2,1,0:T(8,128)(2,1)}, u32[]{:S(2)}) copy-start(bf16[2,128,512]{2,1,0:T(8,128)(2,1)} %param.33) | copy-start | bytes 786436
  116.3 8.6 %all-to-all-start.2 = ((bf16[8,8,128]{2,1,0:T(8,128)(2,1)}), bf16[8,8,128]{2,1,0:T(8,128)(2,1)S(1)}, u32[]{:S(2)}, u32[]{:S(2)}) async-start(bf16[8,8,128]{2,1,0:T(8,128)(2,1)} %broadcast_in_dim.28), calls=%async_computation.2 | async-start | bytes 32768 | tf_op jit(solution)/shard_map/all_to_all | solution.py:55
  126.2 20.0 %all-to-all-start.3 = ((f32[64,1,512]{2,1,0:T(1,128)}), f32[64,1,512]{2,1,0:T(1,128)S(1)}, u32[]{:S(2)}, u32[]{:S(2)}) async-start(f32[64,1,512]{2,1,0:T(1,128)} %reshape.185), calls=%async_computation.3 | async-start | bytes 262144 | tf_op jit(solution)/shard_map/all_to_all | solution.py:73
  190.1 19.6 %all-to-all-start.4 = ((bf16[64,2,256]{2,1,0:T(2,128)(2,1)}), bf16[64,2,256]{2,1,0:T(2,128)(2,1)S(1)}, u32[]{:S(2)}, u32[]{:S(2)}) async-start(bf16[64,2,256]{2,1,0:T(2,128)(2,1)} %reshape.187), calls=%async_computation.4 | async-start | bytes 131072 | tf_op jit(solution)/shard_map/all_to_all | solution.py:55
  211.8 8.6 %all-to-all-start.5 = ((bf16[8,8,448]{2,1,0:T(8,128)(2,1)}), bf16[8,8,448]{2,1,0:T(8,128)(2,1)S(1)}, u32[]{:S(2)}, u32[]{:S(2)}) async-start(bf16[8,8,448]{2,1,0:T(8,128)(2,1)} %bitcast.45), calls=%async_computation.5 | async-start | bytes 131072 | tf_op jit(solution)/shard_map/all_to_all | solution.py:25
  302.7 8.6 %all-to-all-start.6 = ((bf16[8,8,128]{2,1,0:T(8,128)(2,1)}), bf16[8,8,128]{2,1,0:T(8,128)(2,1)S(1)}, u32[]{:S(2)}, u32[]{:S(2)}) async-start(bf16[8,8,128]{2,1,0:T(8,128)(2,1)} %broadcast_in_dim.34), calls=%async_computation.6 | async-start | bytes 32768 | tf_op jit(solution)/shard_map/all_to_all | solution.py:55
  312.5 18.9 %all-to-all-start.7 = ((f32[64,1,512]{2,1,0:T(1,128)}), f32[64,1,512]{2,1,0:T(1,128)S(1)}, u32[]{:S(2)}, u32[]{:S(2)}) async-start(f32[64,1,512]{2,1,0:T(1,128)} %reshape.189), calls=%async_computation.7 | async-start | bytes 262144 | tf_op jit(solution)/shard_map/all_to_all | solution.py:73
  333.4 16.9 %all-to-all-start.8 = ((bf16[64,2,256]{2,1,0:T(2,128)(2,1)}), bf16[64,2,256]{2,1,0:T(2,128)(2,1)S(1)}, u32[]{:S(2)}, u32[]{:S(2)}) async-start(bf16[64,2,256]{2,1,0:T(2,128)(2,1)} %reshape.191), calls=%async_computation.8 | async-start | bytes 131072 | tf_op jit(solution)/shard_map/all_to_all | solution.py:55
where the time goes:
time: 352 us; the launch traced here: 351 us
  blocking collectives  204 us (58%)
  waiting for transfers between devices  64 us (18%)
  starting transfers between devices  53.2 us (15%)
  local copies, waits for them, and re-layouts  16.8 us (5%)
  other arithmetic  7.6 us (2%)
  matrix products  4.45 us (1%)
    psum x8, blocking collectives, over_axes(): shard = lax.psum(shard, axis)  104 us
    all_gather x2, blocking collectives, gather_turned(): lax.all_gather(both, axis, axis=0, tiled=True)  99.6 us
    all_to_all x5, waiting for transfers between devices, copy_for_each(): lax.all_to_all(jnp.broadcast_to(shard[None], (size, *shard.shape)), axis,...  30.7 us
    all_to_all x5, starting transfers between devices, copy_for_each(): lax.all_to_all(jnp.broadcast_to(shard[None], (size, *shard.shape)), axis,...  30.6 us
    all_to_all x2, waiting for transfers between devices, summed_on_arrival_2(): lax.all_to_all(pieces, axis, split_axis=0, concat_axis=0, tiled=True)  24.9 us
    all_to_all x2, starting transfers between devices, summed_on_arrival_2(): lax.all_to_all(pieces, axis, split_axis=0, concat_axis=0, tiled=True)  13.5 us
    unnamed x52, local copies, waits for them, and re-layouts  9.87 us
    all_to_all x2, starting transfers between devices, summed_on_arrival(): pieces = lax.all_to_all(cut_along(shard, dim, size), axis, 0, 0, tiled=True)  9.12 us
  transfers between devices with their start and end apart: 9, of which 9 were waited for; matrix products, arithmetic and copies ran while one was open for 1% of the time, Pallas kernels for 0%

commit v1 on v0

v1 whole, which is shorter than its diff:
```python
import jax
import jax.numpy as jnp
from jax import lax
from jax.sharding import Mesh
from jax.sharding import PartitionSpec as P

D = 4096
HEADS = 128
GROUPS = 16
DP = ("dp_0", "dp_1")
TP = ("tp_0", "tp_1")
Y = "tp_1"
Z = "tp_0"
YD = ("tp_1", "dp_0", "dp_1")
EPS = 1e-06
BF = jnp.bfloat16
F32 = jnp.float32


def exchange(pieces, axis):
    return lax.all_to_all(pieces, axis, 0, 0, tiled=True)


def to_each(shard, axis):
    return exchange(jnp.broadcast_to(shard[None], (lax.axis_size(axis), *shard.shape)), axis)


def split_two(wide):
    high = lax.reduce_precision(wide, 8, 7)
    return high.astype(BF), (wide - high).astype(BF)


def dot(a, b):
    return jnp.dot(a, b, preferred_element_type=F32)


def unshuffle():
    row = jnp.arange(256)[:, None]
    col = jnp.arange(256)[None, :]
    return (row == (col % 128) // 2 * 4 + col // 128 * 2 + col % 2).astype(BF)


def conv(rows, fresh, taps):
    taps = taps.astype(F32)
    total = fresh.astype(F32) * taps[3][None]
    for k in range(3):
        total = total + rows[:, k].astype(F32) * taps[k][None]
    return jax.nn.silu(total)


def shifted(rows, fresh):
    return jnp.concatenate([rows[:, 1:], fresh[:, None]], axis=1)


def mix(raw, step_raw, inner_act, vectors, bias, decay, skip, recurrent):
    write_vec, read_vec = vectors[0], vectors[1]
    step = jax.nn.softplus(step_raw.astype(F32) + bias[None, :])
    retain = jnp.exp(-step * jnp.exp(decay)[None, :])
    heads = inner_act.reshape(8, 2, 64)
    updated = (
        retain[:, :, None, None] * recurrent
        + (step[:, :, None] * heads)[:, :, :, None] * write_vec[:, None, None, :]
    )
    readout = jnp.sum(updated * read_vec[:, None, None, :], axis=3)
    readout = readout + skip[None, :, None] * heads
    gated = readout.reshape(8, 128) * jax.nn.silu(raw.astype(F32))
    return updated, gated.astype(BF)


def local(
    hidden,
    norm_gain,
    gate_weight,
    inner_weight,
    write_weight,
    read_weight,
    step_weight,
    conv_inner,
    conv_write,
    conv_read,
    step_bias,
    decay_log,
    skip_gain,
    group_gain,
    out_weight,
    state_inner,
    state_write,
    state_read,
    recurrent,
):
    t = lax.axis_index(TP)

    by_feature = out_weight.reshape(2, 128, 8, 64)
    moved = jnp.concatenate([by_feature[0], by_feature[1]], axis=2)
    moved = jnp.moveaxis(moved, 1, 0)
    gain_high, gain_low = split_two(group_gain)
    gains = jnp.stack([gain_high[0], gain_low[0], gain_high[1], gain_low[1]])
    gains = jnp.concatenate([gains, jnp.zeros((4, 128), BF)], axis=0)
    moved = jnp.concatenate([moved, jnp.broadcast_to(gains[None], (8, 8, 128))], axis=1)
    slab = exchange(moved, Y)

    def channel_rows(weight, taps, rows):
        return jnp.concatenate(
            [weight[1].T, taps[1].T, rows[1].reshape(24, 32).T, jnp.zeros((32, 92), BF)], axis=1
        )

    later = jnp.stack(
        [
            channel_rows(write_weight, conv_write, state_write),
            channel_rows(read_weight, conv_read, state_read),
        ]
    )

    def project(wide, number, extra):
        scaled = (wide * norm_gain[number][None, :]).astype(BF)
        squares = jnp.sum(wide * wide, axis=1, keepdims=True)
        high, low = split_two(squares)
        step_own = lax.dynamic_slice_in_dim(step_weight[number], 2 * t, 2, 1)
        parts = [
            dot(scaled, gate_weight[number]).astype(BF),
            dot(scaled, inner_weight[number]).astype(BF),
            dot(scaled, write_weight[number]).astype(BF),
            dot(scaled, read_weight[number]).astype(BF),
            dot(scaled, step_own).astype(BF),
            high,
            low,
            jnp.zeros((64, 60), BF),
        ]
        if extra is not None:
            parts.append(
                lax.dot_general(
                    scaled, extra, (((1,), (1,)), ((), ())), preferred_element_type=F32
                ).astype(BF)
            )
        both = jnp.concatenate(parts, axis=1)
        got = exchange(both.reshape(8, 8, -1), DP)
        total = jnp.sum(got.astype(F32), axis=0)
        factor = lax.rsqrt((total[:, 322:323] + total[:, 323:324]) / D + EPS)
        return (total * factor).astype(BF)

    def finish(gated, number, own):
        got = to_each(gated, YD).reshape(8, 64, 128).astype(F32)
        squares = jnp.sum(got * got, axis=2)
        group = jnp.sum(squares.reshape(2, 4, 64), axis=1)
        factor = lax.rsqrt(group / 512 + EPS)
        factor = jnp.broadcast_to(factor[:, None], (2, 4, 64)).reshape(8, 64)
        gain = slab[:, 128 + 2 * number].astype(F32) + slab[:, 129 + 2 * number].astype(F32)
        normed = (got * factor[:, :, None] * gain[:, None, :]).astype(BF)
        normed = jnp.moveaxis(normed, 0, 1).reshape(64, 1024)
        weight = slab[:, :128, 64 * number : 64 * number + 64].reshape(1024, 64)
        part = dot(normed, weight).astype(BF)
        part = jnp.concatenate([part[:32], part[32:]], axis=1)
        pieces = to_each(part, Z)
        own = (own.astype(F32) + jnp.sum(pieces.astype(F32), axis=0)).astype(BF)
        blocks = to_each(own, Y)
        blocks = jnp.concatenate([blocks[:, :, :64], blocks[:, :, 64:]], axis=1)
        return jnp.moveaxis(blocks, 0, 1).reshape(64, 512), own

    order = unshuffle()

    wide = hidden.astype(F32)
    raw = project(wide, 0, None)
    gate0, inner0, write0, read0, step0 = (
        raw[:, :128],
        raw[:, 128:256],
        raw[:, 256:288],
        raw[:, 288:320],
        raw[:, 320:322],
    )
    write_act = conv(state_write[0], write0, conv_write[0]).astype(BF)
    read_act = conv(state_read[0], read0, conv_read[0]).astype(BF)
    acts = jnp.stack([write_act.T, read_act.T])
    message = jnp.concatenate(
        [later[:, :, :512], acts, later[:, :, 512:540], jnp.zeros((2, 32, 92), BF)], axis=2
    )
    message = jnp.transpose(message.reshape(2, 2, 16, 640), (2, 0, 1, 3)).reshape(16, 1, 4, 640)
    message = jnp.broadcast_to(message, (16, 4, 4, 640)).reshape(64, 4, 640)
    got = exchange(message, TP).reshape(256, 640)
    vectors = lax.dot_general(
        got[:, 512:520], order, (((0,), (0,)), ((), ())), preferred_element_type=F32
    )
    later_weight = got[:, :512]
    later_taps = got[:, 520:524].T
    later_rows = got[:, 524:548].T.reshape(8, 3, 256)
    inner_act = conv(state_inner[0], inner0, conv_inner[0])
    updated0, gated = mix(
        gate0,
        step0,
        inner_act,
        (vectors[:, :128], vectors[:, 128:]),
        step_bias[0],
        decay_log[0],
        skip_gain[0],
        recurrent[0],
    )
    own = lax.dynamic_slice_in_dim(hidden, 64 * lax.axis_index(Y), 64, 1)
    own = jnp.concatenate([own[:32], own[32:]], axis=1)
    middle, own = finish(gated, 0, own)

    wide = middle.astype(F32)
    raw = project(wide, 1, later_weight)
    gate1, inner1, write1, read1, step1, group1 = (
        raw[:, :128],
        raw[:, 128:256],
        raw[:, 256:288],
        raw[:, 288:320],
        raw[:, 320:322],
        raw[:, 384:],
    )
    acts = conv(later_rows, group1, later_taps).astype(BF)
    vectors = dot(acts, order)
    inner_act = conv(state_inner[1], inner1, conv_inner[1])
    updated1, gated = mix(
        gate1,
        step1,
        inner_act,
        (vectors[:, :128], vectors[:, 128:]),
        step_bias[1],
        decay_log[1],
        skip_gain[1],
        recurrent[1],
    )
    result, _ = finish(gated, 1, own)

    return (
        result,
        jnp.stack([shifted(state_inner[0], inner0), shifted(state_inner[1], inner1)]),
        jnp.stack([shifted(state_write[0], write0), shifted(state_write[1], write1)]),
        jnp.stack([shifted(state_read[0], read0), shifted(state_read[1], read1)]),
        jnp.stack([updated0, updated1]),
    )


def solution(mesh):
    finer = Mesh(mesh.devices.reshape(8, 8, 4, 2), ("tp_0", "tp_1", "dp_0", "dp_1"))
    placed = (
        P(None, DP),
        P(None, DP),
        P(None, DP, TP),
        P(None, DP, TP),
        P(None, DP, TP),
        P(None, DP, TP),
        P(None, DP, None),
        P(None, None, TP),
        P(None, None, TP),
        P(None, None, TP),
        P(None, TP),
        P(None, TP),
        P(None, TP),
        P(None, TP),
        P(None, TP, DP),
        P(None, DP, None, TP),
        P(None, DP, None, TP),
        P(None, DP, None, TP),
        P(None, DP, TP, None, None),
    )
    return jax.shard_map(
        local,
        mesh=finer,
        in_specs=placed,
        out_specs=(
            P(None, DP),
            P(None, DP, None, TP),
            P(None, DP, None, TP),
            P(None, DP, None, TP),
            P(None, DP, TP, None, None),
        ),
        check_vma=False,
    )
```

time: 352 us -> 165 us (0.47)
  the two profiles are of different devices: /device:TPU:2 before, /device:TPU:8 now
where the time goes in v1:
time: 165 us; the launch traced here: 164 us
  waiting for transfers between devices  78.7 us (48%)
  starting transfers between devices  55.9 us (34%)
  local copies, waits for them, and re-layouts  15.8 us (10%)
  other arithmetic  7.85 us (5%)
  matrix products  4.26 us (3%)
    all_to_all x10, waiting for transfers between devices, exchange(): return lax.all_to_all(pieces, axis, 0, 0, tiled=True)  78.7 us
    all_to_all x10, starting transfers between devices, exchange(): return lax.all_to_all(pieces, axis, 0, 0, tiled=True)  55.9 us
    broadcast_in_dim x6, local copies, waits for them, and re-layouts, to_each(): jnp.broadcast_to(shard[None], (lax.axis_size(axis), *shard.shape))  3.94 us
    dot_general x13, matrix products, dot(): return jnp.dot(a, b, preferred_element_type=F32)  3.88 us
  transfers between devices with their start and end apart: 10, of which 10 were waited for; matrix products, arithmetic and copies ran while one was open for 4% of the time, Pallas kernels for 0%

profile of v1, /device:TPU:8, one launch (start us, length us, event | category | flops | bytes accessed | tf_op | source)
XLA Modules:
  0.0 163.9 jit_solution(7133615477975762874)
XLA Ops:
  0.7 1.0 fusion.26
  1.7 0.8 fusion.121
  2.6 0.9 convolution_convert_fusion.8
  3.6 0.9 convolution_convert_fusion.7
  5.5 0.3 convolution_convert_fusion.10
  6.0 0.7 concatenate.97
  6.7 4.4 %all-to-all-start = ((bf16[8,8,384]{2,1,0:T(8,128)(2,1)}), bf16[8,8,384]{2,1,0:T(8,128)(2,1)S(1)}, u32[]{:S(2)}, u32[]{:S(2)}) async-start(bf16[8,8,384]{2,1,0:T(8,128)(2,1)} %concatenate.97), calls=%async_computation | async-start | bytes 98304 | tf_op jit(solution)/shard_map/all_to_all | solution.py:21
  11.5 0.5 copy-done.8
  12.2 0.6 copy-done.9
  13.4 0.6 copy-done.16
  14.9 0.9 copy.176
  15.8 0.8 all-to-all-done
  16.7 8.1 %all-to-all-start.3 = ((bf16[8,136,128]{2,1,0:T(8,128)(2,1)}), bf16[8,136,128]{2,1,0:T(8,128)(2,1)S(1)}, u32[]{:S(2)}, u32[]{:S(2)}) async-start(bf16[8,136,128]{2,1,0:T(8,128)(2,1)} %copy.176), calls=%async_computation.3 | async-start | bytes 557056 | tf_op jit(solution)/shard_map/all_to_all | solution.py:21
  25.7 10.1 %all-to-all-done.3 = bf16[8,136,128]{2,1,0:T(8,128)(2,1)S(1)} async-done(((bf16[8,136,128]{2,1,0:T(8,128)(2,1)}), bf16[8,136,128]{2,1,0:T(8,128)(2,1)S(1)}, u32[]{:S(2)}, u32[]{:S(2)}) %all-to-all-start.3) | async-done | bytes 278560 | tf_op jit(solution)/shard_map/all_to_all | solution.py:21
  35.7 0.8 broadcast_in_dim.40
  36.6 11.5 %all-to-all-start.1 = ((bf16[64,4,640]{2,1,0:T(4,128)(2,1)}), bf16[64,4,640]{2,1,0:T(4,128)(2,1)S(1)}, u32[]{:S(2)}, u32[]{:S(2)}) async-start(bf16[64,4,640]{2,1,0:T(4,128)(2,1)} %bitcast.57), calls=%async_computation.1 | async-start | bytes 655360 | tf_op jit(solution)/shard_map/all_to_all | solution.py:21
  48.2 14.9 %all-to-all-done.1 = bf16[64,4,640]{2,1,0:T(4,128)(2,1)S(1)} async-done(((bf16[64,4,640]{2,1,0:T(4,128)(2,1)}), bf16[64,4,640]{2,1,0:T(4,128)(2,1)S(1)}, u32[]{:S(2)}, u32[]{:S(2)}) %all-to-all-start.1) | async-done | bytes 327712 | tf_op jit(solution)/shard_map/all_to_all | solution.py:21
  63.3 0.4 fusion.12
  63.9 0.7 broadcast_in_dim.41
  64.6 7.0 %all-to-all-start.2 = ((bf16[64,8,128]{2,1,0:T(8,128)(2,1)}), bf16[64,8,128]{2,1,0:T(8,128)(2,1)S(1)}, u32[]{:S(2)}, u32[]{:S(2)}) async-start(bf16[64,8,128]{2,1,0:T(8,128)(2,1)} %broadcast_in_dim.41), calls=%async_computation.2 | async-start | bytes 262144 | tf_op jit(solution)/shard_map/all_to_all | solution.py:21
  71.8 9.9 %all-to-all-done.2 = bf16[64,8,128]{2,1,0:T(8,128)(2,1)S(1)} async-done(((bf16[64,8,128]{2,1,0:T(8,128)(2,1)}), bf16[64,8,128]{2,1,0:T(8,128)(2,1)S(1)}, u32[]{:S(2)}, u32[]{:S(2)}) %all-to-all-start.2) | async-done | bytes 131104 | tf_op jit(solution)/shard_map/all_to_all | solution.py:21
  82.5 0.6 broadcast_in_dim.45
  83.1 3.4 %all-to-all-start.4 = ((bf16[8,32,128]{2,1,0:T(8,128)(2,1)}), bf16[8,32,128]{2,1,0:T(8,128)(2,1)S(1)}, u32[]{:S(2)}, u32[]{:S(2)}) async-start(bf16[8,32,128]{2,1,0:T(8,128)(2,1)} %broadcast_in_dim.45), calls=%async_computation.4 | async-start | bytes 131072 | tf_op jit(solution)/shard_map/all_to_all | solution.py:21
  86.6 8.2 %all-to-all-done.4 = bf16[8,32,128]{2,1,0:T(8,128)(2,1)S(1)} async-done(((bf16[8,32,128]{2,1,0:T(8,128)(2,1)}), bf16[8,32,128]{2,1,0:T(8,128)(2,1)S(1)}, u32[]{:S(2)}, u32[]{:S(2)}) %all-to-all-start.4) | async-done | bytes 65568 | tf_op jit(solution)/shard_map/all_to_all | solution.py:21
  94.9 0.6 broadcast_in_dim.46
  95.5 4.6 %all-to-all-start.5 = ((bf16[8,32,128]{2,1,0:T(8,128)(2,1)}), bf16[8,32,128]{2,1,0:T(8,128)(2,1)S(1)}, u32[]{:S(2)}, u32[]{:S(2)}) async-start(bf16[8,32,128]{2,1,0:T(8,128)(2,1)} %broadcast_in_dim.46), calls=%async_computation.5 | async-start | bytes 131072 | tf_op jit(solution)/shard_map/all_to_all | solution.py:21
  100.1 6.9 %all-to-all-done.5 = bf16[8,32,128]{2,1,0:T(8,128)(2,1)S(1)} async-done(((bf16[8,32,128]{2,1,0:T(8,128)(2,1)}), bf16[8,32,128]{2,1,0:T(8,128)(2,1)S(1)}, u32[]{:S(2)}, u32[]{:S(2)}) %all-to-all-start.5) | async-done | bytes 65568 | tf_op jit(solution)/shard_map/all_to_all | solution.py:21
  109.6 0.8 concatenate.112
  110.3 3.4 %all-to-all-start.6 = ((bf16[8,8,640]{2,1,0:T(8,128)(2,1)}), bf16[8,8,640]{2,1,0:T(8,128)(2,1)S(1)}, u32[]{:S(2)}, u32[]{:S(2)}) async-start(bf16[8,8,640]{2,1,0:T(8,128)(2,1)} %concatenate.112), calls=%async_computation.6 | async-start | bytes 163840 | tf_op jit(solution)/shard_map/all_to_all | solution.py:21
  113.7 0.4 slice_reduce_fusion.3
  114.1 5.3 %all-to-all-done.6 = bf16[8,8,640]{2,1,0:T(8,128)(2,1)S(1)} async-done(((bf16[8,8,640]{2,1,0:T(8,128)(2,1)}), bf16[8,8,640]{2,1,0:T(8,128)(2,1)S(1)}, u32[]{:S(2)}, u32[]{:S(2)}) %all-to-all-start.6) | async-done | bytes 81952 | tf_op jit(solution)/shard_map/all_to_all | solution.py:21
  120.1 0.4 multiply_add_fusion.1
  120.5 0.4 fusion.9
  121.0 0.7 broadcast_in_dim.47
  121.7 5.5 %all-to-all-start.7 = ((bf16[64,8,128]{2,1,0:T(8,128)(2,1)}), bf16[64,8,128]{2,1,0:T(8,128)(2,1)S(1)}, u32[]{:S(2)}, u32[]{:S(2)}) async-start(bf16[64,8,128]{2,1,0:T(8,128)(2,1)} %broadcast_in_dim.47), calls=%async_computation.7 | async-start | bytes 262144 | tf_op jit(solution)/shard_map/all_to_all | solution.py:21
  127.3 1.1 pad_maximum_fusion
  128.4 0.6 pad_maximum_fusion.3
  129.1 8.5 %all-to-all-done.7 = bf16[64,8,128]{2,1,0:T(8,128)(2,1)S(1)} async-done(((bf16[64,8,128]{2,1,0:T(8,128)(2,1)}), bf16[64,8,128]{2,1,0:T(8,128)(2,1)S(1)}, u32[]{:S(2)}, u32[]{:S(2)}) %all-to-all-start.7) | async-done | bytes 131104 | tf_op jit(solution)/shard_map/all_to_all | solution.py:21
  138.0 0.3 fusion.2
  138.4 0.6 broadcast_in_dim.49
  139.0 3.4 %all-to-all-start.8 = ((bf16[8,32,128]{2,1,0:T(8,128)(2,1)}), bf16[8,32,128]{2,1,0:T(8,128)(2,1)S(1)}, u32[]{:S(2)}, u32[]{:S(2)}) async-start(bf16[8,32,128]{2,1,0:T(8,128)(2,1)} %broadcast_in_dim.49), calls=%async_computation.8 | async-start | bytes 131072 | tf_op jit(solution)/shard_map/all_to_all | solution.py:21
  142.4 0.6 pad_maximum_fusion.5
  143.0 7.7 %all-to-all-done.8 = bf16[8,32,128]{2,1,0:T(8,128)(2,1)S(1)} async-done(((bf16[8,32,128]{2,1,0:T(8,128)(2,1)}), bf16[8,32,128]{2,1,0:T(8,128)(2,1)S(1)}, u32[]{:S(2)}, u32[]{:S(2)}) %all-to-all-start.8) | async-done | bytes 65568 | tf_op jit(solution)/shard_map/all_to_all | solution.py:21
  150.7 0.6 broadcast_in_dim.50
  151.4 4.6 %all-to-all-start.9 = ((bf16[8,32,128]{2,1,0:T(8,128)(2,1)}), bf16[8,32,128]{2,1,0:T(8,128)(2,1)S(1)}, u32[]{:S(2)}, u32[]{:S(2)}) async-start(bf16[8,32,128]{2,1,0:T(8,128)(2,1)} %broadcast_in_dim.50), calls=%async_computation.9 | async-start | bytes 131072 | tf_op jit(solution)/shard_map/all_to_all | solution.py:21
  156.0 0.6 pad_maximum_fusion.4
  156.6 6.3 %all-to-all-done.9 = bf16[8,32,128]{2,1,0:T(8,128)(2,1)S(1)} async-done(((bf16[8,32,128]{2,1,0:T(8,128)(2,1)}), bf16[8,32,128]{2,1,0:T(8,128)(2,1)S(1)}, u32[]{:S(2)}, u32[]{:S(2)}) %all-to-all-start.9) | async-done | bytes 65568 | tf_op jit(solution)/shard_map/all_to_all | solution.py:21
  163.2 0.8 reshape.445
  (184 shorter events, 9.7 us)
Async XLA Ops:
  0.6 1.9 %copy-start.1 = (bf16[64,512]{1,0:T(8,128)(2,1)S(1)}, bf16[64,512]{1,0:T(8,128)(2,1)}, u32[]{:S(2)}) copy-start(bf16[64,512]{1,0:T(8,128)(2,1)} %param.19) | copy-start | bytes 196612
  0.6 4.1 %copy-start.4 = (bf16[2,512,128]{2,1,0:T(8,128)(2,1)S(1)}, bf16[2,512,128]{2,1,0:T(8,128)(2,1)}, u32[]{:S(2)}) copy-start(bf16[2,512,128]{2,1,0:T(8,128)(2,1)} %param.22) | copy-start | bytes 786436
  2.6 2.4 %copy-start.5 = (bf16[2,512,128]{2,1,0:T(8,128)(2,1)S(1)}, bf16[2,512,128]{2,1,0:T(8,128)(2,1)}, u32[]{:S(2)}) copy-start(bf16[2,512,128]{2,1,0:T(8,128)(2,1)} %param.21) | copy-start | bytes 786436
  4.5 1.0 copy-start.2
  5.9 5.3 %copy-start.6 = (bf16[2,512,32]{1,2,0:T(8,128)(2,1)S(1)}, bf16[2,512,32]{1,2,0:T(8,128)(2,1)}, u32[]{:S(2)}) copy-start(bf16[2,512,32]{1,2,0:T(8,128)(2,1)} %param.24) | copy-start | bytes 196612
  5.9 5.2 %copy-start.7 = (bf16[2,512,32]{1,2,0:T(8,128)(2,1)S(1)}, bf16[2,512,32]{1,2,0:T(8,128)(2,1)}, u32[]{:S(2)}) copy-start(bf16[2,512,32]{1,2,0:T(8,128)(2,1)} %param.23) | copy-start | bytes 196612
  5.9 5.3 %copy-start.14 = (f32[2,2]{1,0:T(2,128)S(1)}, f32[2,2]{1,0:T(2,128)}, u32[]{:S(2)}) copy-start(f32[2,2]{1,0:T(2,128)} %param.31) | copy-start | bytes 52
  5.9 5.3 %copy-start.15 = (f32[2,128]{1,0:T(2,128)S(1)}, f32[2,128]{1,0:T(2,128)}, u32[]{:S(2)}) copy-start(f32[2,128]{1,0:T(2,128)} %param.32) | copy-start | bytes 3076
  5.9 5.3 %copy-start.12 = (bf16[2,4,32]{2,1,0:T(4,128)(2,1)S(1)}, bf16[2,4,32]{2,1,0:T(4,128)(2,1)}, u32[]{:S(2)}) copy-start(bf16[2,4,32]{2,1,0:T(4,128)(2,1)} %param.27) | copy-start | bytes 1540
  5.9 5.3 %copy-start.13 = (bf16[2,4,32]{2,1,0:T(4,128)(2,1)S(1)}, bf16[2,4,32]{2,1,0:T(4,128)(2,1)}, u32[]{:S(2)}) copy-start(bf16[2,4,32]{2,1,0:T(4,128)(2,1)} %param.28) | copy-start | bytes 1540
  5.9 5.3 %copy-start.11 = (bf16[2,4,128]{2,1,0:T(4,128)(2,1)S(1)}, bf16[2,4,128]{2,1,0:T(4,128)(2,1)}, u32[]{:S(2)}) copy-start(bf16[2,4,128]{2,1,0:T(4,128)(2,1)} %param.26) | copy-start | bytes 6148
  6.7 6.3 %copy-start.3 = (bf16[2,128,512]{2,1,0:T(8,128)(2,1)S(1)}, bf16[2,128,512]{2,1,0:T(8,128)(2,1)}, u32[]{:S(2)}) copy-start(bf16[2,128,512]{2,1,0:T(8,128)(2,1)} %param.33) | copy-start | bytes 786436
  6.7 10.0 %all-to-all-start = ((bf16[8,8,384]{2,1,0:T(8,128)(2,1)}), bf16[8,8,384]{2,1,0:T(8,128)(2,1)S(1)}, u32[]{:S(2)}, u32[]{:S(2)}) async-start(bf16[8,8,384]{2,1,0:T(8,128)(2,1)} %concatenate.97), calls=%async_computation | async-start | bytes 98304 | tf_op jit(solution)/shard_map/all_to_all | solution.py:21
  11.3 0.7 copy-start.8
  12.1 0.7 copy-start.9
  12.1 0.7 copy-start.10
  13.3 0.7 copy-start.16
  13.3 0.7 copy-start.17
  16.7 19.1 %all-to-all-start.3 = ((bf16[8,136,128]{2,1,0:T(8,128)(2,1)}), bf16[8,136,128]{2,1,0:T(8,128)(2,1)S(1)}, u32[]{:S(2)}, u32[]{:S(2)}) async-start(bf16[8,136,128]{2,1,0:T(8,128)(2,1)} %copy.176), calls=%async_computation.3 | async-start | bytes 557056 | tf_op jit(solution)/shard_map/all_to_all | solution.py:21
  25.5 37.8 %copy-start = (f32[2,8,2,64,128]{4,3,2,1,0:T(8,128)S(1)}, f32[2,8,2,64,128]{4,3,2,1,0:T(8,128)}, u32[]{:S(2)}) copy-start(f32[2,8,2,64,128]{4,3,2,1,0:T(8,128)} %param.37) | copy-start | bytes 3145732
  36.6 26.5 %all-to-all-start.1 = ((bf16[64,4,640]{2,1,0:T(4,128)(2,1)}), bf16[64,4,640]{2,1,0:T(4,128)(2,1)S(1)}, u32[]{:S(2)}, u32[]{:S(2)}) async-start(bf16[64,4,640]{2,1,0:T(4,128)(2,1)} %bitcast.57), calls=%async_computation.1 | async-start | bytes 655360 | tf_op jit(solution)/shard_map/all_to_all | solution.py:21
  64.6 17.2 %all-to-all-start.2 = ((bf16[64,8,128]{2,1,0:T(8,128)(2,1)}), bf16[64,8,128]{2,1,0:T(8,128)(2,1)S(1)}, u32[]{:S(2)}, u32[]{:S(2)}) async-start(bf16[64,8,128]{2,1,0:T(8,128)(2,1)} %broadcast_in_dim.41), calls=%async_computation.2 | async-start | bytes 262144 | tf_op jit(solution)/shard_map/all_to_all | solution.py:21
  83.1 11.7 %all-to-all-start.4 = ((bf16[8,32,128]{2,1,0:T(8,128)(2,1)}), bf16[8,32,128]{2,1,0:T(8,128)(2,1)S(1)}, u32[]{:S(2)}, u32[]{:S(2)}) async-start(bf16[8,32,128]{2,1,0:T(8,128)(2,1)} %broadcast_in_dim.45), calls=%async_computation.4 | async-start | bytes 131072 | tf_op jit(solution)/shard_map/all_to_all | solution.py:21
  95.5 11.5 %all-to-all-start.5 = ((bf16[8,32,128]{2,1,0:T(8,128)(2,1)}), bf16[8,32,128]{2,1,0:T(8,128)(2,1)S(1)}, u32[]{:S(2)}, u32[]{:S(2)}) async-start(bf16[8,32,128]{2,1,0:T(8,128)(2,1)} %broadcast_in_dim.46), calls=%async_computation.5 | async-start | bytes 131072 | tf_op jit(solution)/shard_map/all_to_all | solution.py:21
  110.3 9.0 %all-to-all-start.6 = ((bf16[8,8,640]{2,1,0:T(8,128)(2,1)}), bf16[8,8,640]{2,1,0:T(8,128)(2,1)S(1)}, u32[]{:S(2)}, u32[]{:S(2)}) async-start(bf16[8,8,640]{2,1,0:T(8,128)(2,1)} %concatenate.112), calls=%async_computation.6 | async-start | bytes 163840 | tf_op jit(solution)/shard_map/all_to_all | solution.py:21
  121.7 15.9 %all-to-all-start.7 = ((bf16[64,8,128]{2,1,0:T(8,128)(2,1)}), bf16[64,8,128]{2,1,0:T(8,128)(2,1)S(1)}, u32[]{:S(2)}, u32[]{:S(2)}) async-start(bf16[64,8,128]{2,1,0:T(8,128)(2,1)} %broadcast_in_dim.47), calls=%async_computation.7 | async-start | bytes 262144 | tf_op jit(solution)/shard_map/all_to_all | solution.py:21
  139.0 11.7 %all-to-all-start.8 = ((bf16[8,32,128]{2,1,0:T(8,128)(2,1)}), bf16[8,32,128]{2,1,0:T(8,128)(2,1)S(1)}, u32[]{:S(2)}, u32[]{:S(2)}) async-start(bf16[8,32,128]{2,1,0:T(8,128)(2,1)} %broadcast_in_dim.49), calls=%async_computation.8 | async-start | bytes 131072 | tf_op jit(solution)/shard_map/all_to_all | solution.py:21
  151.4 11.6 %all-to-all-start.9 = ((bf16[8,32,128]{2,1,0:T(8,128)(2,1)}), bf16[8,32,128]{2,1,0:T(8,128)(2,1)S(1)}, u32[]{:S(2)}, u32[]{:S(2)}) async-start(bf16[8,32,128]{2,1,0:T(8,128)(2,1)} %broadcast_in_dim.50), calls=%async_computation.9 | async-start | bytes 131072 | tf_op jit(solution)/shard_map/all_to_all | solution.py:21

commit v2 on v0

v2 whole, which is shorter than its diff:
```python
import functools

import jax
import jax.numpy as jnp
from jax import lax
from jax.experimental import pallas as pl
from jax.experimental.pallas import tpu as pltpu
from jax.sharding import Mesh
from jax.sharding import PartitionSpec as P

D = 4096
DP = ("dp_0", "dp_1")
TP = ("tp_0", "tp_1")
EPS = 1e-06
BF = jnp.bfloat16
F32 = jnp.float32


def iota(shape, dim):
    return lax.broadcasted_iota(jnp.int32, shape, dim)


def dot(a, b):
    return lax.dot_general(a, b, (((1,), (0,)), ((), ())), preferred_element_type=F32)


def dot_rows(a, b):
    return lax.dot_general(a, b, (((1,), (1,)), ((), ())), preferred_element_type=F32)


def silu(a):
    return a * (1.0 / (1.0 + jnp.exp(-a)))


def rounded(a):
    return a.astype(BF).astype(F32)


def project(t, wide, gain, gate_w, inner_w, write_w, read_w, step_w, extra):
    scaled = (wide * gain).astype(BF)
    squares = jnp.sum(wide * wide, axis=1, keepdims=True)
    high = rounded(squares)
    vectors = dot_rows(scaled, jnp.concatenate([write_w, read_w], axis=0))
    step = dot(scaled, step_w).astype(BF)
    row, col = iota((128, 128), 0), iota((128, 128), 1)
    mine = ((col - 64 == row - 2 * t) & (col >= 64) & (col < 66)).astype(F32).astype(BF)
    lane = iota((64, 128), 1)
    third = jnp.concatenate([vectors, jnp.zeros((64, 64), F32)], axis=1) + dot(step, mine)
    third = jnp.where(lane == 66, high, jnp.where(lane == 67, squares - high, third))
    parts = [dot(scaled, gate_w), dot(scaled, inner_w), third]
    if extra is not None:
        parts.append(dot_rows(scaled, extra))
    return jnp.concatenate(parts, axis=1).astype(BF)


def first_project(t, hidden, gain, gate_w, inner_w, write_w, read_w, step_w):
    out = project(
        t, hidden.astype(F32), gain[0:1], gate_w[0], inner_w[0], write_w[0], read_w[0], step_w[0], None
    )
    pick = (iota((8, 512), 1) == iota((8, 512), 0) + 8 * t).astype(F32).astype(BF)
    own = jnp.concatenate([dot_rows(pick, hidden), jnp.zeros((8, 64), F32)], axis=1)
    return out, own


def turned_back(got):
    return jnp.transpose(got.reshape(512, 128).astype(F32))[:64]


def second_project(t, got, gain, gate_w, inner_w, write_w, read_w, step_w, later):
    wide = turned_back(got)
    return (
        project(
            t, wide, gain[1:2], gate_w[1], inner_w[1], write_w[1], read_w[1], step_w[1], later[:, :512]
        ),
    )


def arrive(got):
    total = got[0].astype(F32)
    for k in range(1, 8):
        total = total + got[k].astype(F32)
    squares = total[:, 322:323] + total[:, 323:324]
    return (total * lax.rsqrt(squares / D + EPS)).astype(BF)


def convolve(rows, fresh, taps):
    total = fresh.astype(F32) * taps[3:4].astype(F32)
    for k in range(3):
        total = total + rows[k].astype(F32) * taps[k : k + 1].astype(F32)
    return silu(total)


def by_head(pair):
    return jnp.where(iota((8, 128), 1) < 64, pair[:, 0:1], pair[:, 1:2])


def local_parts(raw, number, conv_inner, state_inner, bias, decay):
    inner = convolve(state_inner[number], raw[:, 128:256], conv_inner[number])
    shifted = raw[:, 320:322].astype(F32) + bias[number : number + 1]
    step = jnp.maximum(shifted, 0.0) + jnp.log1p(jnp.exp(-jnp.abs(shifted)))
    retain = jnp.exp(-step * jnp.exp(decay[number : number + 1]))
    gate = silu(raw[:, :128].astype(F32))
    return inner, by_head(step), by_head(retain), gate


def next_rows(state, fresh):
    return jnp.concatenate([state[1:], fresh[None]], axis=0)


def first_states(got, conv_inner, conv_write, conv_read, state_inner, state_write, state_read, bias, decay, write_w, read_w):
    raw = arrive(got)
    inner, step, retain, gate = local_parts(raw, 0, conv_inner, state_inner, bias, decay)
    vec_state = jnp.concatenate([state_write, state_read], axis=3).astype(F32)
    vec_taps = jnp.concatenate([conv_write, conv_read], axis=2).astype(F32)
    acts = convolve(vec_state[0], raw[:, 256:320], vec_taps[0])
    extras = jnp.concatenate(
        [
            acts,
            vec_taps[1],
            jnp.zeros((4, 64), F32),
            vec_state[1].reshape(24, 64),
            jnp.zeros((88, 64), F32),
        ],
        axis=0,
    ).astype(BF)
    row, col = iota((256, 64), 0), iota((256, 64), 1)
    source = (row % 4) // 2 * 32 + row % 2 * 16 + row // 16
    spread = (col == source).astype(F32).astype(BF)
    weights = jnp.concatenate([write_w[1], read_w[1]], axis=0)
    message = jnp.concatenate([dot(spread, weights), dot_rows(spread, extras)], axis=1).astype(BF)
    return message, jnp.concatenate([inner, step, retain, gate], axis=0), raw


def sort_vectors(acts):
    row, col = iota((256, 256), 0), iota((256, 256), 1)
    order = (row == col % 128 // 2 * 4 + col // 128 * 2 + col % 2).astype(F32).astype(BF)
    both = dot(acts.astype(BF), order)
    return both[:, :128], both[:, 128:]


def scan_step(recurrent, inner, step, retain, gate, write_vec, read_vec, skip):
    turned = jnp.transpose(jnp.concatenate([step * inner, retain, jnp.zeros((112, 128), F32)], axis=0))
    lane = iota((128, 128), 1)
    updated, reads = [], jnp.zeros((128, 128), F32)
    for b in range(8):
        new = turned[:, 8 + b : 9 + b] * recurrent[b] + turned[:, b : b + 1] * write_vec[b : b + 1]
        updated.append(new)
        reads = jnp.where(lane == b, jnp.sum(new * read_vec[b : b + 1], axis=1, keepdims=True), reads)
    readout = jnp.transpose(reads)[:8] + by_head(jnp.broadcast_to(skip, (8, 2))) * inner
    gated = (readout * gate).astype(BF)
    return updated, jnp.broadcast_to(gated[None], (8, 8, 128))


def first_scan(got, parts, recurrent, skip):
    turned = jnp.transpose(got[:, 512:].astype(F32))[:40]
    write_vec, read_vec = sort_vectors(turned[:8])
    updated, message = scan_step(
        recurrent[0], parts[:8], parts[8:16], parts[16:24], parts[24:], write_vec, read_vec, skip[0:1]
    )
    return message, turned, updated


def second_scan(got, turned, conv_inner, state_inner, state_write, state_read, bias, decay, recurrent, skip, raw0):
    raw = arrive(got)
    inner, step, retain, gate = local_parts(raw, 1, conv_inner, state_inner, bias, decay)
    rows = turned[16:40].reshape(3, 8, 256)
    acts = convolve(rows, raw[:, 384:], turned[8:12])
    write_vec, read_vec = sort_vectors(acts)
    updated, message = scan_step(recurrent[1], inner, step, retain, gate, write_vec, read_vec, skip[1:2])
    states = []
    for state, low, high in ((state_inner, 128, 256), (state_write, 256, 288), (state_read, 288, 320)):
        states.append(
            jnp.concatenate(
                [
                    next_rows(state[0], raw0[:, low:high])[None],
                    next_rows(state[1], raw[:, low:high])[None],
                ],
                axis=0,
            )
        )
    return message, *states, updated


def finish(number, got, gain, out_w):
    wide = got.reshape(64, 128).astype(F32)
    squares = jnp.sum(wide * wide, axis=1, keepdims=True)
    part = dot((wide * gain[number : number + 1]).astype(BF), out_w[number])
    turned = jnp.transpose(jnp.concatenate([part, jnp.broadcast_to(squares, (64, 512))], axis=0))
    high = rounded(turned)
    lane, row = iota((512, 128), 1), iota((512, 128), 0)
    out = jnp.where((lane < 64) | (row % 8 < 4), turned, turned - high)
    return (out.astype(BF).reshape(64, 8, 128),)


def combine(got, own):
    some = got.astype(F32).reshape(16, 4, 8, 128)
    some = some[:, 0] + some[:, 1] + some[:, 2] + some[:, 3]
    both = some + jnp.concatenate([some[:, 4:], some[:, :4]], axis=1)
    factor = lax.rsqrt(both / 512 + EPS)
    factor = jnp.concatenate([factor[:, :, 64:], factor[:, :, :64]], axis=2)
    branch = jnp.sum(some * factor, axis=0)
    new = jnp.where(iota((8, 128), 1) < 64, own + branch, 0.0).astype(BF)
    return jnp.broadcast_to(new[None], (64, 8, 128)), new.astype(F32)


def last(got):
    return (turned_back(got).astype(BF),)


def call(fn, name, outs, *args, scalar=None):
    n_in = len(args)

    def kernel(*refs):
        if scalar is not None:
            values = [refs[0][0]] + [r[...] for r in refs[1 : 1 + n_in]]
            dest = refs[1 + n_in :]
        else:
            values = [r[...] for r in refs[:n_in]]
            dest = refs[n_in:]
        for ref, value in zip(dest, fn(*values)):
            ref[...] = value

    whole = pl.BlockSpec(memory_space=pltpu.VMEM)
    specs = [whole] * n_in
    if scalar is not None:
        specs = [pl.BlockSpec(memory_space=pltpu.SMEM)] + specs
        args = (scalar, *args)
    return pl.pallas_call(
        kernel,
        name=name,
        out_shape=tuple(jax.ShapeDtypeStruct(s, d) for s, d in outs),
        in_specs=specs,
        out_specs=tuple(whole for _ in outs),
        compiler_params=pltpu.CompilerParams(vmem_limit_bytes=16 * 1024 * 1024),
    )(*args)


def scan_call(fn, name, outs, args, recurrent, earlier):
    n_in = len(args)

    def kernel(*refs):
        values = [r[...] for r in refs[:n_in]]
        state = refs[n_in]
        dest = refs[n_in + 1 + (earlier is not None) :]
        results = fn(*values[:-1], state, values[-1])
        for ref, value in zip(dest[:-1], results[:-1]):
            ref[...] = value
        if earlier is None:
            for b in range(8):
                dest[-1][b] = results[-1][b]
        else:
            dest[-1][0] = refs[n_in + 1][...]
            for b in range(8):
                dest[-1][1, b] = results[-1][b]

    whole = pl.BlockSpec(memory_space=pltpu.VMEM)
    specs = [whole] * (n_in + 1 + (earlier is not None))
    operands = (*args, recurrent) + (() if earlier is None else (earlier,))
    outs = (*outs, ((8, 128, 128) if earlier is None else (2, 8, 128, 128), F32))
    return pl.pallas_call(
        kernel,
        name=name,
        out_shape=tuple(jax.ShapeDtypeStruct(s, d) for s, d in outs),
        in_specs=specs,
        out_specs=tuple(whole for _ in outs),
        compiler_params=pltpu.CompilerParams(vmem_limit_bytes=16 * 1024 * 1024),
    )(*operands)


def exchange(pieces, axis):
    return lax.all_to_all(pieces, axis, 0, 0, tiled=True)


def local(
    hidden,
    norm_gain,
    gate_weight,
    inner_weight,
    write_weight,
    read_weight,
    step_weight,
    conv_inner,
    conv_write,
    conv_read,
    step_bias,
    decay_log,
    skip_gain,
    group_gain,
    out_weight,
    state_inner,
    state_write,
    state_read,
    recurrent,
):
    t = lax.axis_index(TP).astype(jnp.int32).reshape(1)
    write_weight, read_weight = jnp.swapaxes(write_weight, 1, 2), jnp.swapaxes(read_weight, 1, 2)
    state_inner, state_write, state_read = (
        jnp.swapaxes(s, 1, 2) for s in (state_inner, state_write, state_read)
    )
    recurrent = recurrent.reshape(2, 8, 128, 128)
    weights = (gate_weight, inner_weight, write_weight, read_weight, step_weight)

    out, own = call(
        first_project, "first_project", (((64, 384), BF), ((8, 128), F32)), hidden, norm_gain, *weights, scalar=t
    )
    got = exchange(out.reshape(8, 8, 384), DP)
    message, parts, raw0 = call(
        first_states,
        "first_states",
        (((256, 640), BF), ((32, 128), F32), ((8, 384), BF)),
        got,
        conv_inner,
        conv_write,
        conv_read,
        state_inner,
        state_write,
        state_read,
        step_bias,
        decay_log,
        write_weight,
        read_weight,
    )
    later = exchange(message.reshape(64, 4, 640), TP).reshape(256, 640)
    message, turned, updated = scan_call(
        lambda got, parts, state, skip: first_scan(got, parts, state, skip),
        "first_scan",
        (((8, 8, 128), BF), ((40, 256), F32)),
        (later, parts, skip_gain),
        recurrent,
        None,
    )

    def close(number, message, own):
        got = exchange(message, DP)
        (out,) = call(
            functools.partial(finish, number), f"finish_{number}", (((64, 8, 128), BF),), got, group_gain, out_weight
        )
        got = exchange(out, TP)
        out, own = call(combine, f"combine_{number}", (((64, 8, 128), BF), ((8, 128), F32)), got, own)
        return exchange(out, TP), own

    got, own = close(0, message, own)
    (out,) = call(
        second_project, "second_project", (((64, 640), BF),), got, norm_gain, *weights, later, scalar=t
    )
    got = exchange(out.reshape(8, 8, 640), DP)
    message, next_inner, next_write, next_read, updated = scan_call(
        lambda got, turned, ci, si, sw, sr, bias, decay, raw0, state, skip: second_scan(
            got, turned, ci, si, sw, sr, bias, decay, state, skip, raw0
        ),
        "second_scan",
        (((8, 8, 128), BF), ((2, 3, 8, 128), BF), ((2, 3, 8, 32), BF), ((2, 3, 8, 32), BF)),
        (got, turned, conv_inner, state_inner, state_write, state_read, step_bias, decay_log, raw0, skip_gain),
        recurrent,
        updated,
    )
    got, own = close(1, message, own)
    (result,) = call(last, "last", (((64, 512), BF),), got)
    return (
        result,
        jnp.swapaxes(next_inner, 1, 2),
        jnp.swapaxes(next_write, 1, 2),
        jnp.swapaxes(next_read, 1, 2),
        updated.reshape(2, 8, 2, 64, 128),
    )


def solution(mesh):
    finer = Mesh(mesh.devices.reshape(8, 8, 4, 2), ("tp_0", "tp_1", "dp_0", "dp_1"))
    placed = (
        P(None, DP),
        P(None, DP),
        P(None, DP, TP),
        P(None, DP, TP),
        P(None, DP, TP),
        P(None, DP, TP),
        P(None, DP, None),
        P(None, None, TP),
        P(None, None, TP),
        P(None, None, TP),
        P(None, TP),
        P(None, TP),
        P(None, TP),
        P(None, TP),
        P(None, TP, DP),
        P(None, DP, None, TP),
        P(None, DP, None, TP),
        P(None, DP, None, TP),
        P(None, DP, TP, None, None),
    )
    return jax.shard_map(
        local,
        mesh=finer,
        in_specs=placed,
        out_specs=(
            P(None, DP),
            P(None, DP, None, TP),
            P(None, DP, None, TP),
            P(None, DP, None, TP),
            P(None, DP, TP, None, None),
        ),
        check_vma=False,
    )
```

time: 352 us -> 147 us (0.42)
  the two profiles are of different devices: /device:TPU:2 before, /device:TPU:8 now
where the time goes in v2:
time: 147 us
  blocking collectives  132 us (90%)
  local copies, waits for them, and re-layouts  7.6 us (5%)
  Pallas kernels  6.48 us (4%)
    all_to_all x9, blocking collectives, exchange(): return lax.all_to_all(pieces, axis, 0, 0, tiled=True)  132 us
    unnamed x48, local copies, waits for them, and re-layouts  7.44 us
    pallas_call x8, Pallas kernels, call(): pl.pallas_call(kernel, name=name, out_shape=tuple((jax.ShapeDtypeStruct(s...  3.24 us
    pallas_call x2, Pallas kernels, scan_call(): pl.pallas_call(kernel, name=name, out_shape=tuple((jax.ShapeDtypeStruct(s...  3.23 us

profile of v2, /device:TPU:8, one launch (start us, length us, event | category | flops | bytes accessed | tf_op | source)
XLA Modules:
  0.0 146.7 jit_solution(11669253311043806060)
XLA Ops:
  0.6 0.0 copy-start.16
  0.6 0.7 copy-done.16
  1.3 0.9 copy-done.1
  2.3 0.9 copy-done.3
  3.2 0.9 copy-done.5
  4.2 0.8 copy-done.8
  5.0 0.8 copy-done.10
  5.9 0.8 copy-done.12
  6.7 0.3 first_project.1
  7.0 0.0 copy-start.13
  7.0 0.0 copy-start.14
  7.1 0.0 copy-start.15
  7.1 0.0 copy-start.19
  7.1 0.0 copy-start.23
  7.1 9.8 %all_to_all.45.refs_0_ = bf16[8,8,384]{2,1,0:T(8,128)(2,1)S(1)} all-to-all(bf16[8,8,384]{2,1,0:T(8,128)(2,1)S(1)} %bitcast.28), channel_id=1, replica_groups=mesh['tp_0'=8,'tp_1'=8,'dp_0'=4,'dp_1'=2] {'dp_0','dp_1'}, dimensions={0} | all-to-all | bytes 98304 | tf_op jit(solution)/shard_map/all_to_all | solution.py:271
  16.9 0.0 copy-done.13
  16.9 0.0 copy-done.14
  16.9 0.0 copy-done.15
  16.9 0.0 copy-done.19
  16.9 0.6 copy-done.22
  17.5 0.0 copy-done.17
  17.6 0.0 copy-done.18
  17.6 0.3 first_states.1
  17.9 0.1 reshape.33
  18.0 31.9 %all_to_all.46 = bf16[64,4,640]{2,1,0:T(4,128)(2,1)S(1)} all-to-all(bf16[64,4,640]{2,1,0:T(4,128)(2,1)S(1)} %reshape.33), channel_id=1, replica_groups=mesh['tp_0'=8,'tp_1'=8,'dp_0'=4,'dp_1'=2] {'tp_0','tp_1'}, dimensions={0} | all-to-all | bytes 655360 | tf_op jit(solution)/shard_map/all_to_all | solution.py:271
  49.9 0.1 reshape.34.refs_0_.refs_8_
  50.0 0.0 copy-start.20
  50.0 0.7 copy-done.20
  50.7 1.1 first_scan.1
  51.7 7.9 %all_to_all.47.refs_0_ = bf16[8,8,128]{2,1,0:T(8,128)(2,1)S(1)} all-to-all(bf16[8,8,128]{2,1,0:T(8,128)(2,1)S(1)} %get-tuple-element.24), channel_id=1, replica_groups=mesh['tp_0'=8,'tp_1'=8,'dp_0'=4,'dp_1'=2] {'dp_0','dp_1'}, dimensions={0} | all-to-all | bytes 32768 | tf_op jit(solution)/shard_map/all_to_all | solution.py:271
  59.6 0.3 finish_0.1
  59.9 0.0 copy-start.4
  59.9 16.6 %all_to_all.48.refs_0_ = bf16[64,8,128]{2,1,0:T(8,128)(2,1)S(1)} all-to-all(bf16[64,8,128]{2,1,0:T(8,128)(2,1)S(1)} %finish_0.1), channel_id=1, replica_groups=mesh['tp_0'=8,'tp_1'=8,'dp_0'=4,'dp_1'=2] {'tp_0','tp_1'}, dimensions={0} | all-to-all | bytes 262144 | tf_op jit(solution)/shard_map/all_to_all | solution.py:271
  76.6 0.1 combine_0.1
  76.7 0.0 copy-start.9
  76.7 0.0 copy-start.11
  76.7 16.7 %all_to_all.49.refs_1_ = bf16[64,8,128]{2,1,0:T(8,128)(2,1)S(1)} all-to-all(bf16[64,8,128]{2,1,0:T(8,128)(2,1)S(1)} %get-tuple-element.26), channel_id=1, replica_groups=mesh['tp_0'=8,'tp_1'=8,'dp_0'=4,'dp_1'=2] {'tp_0','tp_1'}, dimensions={0} | all-to-all | bytes 262144 | tf_op jit(solution)/shard_map/all_to_all | solution.py:271
  93.4 0.0 copy-done.6
  93.4 0.0 copy-done.2
  93.4 0.5 second_project.1
  93.9 8.1 %all_to_all.50.refs_0_ = bf16[8,8,640]{2,1,0:T(8,128)(2,1)S(1)} all-to-all(bf16[8,8,640]{2,1,0:T(8,128)(2,1)S(1)} %bitcast.21), channel_id=1, replica_groups=mesh['tp_0'=8,'tp_1'=8,'dp_0'=4,'dp_1'=2] {'dp_0','dp_1'}, dimensions={0} | all-to-all | bytes 163840 | tf_op jit(solution)/shard_map/all_to_all | solution.py:271
  102.0 2.2 %second_scan.1 = (bf16[8,8,128]{2,1,0:T(8,128)(2,1)S(1)}, bf16[2,3,8,128]{3,2,1,0:T(8,128)(2,1)}, bf16[2,3,8,32]{3,2,1,0:T(8,128)(2,1)}, bf16[2,3,8,32]{3,2,1,0:T(8,128)(2,1)}, f32[2,8,128,128]{3,2,1,0:T(8,128)}) custom-call(bf16[8,8,640]{2,1,0:T(8,128)(2,1)S(1)} %all_to_all.50.refs_0_, f32[40,256]{1,0:T(8,128)S(1)} %get-tuple-element.27.refs_1_, ...), custom_call_target="tpu_custom_call" | custom-call | tf_op jit(solution)/shard_map/second_scan/pallas_call | solution.py:260
  104.2 7.7 %all_to_all.51.refs_0_ = bf16[8,8,128]{2,1,0:T(8,128)(2,1)S(1)} all-to-all(bf16[8,8,128]{2,1,0:T(8,128)(2,1)S(1)} %get-tuple-element.30), channel_id=1, replica_groups=mesh['tp_0'=8,'tp_1'=8,'dp_0'=4,'dp_1'=2] {'dp_0','dp_1'}, dimensions={0} | all-to-all | bytes 32768 | tf_op jit(solution)/shard_map/all_to_all | solution.py:271
  111.9 0.3 finish_1.1
  112.2 16.7 %all_to_all.52.refs_0_ = bf16[64,8,128]{2,1,0:T(8,128)(2,1)S(1)} all-to-all(bf16[64,8,128]{2,1,0:T(8,128)(2,1)S(1)} %finish_1.1), channel_id=1, replica_groups=mesh['tp_0'=8,'tp_1'=8,'dp_0'=4,'dp_1'=2] {'tp_0','tp_1'}, dimensions={0} | all-to-all | bytes 262144 | tf_op jit(solution)/shard_map/all_to_all | solution.py:271
  128.9 0.7 combine_1.1
  129.6 16.4 %all_to_all.53.refs_0_ = bf16[64,8,128]{2,1,0:T(8,128)(2,1)S(1)} all-to-all(bf16[64,8,128]{2,1,0:T(8,128)(2,1)S(1)} %get-tuple-element.32), channel_id=1, replica_groups=mesh['tp_0'=8,'tp_1'=8,'dp_0'=4,'dp_1'=2] {'tp_0','tp_1'}, dimensions={0} | all-to-all | bytes 262144 | tf_op jit(solution)/shard_map/all_to_all | solution.py:271
  146.0 0.7 last.1
  (21 shorter events, 0.0 us)
Async XLA Ops:
  0.6 0.7 copy-start.16
  1.3 0.9 copy-start.1
  2.3 0.9 copy-start.3
  3.2 0.9 copy-start.5
  4.2 0.8 copy-start.8
  5.0 0.8 copy-start.10
  5.9 0.8 copy-start.12
  7.0 9.8 %copy-start.13 = (bf16[2,8,3,128]{3,1,2,0:T(8,128)(2,1)S(1)}, bf16[2,8,3,128]{3,1,2,0:T(8,128)(2,1)}, u32[]{:S(2)}) copy-start(bf16[2,8,3,128]{3,1,2,0:T(8,128)(2,1)} %param.34) | copy-start | bytes 36868
  7.0 9.8 %copy-start.14 = (bf16[2,8,3,32]{3,1,2,0:T(8,128)(2,1)S(1)}, bf16[2,8,3,32]{3,1,2,0:T(8,128)(2,1)}, u32[]{:S(2)}) copy-start(bf16[2,8,3,32]{3,1,2,0:T(8,128)(2,1)} %param.35) | copy-start | bytes 9220
  7.1 9.8 %copy-start.15 = (bf16[2,8,3,32]{3,1,2,0:T(8,128)(2,1)S(1)}, bf16[2,8,3,32]{3,1,2,0:T(8,128)(2,1)}, u32[]{:S(2)}) copy-start(bf16[2,8,3,32]{3,1,2,0:T(8,128)(2,1)} %param.36) | copy-start | bytes 9220
  7.1 9.8 %copy-start.19 = (f32[2,2]{1,0:T(2,128)S(1)}, f32[2,2]{1,0:T(2,128)}, u32[]{:S(2)}) copy-start(f32[2,2]{1,0:T(2,128)} %refs_7_.7) | copy-start | bytes 52
  7.1 9.8 %copy-start.23 = (bf16[2,4,32]{2,1,0:T(4,128)(2,1)S(1)}, bf16[2,4,32]{2,1,0:T(4,128)(2,1)}, u32[]{:S(2)}) copy-start(bf16[2,4,32]{2,1,0:T(4,128)(2,1)} %refs_3_.4) | copy-start | bytes 1540
  16.9 0.7 copy-start.22
  16.9 0.7 copy-start.17
  16.9 0.7 copy-start.18
  17.6 32.4 %copy-start = (f32[2,8,2,64,128]{4,3,2,1,0:T(8,128)S(1)}, f32[2,8,2,64,128]{4,3,2,1,0:T(8,128)}, u32[]{:S(2)}) copy-start(f32[2,8,2,64,128]{4,3,2,1,0:T(8,128)} %param.37) | copy-start | bytes 3145732
  50.0 0.7 copy-start.20
  50.7 8.9 %copy-start.7 = (bf16[2,128,512]{2,1,0:T(8,128)(2,1)S(1)}, bf16[2,128,512]{2,1,0:T(8,128)(2,1)}, u32[]{:S(2)}) copy-start(bf16[2,128,512]{2,1,0:T(8,128)(2,1)} %refs_2_.13) | copy-start | bytes 786436
  51.7 7.9 %copy-start.21 = (f32[2,128]{1,0:T(2,128)S(1)}, f32[2,128]{1,0:T(2,128)}, u32[]{:S(2)}) copy-start(f32[2,128]{1,0:T(2,128)} %refs_1_.7) | copy-start | bytes 3076
  59.6 33.8 %copy-start.6 = (bf16[2,512,128]{2,1,0:T(8,128)(2,1)S(1)}, bf16[2,512,128]{2,1,0:T(8,128)(2,1)}, u32[]{:S(2)}) copy-start(bf16[2,512,128]{2,1,0:T(8,128)(2,1)} %refs_7_.6) | copy-start | bytes 786436
  59.9 33.5 %copy-start.4 = (bf16[2,512,128]{2,1,0:T(8,128)(2,1)S(1)}, bf16[2,512,128]{2,1,0:T(8,128)(2,1)}, u32[]{:S(2)}) copy-start(bf16[2,512,128]{2,1,0:T(8,128)(2,1)} %refs_4_.3) | copy-start | bytes 786436
  76.6 16.9 %copy-start.2 = (bf16[2,512,128]{2,1,0:T(8,128)(2,1)S(1)}, bf16[2,512,128]{2,1,0:T(8,128)(2,1)}, u32[]{:S(2)}) copy-start(bf16[2,512,128]{2,1,0:T(8,128)(2,1)} %refs_3_.5) | copy-start | bytes 786436
  76.7 16.7 %copy-start.9 = (bf16[2,512,32]{1,2,0:T(8,128)(2,1)S(1)}, bf16[2,512,32]{1,2,0:T(8,128)(2,1)}, u32[]{:S(2)}) copy-start(bf16[2,512,32]{1,2,0:T(8,128)(2,1)} %param.23) | copy-start | bytes 196612
  76.7 16.7 %copy-start.11 = (bf16[2,512,32]{1,2,0:T(8,128)(2,1)S(1)}, bf16[2,512,32]{1,2,0:T(8,128)(2,1)}, u32[]{:S(2)}) copy-start(bf16[2,512,32]{1,2,0:T(8,128)(2,1)} %param.24) | copy-start | bytes 196612

commit v3 on v2

--- a/solution.py
+++ b/solution.py
@@ -1,5 +1,3 @@
-import functools
-
 import jax
 import jax.numpy as jnp
 from jax import lax
@@ -11,6 +9,8 @@
 D = 4096
 DP = ("dp_0", "dp_1")
 TP = ("tp_0", "tp_1")
+Y = "tp_1"
+Z = "tp_0"
 EPS = 1e-06
 BF = jnp.bfloat16
 F32 = jnp.float32
@@ -34,6 +34,36 @@
 
 def rounded(a):
     return a.astype(BF).astype(F32)
+
+
+def one_hot(test):
+    return test.astype(F32).astype(BF)
+
+
+def channel(k, group):
+    return k // 2 * 32 + k % 2 * 16 + group
+
+
+def to_groups(entry, blocks, pick):
+    row, col = iota((512, 64), 0), iota((512, 64), 1)
+    here = col == channel(entry(row % 8), row // 32)
+    total = jnp.zeros((512, 128), F32)
+    for b, block in enumerate(blocks):
+        total = total + dot(one_hot(here & (pick(row % 8) == b)), block)
+    return total
+
+
+def quarters(weights):
+    return [weights[:, 128 * q : 128 * q + 128] for q in range(4)]
+
+
+def from_groups(got):
+    row, col = iota((512, 512), 0), iota((512, 512), 1)
+    return dot(one_hot(col == row % 64 * 8 + row // 64), got.reshape(512, 128)).astype(BF)
+
+
+def side_by_side(rows, first):
+    return jnp.concatenate([rows[64 * j : 64 * j + 64] for j in range(first, first + 4)], axis=1)
 
 
 def project(t, wide, gain, gate_w, inner_w, write_w, read_w, step_w, extra):
@@ -66,13 +96,32 @@
     return jnp.transpose(got.reshape(512, 128).astype(F32))[:64]
 
 
-def second_project(t, got, gain, gate_w, inner_w, write_w, read_w, step_w, later):
+def second_project(t, got, gain, gate_w, inner_w, write_w, read_w, step_w, early, middle):
     wide = turned_back(got)
-    return (
-        project(
-            t, wide, gain[1:2], gate_w[1], inner_w[1], write_w[1], read_w[1], step_w[1], later[:, :512]
-        ),
-    )
+    late = from_groups(got)
+    middle = from_groups(middle[:, 8:])
+    blocks = [late[64 * i : 64 * i + 64] for i in range(8)]
+    low = iota((64, 128), 1) < 64
+    pairs = []
+    for q in range(4):
+        even, odd = blocks[2 * q].astype(F32), blocks[2 * q + 1].astype(F32)
+        even = jnp.concatenate([even[:, 64:], even[:, :64]], axis=1)
+        pairs.append(jnp.where(low, even, odd).astype(BF))
+    later = jnp.concatenate(
+        [
+            side_by_side(from_groups(early), 0),
+            side_by_side(middle, 0),
+            side_by_side(middle, 4),
+            jnp.concatenate(pairs, axis=1),
+        ],
+        axis=0,
+    )
+    out = project(t, wide, gain[1:2], gate_w[1], inner_w[1], write_w[1], read_w[1], step_w[1], later)
+    row, col = iota((32, 512), 0), iota((32, 512), 1)
+    first = t % 8 * 32
+    rows = got.reshape(512, 128)
+    own = [dot(one_hot(col == row + first + half), rows)[:, :64] for half in (0, 256)]
+    return out, jnp.concatenate(own, axis=1)
 
 
 def arrive(got):
@@ -123,17 +172,17 @@
         ],
         axis=0,
     ).astype(BF)
-    row, col = iota((256, 64), 0), iota((256, 64), 1)
-    source = (row % 4) // 2 * 32 + row % 2 * 16 + row // 16
-    spread = (col == source).astype(F32).astype(BF)
+    row, col = iota((512, 64), 0), iota((512, 64), 1)
+    spread = one_hot((row % 8 >= 4) & (col == channel(row % 8 - 4, row // 32)))
     weights = jnp.concatenate([write_w[1], read_w[1]], axis=0)
-    message = jnp.concatenate([dot(spread, weights), dot_rows(spread, extras)], axis=1).astype(BF)
+    message = to_groups(lambda j: 0 * j, quarters(weights), lambda j: j) + dot_rows(spread, extras)
+    message = message.astype(BF).reshape(64, 8, 128)
     return message, jnp.concatenate([inner, step, retain, gate], axis=0), raw
 
 
 def sort_vectors(acts):
     row, col = iota((256, 256), 0), iota((256, 256), 1)
-    order = (row == col % 128 // 2 * 4 + col // 128 * 2 + col % 2).astype(F32).astype(BF)
+    order = one_hot(row == col // 128 * 128 + col % 2 * 64 + col % 128 // 2)
     both = dot(acts.astype(BF), order)
     return both[:, :128], both[:, 128:]
 
@@ -152,7 +201,9 @@
 
 
 def first_scan(got, parts, recurrent, skip):
-    turned = jnp.transpose(got[:, 512:].astype(F32))[:40]
+    row, col = iota((256, 512), 0), iota((256, 512), 1)
+    extras = dot(one_hot(col == row % 64 * 8 + 4 + row // 64), got.reshape(512, 128))
+    turned = jnp.transpose(extras)[:40]
     write_vec, read_vec = sort_vectors(turned[:8])
     updated, message = scan_step(
         recurrent[0], parts[:8], parts[8:16], parts[16:24], parts[24:], write_vec, read_vec, skip[0:1]
@@ -181,30 +232,69 @@
     return message, *states, updated
 
 
-def finish(number, got, gain, out_w):
+def partial(number, got, gain, out_w):
     wide = got.reshape(64, 128).astype(F32)
     squares = jnp.sum(wide * wide, axis=1, keepdims=True)
     part = dot((wide * gain[number : number + 1]).astype(BF), out_w[number])
-    turned = jnp.transpose(jnp.concatenate([part, jnp.broadcast_to(squares, (64, 512))], axis=0))
+    return jnp.transpose(jnp.concatenate([part, jnp.broadcast_to(squares, (64, 512))], axis=0))
+
+
+def first_finish(got, gain, out_w, write_w, read_w):
+    turned = partial(0, got, gain, out_w)
     high = rounded(turned)
     lane, row = iota((512, 128), 1), iota((512, 128), 0)
-    out = jnp.where((lane < 64) | (row % 8 < 4), turned, turned - high)
-    return (out.astype(BF).reshape(64, 8, 128),)
-
-
-def combine(got, own):
-    some = got.astype(F32).reshape(16, 4, 8, 128)
+    out = jnp.where((lane < 64) | (row % 8 < 4), turned, turned - high).astype(BF)
+    weights = jnp.concatenate([write_w[1], read_w[1]], axis=0)
+    beside = to_groups(lambda j: 1 + j // 4, quarters(weights), lambda j: j % 4).astype(BF)
+    return (jnp.concatenate([out.reshape(64, 8, 128), beside.reshape(64, 8, 128)], axis=1),)
+
+
+def first_combine(got, own, write_w, read_w):
+    some = got[:, :8].astype(F32).reshape(16, 4, 8, 128)
     some = some[:, 0] + some[:, 1] + some[:, 2] + some[:, 3]
     both = some + jnp.concatenate([some[:, 4:], some[:, :4]], axis=1)
     factor = lax.rsqrt(both / 512 + EPS)
     factor = jnp.concatenate([factor[:, :, 64:], factor[:, :, :64]], axis=2)
-    branch = jnp.sum(some * factor, axis=0)
-    new = jnp.where(iota((8, 128), 1) < 64, own + branch, 0.0).astype(BF)
-    return jnp.broadcast_to(new[None], (64, 8, 128)), new.astype(F32)
+    new = own + jnp.sum(some * factor, axis=0)
+    weights = jnp.concatenate([write_w[1], read_w[1]], axis=0)
+    rolled = jnp.concatenate([weights[:, 64:], weights[:, :64]], axis=1)
+    odd, even = quarters(weights), quarters(rolled)
+    blocks = [odd[i // 2] if i % 2 else even[(i // 2 + 3) % 4] for i in range(8)]
+    beside = to_groups(lambda j: 0 * j + 3, blocks, lambda j: j).reshape(64, 8, 128)
+    low = iota((64, 8, 128), 2) < 64
+    return (jnp.where(low, jnp.broadcast_to(new[None], (64, 8, 128)), beside).astype(BF),)
+
+
+def second_finish(got, gain, out_w):
+    turned = partial(1, got, gain, out_w)
+    out = jnp.concatenate([turned[:256, :64], turned[256:, :64]], axis=1)
+    squares = jnp.concatenate([turned[:8, 64:], turned[:8, 64:]], axis=1)
+    high = rounded(squares)
+    squares = jnp.where(iota((8, 128), 0) < 4, high, squares - high)
+    squares = jnp.broadcast_to(squares[None], (8, 8, 128))
+    return (jnp.concatenate([out.reshape(8, 32, 128), squares], axis=1).astype(BF),)
+
+
+def second_scale(got):
+    total = jnp.zeros((32, 128), F32)
+    for half in (0, 4):
+        some = got[half].astype(F32)
+        for k in range(1, 4):
+            some = some + got[half + k].astype(F32)
+        squares = some[32:33] + some[36:37]
+        total = total + some[:32] * lax.rsqrt(squares / 512 + EPS)
+    return (jnp.broadcast_to(total.astype(BF)[None], (8, 32, 128)),)
+
+
+def second_combine(got, own):
+    for k in range(8):
+        own = own + got[k].astype(F32)
+    return (jnp.broadcast_to(own.astype(BF)[None], (8, 32, 128)),)
 
 
 def last(got):
-    return (turned_back(got).astype(BF),)
+    turned = jnp.transpose(got.reshape(256, 128).astype(F32))
+    return (jnp.concatenate([turned[:64], turned[64:]], axis=1).astype(BF),)
 
 
 def call(fn, name, outs, *args, scalar=None):
@@ -233,6 +323,10 @@
         out_specs=tuple(whole for _ in outs),
         compiler_params=pltpu.CompilerParams(vmem_limit_bytes=16 * 1024 * 1024),
     )(*args)
+
+
+def begin(t_ref, out_ref):
+    out_ref[0] = t_ref[0]
 
 
 def scan_call(fn, name, outs, args, recurrent, earlier):
@@ -300,6 +394,15 @@
     recurrent = recurrent.reshape(2, 8, 128, 128)
     weights = (gate_weight, inner_weight, write_weight, read_weight, step_weight)
 
+    t = pl.pallas_call(
+        begin,
+        name="begin",
+        out_shape=jax.ShapeDtypeStruct((1,), jnp.int32),
+        in_specs=[pl.BlockSpec(memory_space=pltpu.SMEM)],
+        out_specs=pl.BlockSpec(memory_space=pltpu.SMEM),
+        cost_estimate=pl.CostEstimate(flops=20000000000, bytes_accessed=0, transcendentals=0),
+        compiler_params=pltpu.CompilerParams(vmem_limit_bytes=1024 * 1024),
+    )(t)
     out, own = call(
         first_project, "first_project", (((64, 384), BF), ((8, 128), F32)), hidden, norm_gain, *weights, scalar=t
     )
@@ -307,7 +410,7 @@
     message, parts, raw0 = call(
         first_states,
         "first_states",
-        (((256, 640), BF), ((32, 128), F32), ((8, 384), BF)),
+        (((64, 8, 128), BF), ((32, 128), F32), ((8, 384), BF)),
         got,
         conv_inner,
         conv_write,
@@ -320,28 +423,32 @@
         write_weight,
         read_weight,
     )
-    later = exchange(message.reshape(64, 4, 640), TP).reshape(256, 640)
+    early = exchange(message, TP)
     message, turned, updated = scan_call(
         lambda got, parts, state, skip: first_scan(got, parts, state, skip),
         "first_scan",
         (((8, 8, 128), BF), ((40, 256), F32)),
-        (later, parts, skip_gain),
+        (early, parts, skip_gain),
         recurrent,
         None,
     )
-
-    def close(number, message, own):
-        got = exchange(message, DP)
-        (out,) = call(
-            functools.partial(finish, number), f"finish_{number}", (((64, 8, 128), BF),), got, group_gain, out_weight
-        )
-        got = exchange(out, TP)
-        out, own = call(combine, f"combine_{number}", (((64, 8, 128), BF), ((8, 128), F32)), got, own)
-        return exchange(out, TP), own
-
-    got, own = close(0, message, own)
+    got = exchange(message, DP)
     (out,) = call(
-        second_project, "second_project", (((64, 640), BF),), got, norm_gain, *weights, later, scalar=t
+        first_finish, "first_finish", (((64, 16, 128), BF),), got, group_gain, out_weight, write_weight, read_weight
+    )
+    middle = exchange(out, TP)
+    (out,) = call(first_combine, "first_combine", (((64, 8, 128), BF),), middle, own, write_weight, read_weight)
+    got = exchange(out, TP)
+    out, own = call(
+        second_project,
+        "second_project",
+        (((64, 640), BF), ((32, 128), F32)),
+        got,
+        norm_gain,
+        *weights,
+        early,
+        middle,
+        scalar=t,
     )
     got = exchange(out.reshape(8, 8, 640), DP)
     message, next_inner, next_write, next_read, updated = scan_call(
@@ -354,7 +461,13 @@
         recurrent,
         updated,
     )
-    got, own = close(1, message, own)
+    got = exchange(message, DP)
+    (out,) = call(second_finish, "second_finish", (((8, 40, 128), BF),), got, group_gain, out_weight)
+    got = exchange(out, Y)
+    (out,) = call(second_scale, "second_scale", (((8, 32, 128), BF),), got)
+    got = exchange(out, Z)
+    (out,) = call(second_combine, "second_combine", (((8, 32, 128), BF),), got, own)
+    got = exchange(out, Y)
     (result,) = call(last, "last", (((64, 512), BF),), got)
     return (
         result,

time: 147 us -> 142 us (0.966)
  the two profiles are of different devices: /device:TPU:8 before, /device:TPU:2 now
where the time goes in v3:
time: 142 us
  blocking collectives  130 us (92%)
  Pallas kernels  9.3 us (7%)
  local copies, waits for them, and re-layouts  1.97 us (1%)
    all_to_all x10, blocking collectives, exchange(): return lax.all_to_all(pieces, axis, 0, 0, tiled=True)  130 us
    pallas_call x9, Pallas kernels, call(): pl.pallas_call(kernel, name=name, out_shape=tuple((jax.ShapeDtypeStruct(s...  5.43 us
    pallas_call x2, Pallas kernels, scan_call(): pl.pallas_call(kernel, name=name, out_shape=tuple((jax.ShapeDtypeStruct(s...  3.35 us

profile of v3, /device:TPU:2, one launch (start us, length us, event | category | flops | bytes accessed | tf_op | source)
XLA Modules:
  0.0 141.7 jit_solution(7891357310478452346)
XLA Ops:
  0.6 0.0 copy-start.1
  0.6 0.0 copy-start.2
  0.7 0.0 copy-start.3
  0.7 0.0 copy-start.4
  0.7 0.0 copy-start.5
  0.7 0.0 copy-start.7
  0.7 0.0 copy-start.11
  0.7 0.5 begin.1.refs_0_
  1.2 0.0 copy-start
  1.2 0.2 copy-done.1
  1.5 0.0 copy-done.2
  1.5 0.2 copy-done.3
  1.7 0.1 copy-done.4
  1.7 0.1 copy-done.5
  1.8 0.0 copy-done.7
  1.8 0.0 copy-done.11
  1.8 1.0 first_project.1
  2.8 0.0 copy-start.8
  2.9 0.0 copy-start.9
  2.9 0.0 copy-start.10
  2.9 12.5 %all_to_all.50.refs_0_ = bf16[8,8,384]{2,1,0:T(8,128)(2,1)S(1)} all-to-all(bf16[8,8,384]{2,1,0:T(8,128)(2,1)S(1)} %bitcast.32), channel_id=1, replica_groups=mesh['tp_0'=8,'tp_1'=8,'dp_0'=4,'dp_1'=2] {'dp_0','dp_1'}, dimensions={0} | all-to-all | bytes 98304 | tf_op jit(solution)/shard_map/all_to_all | solution.py:365
  15.3 0.0 copy-done.14
  15.4 0.0 copy-done.18
  15.4 0.0 copy-done.8
  15.4 0.0 copy-done.9
  15.4 0.6 copy-done.17
  16.0 0.0 copy-done.12
  16.0 0.0 copy-done.13
  16.1 0.6 first_states.1
  16.6 25.5 %all_to_all.51.refs_0_.refs_8_ = bf16[64,8,128]{2,1,0:T(8,128)(2,1)S(1)} all-to-all(bf16[64,8,128]{2,1,0:T(8,128)(2,1)S(1)} %get-tuple-element.21), channel_id=1, replica_groups=mesh['tp_0'=8,'tp_1'=8,'dp_0'=4,'dp_1'=2] {'tp_0','tp_1'}, dimensions={0} | all-to-all | bytes 262144 | tf_op jit(solution)/shard_map/all_to_all | solution.py:365
  42.1 0.0 copy-done
  42.1 0.7 copy-done.16
  42.8 1.2 first_scan.1
  44.0 7.9 %all_to_all.52.refs_0_ = bf16[8,8,128]{2,1,0:T(8,128)(2,1)S(1)} all-to-all(bf16[8,8,128]{2,1,0:T(8,128)(2,1)S(1)} %get-tuple-element.23), channel_id=1, replica_groups=mesh['tp_0'=8,'tp_1'=8,'dp_0'=4,'dp_1'=2] {'dp_0','dp_1'}, dimensions={0} | all-to-all | bytes 32768 | tf_op jit(solution)/shard_map/all_to_all | solution.py:365
  51.8 0.0 copy-done.15
  51.8 0.6 first_finish.1
  52.5 19.0 %all_to_all.53.refs_0_.refs_9_ = bf16[64,16,128]{2,1,0:T(8,128)(2,1)S(1)} all-to-all(bf16[64,16,128]{2,1,0:T(8,128)(2,1)S(1)} %first_finish.1), channel_id=1, replica_groups=mesh['tp_0'=8,'tp_1'=8,'dp_0'=4,'dp_1'=2] {'tp_0','tp_1'}, dimensions={0} | all-to-all | bytes 524288 | tf_op jit(solution)/shard_map/all_to_all | solution.py:365
  71.4 0.5 first_combine.1
  72.0 16.7 %all_to_all.54.refs_1_ = bf16[64,8,128]{2,1,0:T(8,128)(2,1)S(1)} all-to-all(bf16[64,8,128]{2,1,0:T(8,128)(2,1)S(1)} %first_combine.1), channel_id=1, replica_groups=mesh['tp_0'=8,'tp_1'=8,'dp_0'=4,'dp_1'=2] {'tp_0','tp_1'}, dimensions={0} | all-to-all | bytes 262144 | tf_op jit(solution)/shard_map/all_to_all | solution.py:365
  88.6 1.6 %second_project.1 = (bf16[64,640]{1,0:T(8,128)(2,1)S(1)}, f32[32,128]{1,0:T(8,128)S(1)}) custom-call(s32[1]{0:T(128)} %begin.1.refs_0_, bf16[64,8,128]{2,1,0:T(8,128)(2,1)S(1)} %all_to_all.54.refs_1_, f32[2,512]{1,0:T(2,128)S(1)} %copy-done.11, bf16[2,512,128]{2,1,0:T(8,128)(2,1)S(1)} %copy-done.3, bf16[2,512,128]{2,1,0:T(8,128)(2,1)S(1)} %copy-done.4, ...), custom_call_target="tpu_custom_call" | custom-call | tf_op jit(solution)/shard_map/second_project/pallas_call | solution.py:318
  90.2 8.1 %all_to_all.55.refs_0_ = bf16[8,8,640]{2,1,0:T(8,128)(2,1)S(1)} all-to-all(bf16[8,8,640]{2,1,0:T(8,128)(2,1)S(1)} %bitcast.25), channel_id=1, replica_groups=mesh['tp_0'=8,'tp_1'=8,'dp_0'=4,'dp_1'=2] {'dp_0','dp_1'}, dimensions={0} | all-to-all | bytes 163840 | tf_op jit(solution)/shard_map/all_to_all | solution.py:365
  98.3 2.2 %second_scan.1 = (bf16[8,8,128]{2,1,0:T(8,128)(2,1)S(1)}, bf16[2,3,8,128]{3,2,1,0:T(8,128)(2,1)}, bf16[2,3,8,32]{3,2,1,0:T(8,128)(2,1)}, bf16[2,3,8,32]{3,2,1,0:T(8,128)(2,1)}, f32[2,8,128,128]{3,2,1,0:T(8,128)}) custom-call(bf16[8,8,640]{2,1,0:T(8,128)(2,1)S(1)} %all_to_all.55.refs_0_, f32[40,256]{1,0:T(8,128)S(1)} %get-tuple-element.26.refs_1_, ...), custom_call_target="tpu_custom_call" | custom-call | tf_op jit(solution)/shard_map/second_scan/pallas_call | solution.py:354
  100.5 7.7 %all_to_all.56.refs_0_ = bf16[8,8,128]{2,1,0:T(8,128)(2,1)S(1)} all-to-all(bf16[8,8,128]{2,1,0:T(8,128)(2,1)S(1)} %get-tuple-element.29), channel_id=1, replica_groups=mesh['tp_0'=8,'tp_1'=8,'dp_0'=4,'dp_1'=2] {'dp_0','dp_1'}, dimensions={0} | all-to-all | bytes 32768 | tf_op jit(solution)/shard_map/all_to_all | solution.py:365
  108.2 0.3 second_finish.1
  108.5 10.9 %all_to_all.57.refs_0_ = bf16[8,40,128]{2,1,0:T(8,128)(2,1)S(1)} all-to-all(bf16[8,40,128]{2,1,0:T(8,128)(2,1)S(1)} %second_finish.1), channel_id=1, replica_groups=mesh['tp_0'=8,'tp_1'=8,'dp_0'=4,'dp_1'=2] {'tp_1'}, dimensions={0} | all-to-all | bytes 163840 | tf_op jit(solution)/shard_map/all_to_all | solution.py:365
  119.5 10.8 %all_to_all.58.refs_0_ = bf16[8,32,128]{2,1,0:T(8,128)(2,1)S(1)} all-to-all(bf16[8,32,128]{2,1,0:T(8,128)(2,1)S(1)} %second_scale.1), channel_id=1, replica_groups=mesh['tp_0'=8,'tp_1'=8,'dp_0'=4,'dp_1'=2] {'tp_0'}, dimensions={0} | all-to-all | bytes 131072 | tf_op jit(solution)/shard_map/all_to_all | solution.py:365
  130.3 10.7 %all_to_all.59.refs_0_ = bf16[8,32,128]{2,1,0:T(8,128)(2,1)S(1)} all-to-all(bf16[8,32,128]{2,1,0:T(8,128)(2,1)S(1)} %second_combine.1), channel_id=1, replica_groups=mesh['tp_0'=8,'tp_1'=8,'dp_0'=4,'dp_1'=2] {'tp_1'}, dimensions={0} | all-to-all | bytes 131072 | tf_op jit(solution)/shard_map/all_to_all | solution.py:365
  141.0 0.7 last.1
  (12 shorter events, 0.1 us)
Async XLA Ops:
  0.6 0.8 copy-start.1
  0.6 0.9 copy-start.2
  0.7 1.0 copy-start.3
  0.7 1.1 copy-start.4
  0.7 1.1 copy-start.5
  0.7 1.1 copy-start.7
  0.7 1.1 copy-start.11
  1.2 40.9 %copy-start = (f32[2,8,2,64,128]{4,3,2,1,0:T(8,128)S(1)}, f32[2,8,2,64,128]{4,3,2,1,0:T(8,128)}, u32[]{:S(2)}) copy-start(f32[2,8,2,64,128]{4,3,2,1,0:T(8,128)} %param.37) | copy-start | bytes 3145732
  1.8 13.5 %copy-start.14 = (f32[2,2]{1,0:T(2,128)S(1)}, f32[2,2]{1,0:T(2,128)}, u32[]{:S(2)}) copy-start(f32[2,2]{1,0:T(2,128)} %refs_7_.7) | copy-start | bytes 52
  1.8 13.5 %copy-start.18 = (bf16[2,4,32]{2,1,0:T(4,128)(2,1)S(1)}, bf16[2,4,32]{2,1,0:T(4,128)(2,1)}, u32[]{:S(2)}) copy-start(bf16[2,4,32]{2,1,0:T(4,128)(2,1)} %refs_3_.4) | copy-start | bytes 1540
  2.8 12.5 %copy-start.8 = (bf16[2,8,3,128]{3,1,2,0:T(8,128)(2,1)S(1)}, bf16[2,8,3,128]{3,1,2,0:T(8,128)(2,1)}, u32[]{:S(2)}) copy-start(bf16[2,8,3,128]{3,1,2,0:T(8,128)(2,1)} %param.34) | copy-start | bytes 36868
  2.9 12.5 %copy-start.9 = (bf16[2,8,3,32]{3,1,2,0:T(8,128)(2,1)S(1)}, bf16[2,8,3,32]{3,1,2,0:T(8,128)(2,1)}, u32[]{:S(2)}) copy-start(bf16[2,8,3,32]{3,1,2,0:T(8,128)(2,1)} %param.35) | copy-start | bytes 9220
  2.9 12.5 %copy-start.10 = (bf16[2,8,3,32]{3,1,2,0:T(8,128)(2,1)S(1)}, bf16[2,8,3,32]{3,1,2,0:T(8,128)(2,1)}, u32[]{:S(2)}) copy-start(bf16[2,8,3,32]{3,1,2,0:T(8,128)(2,1)} %param.36) | copy-start | bytes 9220
  15.3 0.7 copy-start.17
  15.3 0.7 copy-start.12
  15.3 0.7 copy-start.13
  42.1 0.7 copy-start.16
  42.8 9.1 %copy-start.6 = (bf16[2,128,512]{2,1,0:T(8,128)(2,1)S(1)}, bf16[2,128,512]{2,1,0:T(8,128)(2,1)}, u32[]{:S(2)}) copy-start(bf16[2,128,512]{2,1,0:T(8,128)(2,1)} %refs_2_.13) | copy-start | bytes 786436
  44.0 7.9 %copy-start.15 = (f32[2,128]{1,0:T(2,128)S(1)}, f32[2,128]{1,0:T(2,128)}, u32[]{:S(2)}) copy-start(f32[2,128]{1,0:T(2,128)} %refs_1_.7) | copy-start | bytes 3076

commit v4 on v3

--- a/solution.py
+++ b/solution.py
@@ -57,9 +57,10 @@
     return [weights[:, 128 * q : 128 * q + 128] for q in range(4)]
 
 
-def from_groups(got):
+def from_groups(*got):
     row, col = iota((512, 512), 0), iota((512, 512), 1)
-    return dot(one_hot(col == row % 64 * 8 + row // 64), got.reshape(512, 128)).astype(BF)
+    side = jnp.concatenate([g.reshape(512, 128) for g in got], axis=1)
+    return dot(one_hot(col == row % 64 * 8 + row // 64), side).astype(BF)
 
 
 def side_by_side(rows, first):
@@ -98,8 +99,8 @@
 
 def second_project(t, got, gain, gate_w, inner_w, write_w, read_w, step_w, early, middle):
     wide = turned_back(got)
-    late = from_groups(got)
-    middle = from_groups(middle[:, 8:])
+    both = from_groups(early, middle[:, 8:], got)
+    early, middle, late = both[:, :128], both[:, 128:256], both[:, 256:]
     blocks = [late[64 * i : 64 * i + 64] for i in range(8)]
     low = iota((64, 128), 1) < 64
     pairs = []
@@ -109,7 +110,7 @@
         pairs.append(jnp.where(low, even, odd).astype(BF))
     later = jnp.concatenate(
         [
-            side_by_side(from_groups(early), 0),
+            side_by_side(early, 0),
             side_by_side(middle, 0),
             side_by_side(middle, 4),
             jnp.concatenate(pairs, axis=1),
@@ -211,25 +212,14 @@
     return message, turned, updated
 
 
-def second_scan(got, turned, conv_inner, state_inner, state_write, state_read, bias, decay, recurrent, skip, raw0):
+def second_scan(got, turned, conv_inner, state_inner, bias, decay, recurrent, skip):
     raw = arrive(got)
     inner, step, retain, gate = local_parts(raw, 1, conv_inner, state_inner, bias, decay)
     rows = turned[16:40].reshape(3, 8, 256)
     acts = convolve(rows, raw[:, 384:], turned[8:12])
     write_vec, read_vec = sort_vectors(acts)
     updated, message = scan_step(recurrent[1], inner, step, retain, gate, write_vec, read_vec, skip[1:2])
-    states = []
-    for state, low, high in ((state_inner, 128, 256), (state_write, 256, 288), (state_read, 288, 320)):
-        states.append(
-            jnp.concatenate(
-                [
-                    next_rows(state[0], raw0[:, low:high])[None],
-                    next_rows(state[1], raw[:, low:high])[None],
-                ],
-                axis=0,
-            )
-        )
-    return message, *states, updated
+    return message, raw, updated
 
 
 def partial(number, got, gain, out_w):
@@ -292,29 +282,28 @@
     return (jnp.broadcast_to(own.astype(BF)[None], (8, 32, 128)),)
 
 
-def last(got):
+def last(got, raw0, raw1, state_inner, state_write, state_read):
     turned = jnp.transpose(got.reshape(256, 128).astype(F32))
-    return (jnp.concatenate([turned[:64], turned[64:]], axis=1).astype(BF),)
-
-
-def call(fn, name, outs, *args, scalar=None):
+    outs = [jnp.concatenate([turned[:64], turned[64:]], axis=1).astype(BF)]
+    for state, low, high in ((state_inner, 128, 256), (state_write, 256, 288), (state_read, 288, 320)):
+        rows = [next_rows(state[0], raw0[:, low:high])[None], next_rows(state[1], raw1[:, low:high])[None]]
+        outs.append(jnp.concatenate(rows, axis=0))
+    return tuple(outs)
+
+
+def call(fn, name, outs, *args, placed=False):
     n_in = len(args)
 
     def kernel(*refs):
-        if scalar is not None:
-            values = [refs[0][0]] + [r[...] for r in refs[1 : 1 + n_in]]
-            dest = refs[1 + n_in :]
-        else:
-            values = [r[...] for r in refs[:n_in]]
-            dest = refs[n_in:]
+        values = [r[...] for r in refs[:n_in]]
+        dest = refs[n_in:]
+        if placed:
+            values = [lax.axis_index(Z) * 8 + lax.axis_index(Y)] + values
         for ref, value in zip(dest, fn(*values)):
             ref[...] = value
 
     whole = pl.BlockSpec(memory_space=pltpu.VMEM)
     specs = [whole] * n_in
-    if scalar is not None:
-        specs = [pl.BlockSpec(memory_space=pltpu.SMEM)] + specs
-        args = (scalar, *args)
     return pl.pallas_call(
         kernel,
         name=name,
@@ -325,8 +314,8 @@
     )(*args)
 
 
-def begin(t_ref, out_ref):
-    out_ref[0] = t_ref[0]
+def begin(out_ref):
+    out_ref[...] = jnp.zeros((8, 128), F32)
 
 
 def scan_call(fn, name, outs, args, recurrent, earlier):
@@ -335,30 +324,62 @@
     def kernel(*refs):
         values = [r[...] for r in refs[:n_in]]
         state = refs[n_in]
-        dest = refs[n_in + 1 + (earlier is not None) :]
+        if earlier is None:
+            dest = refs[n_in + 1 :]
+        else:
+            dest, whole_ref, sem = refs[n_in + 2 : -2], refs[-2], refs[-1]
+            copy = pltpu.make_async_copy(refs[n_in + 1], whole_ref.at[0], sem)
+            copy.start()
         results = fn(*values[:-1], state, values[-1])
         for ref, value in zip(dest[:-1], results[:-1]):
             ref[...] = value
-        if earlier is None:
-            for b in range(8):
-                dest[-1][b] = results[-1][b]
-        else:
-            dest[-1][0] = refs[n_in + 1][...]
-            for b in range(8):
-                dest[-1][1, b] = results[-1][b]
+        for b in range(8):
+            dest[-1][b] = results[-1][b]
+        if earlier is not None:
+            copy.wait()
 
     whole = pl.BlockSpec(memory_space=pltpu.VMEM)
     specs = [whole] * (n_in + 1 + (earlier is not None))
     operands = (*args, recurrent) + (() if earlier is None else (earlier,))
-    outs = (*outs, ((8, 128, 128) if earlier is None else (2, 8, 128, 128), F32))
+    outs = (*outs, ((8, 128, 128), F32))
+    out_specs = [whole] * len(outs)
+    if earlier is not None:
+        outs = (*outs, ((2, 8, 128, 128), F32))
+        out_specs.append(pl.BlockSpec(memory_space=pl.ANY))
     return pl.pallas_call(
         kernel,
         name=name,
         out_shape=tuple(jax.ShapeDtypeStruct(s, d) for s, d in outs),
         in_specs=specs,
-        out_specs=tuple(whole for _ in outs),
+        out_specs=tuple(out_specs),
+        scratch_shapes=[] if earlier is None else [pltpu.SemaphoreType.DMA],
         compiler_params=pltpu.CompilerParams(vmem_limit_bytes=16 * 1024 * 1024),
     )(*operands)
+
+
+def last_call(outs, args, state, whole_state):
+    n_in = len(args)
+
+    def kernel(*refs):
+        state_ref, dest, whole_ref, sem = refs[n_in], refs[n_in + 2 : -2], refs[-2], refs[-1]
+        copy = pltpu.make_async_copy(state_ref, whole_ref.at[1], sem)
+        copy.start()
+        for ref, value in zip(dest, last(*[r[...] for r in refs[:n_in]])):
+            ref[...] = value
+        copy.wait()
+
+    whole, anywhere = pl.BlockSpec(memory_space=pltpu.VMEM), pl.BlockSpec(memory_space=pl.ANY)
+    return pl.pallas_call(
+        kernel,
+        name="last",
+        out_shape=tuple(jax.ShapeDtypeStruct(s, d) for s, d in outs)
+        + (jax.ShapeDtypeStruct(whole_state.shape, F32),),
+        in_specs=[whole] * (n_in + 1) + [anywhere],
+        out_specs=tuple(whole for _ in outs) + (anywhere,),
+        input_output_aliases={n_in + 1: len(outs)},
+        scratch_shapes=[pltpu.SemaphoreType.DMA],
+        compiler_params=pltpu.CompilerParams(vmem_limit_bytes=16 * 1024 * 1024),
+    )(*args, state, whole_state)
 
 
 def exchange(pieces, axis):
@@ -386,7 +407,6 @@
     state_read,
     recurrent,
 ):
-    t = lax.axis_index(TP).astype(jnp.int32).reshape(1)
     write_weight, read_weight = jnp.swapaxes(write_weight, 1, 2), jnp.swapaxes(read_weight, 1, 2)
     state_inner, state_write, state_read = (
         jnp.swapaxes(s, 1, 2) for s in (state_inner, state_write, state_read)
@@ -394,18 +414,30 @@
     recurrent = recurrent.reshape(2, 8, 128, 128)
     weights = (gate_weight, inner_weight, write_weight, read_weight, step_weight)
 
-    t = pl.pallas_call(
+    first = pl.pallas_call(
         begin,
         name="begin",
-        out_shape=jax.ShapeDtypeStruct((1,), jnp.int32),
-        in_specs=[pl.BlockSpec(memory_space=pltpu.SMEM)],
-        out_specs=pl.BlockSpec(memory_space=pltpu.SMEM),
+        out_shape=jax.ShapeDtypeStruct((8, 128), F32),
+        out_specs=pl.BlockSpec(memory_space=pltpu.VMEM),
         cost_estimate=pl.CostEstimate(flops=20000000000, bytes_accessed=0, transcendentals=0),
         compiler_params=pltpu.CompilerParams(vmem_limit_bytes=1024 * 1024),
-    )(t)
-    out, own = call(
-        first_project, "first_project", (((64, 384), BF), ((8, 128), F32)), hidden, norm_gain, *weights, scalar=t
-    )
+    )()
+    small = (conv_inner, conv_write, conv_read, step_bias, decay_log, skip_gain, group_gain)
+    out, own, *small = call(
+        lambda t, first, hidden, gain, gate, inner, write, read, step, *small: (
+            *first_project(t, hidden, gain, gate, inner, write, read, step),
+            *small,
+        ),
+        "first_project",
+        (((64, 384), BF), ((8, 128), F32)) + tuple((a.shape, a.dtype) for a in small),
+        first,
+        hidden,
+        norm_gain,
+        *weights,
+        *small,
+        placed=True,
+    )
+    conv_inner, conv_write, conv_read, step_bias, decay_log, skip_gain, group_gain = small
     got = exchange(out.reshape(8, 8, 384), DP)
     message, parts, raw0 = call(
         first_states,
@@ -448,16 +480,14 @@
         *weights,
         early,
         middle,
-        scalar=t,
+        placed=True,
     )
     got = exchange(out.reshape(8, 8, 640), DP)
-    message, next_inner, next_write, next_read, updated = scan_call(
-        lambda got, turned, ci, si, sw, sr, bias, decay, raw0, state, skip: second_scan(
-            got, turned, ci, si, sw, sr, bias, decay, state, skip, raw0
-        ),
+    message, raw1, second, updated = scan_call(
+        second_scan,
         "second_scan",
-        (((8, 8, 128), BF), ((2, 3, 8, 128), BF), ((2, 3, 8, 32), BF), ((2, 3, 8, 32), BF)),
-        (got, turned, conv_inner, state_inner, state_write, state_read, step_bias, decay_log, raw0, skip_gain),
+        (((8, 8, 128), BF), ((8, 640), BF)),
+        (got, turned, conv_inner, state_inner, step_bias, decay_log, skip_gain),
         recurrent,
         updated,
     )
@@ -468,7 +498,12 @@
     got = exchange(out, Z)
     (out,) = call(second_combine, "second_combine", (((8, 32, 128), BF),), got, own)
     got = exchange(out, Y)
-    (result,) = call(last, "last", (((64, 512), BF),), got)
+    result, next_inner, next_write, next_read, updated = last_call(
+        (((64, 512), BF), ((2, 3, 8, 128), BF), ((2, 3, 8, 32), BF), ((2, 3, 8, 32), BF)),
+        (got, raw0, raw1, state_inner, state_write, state_read),
+        second,
+        updated,
+    )
     return (
         result,
         jnp.swapaxes(next_inner, 1, 2),

time: 142 us -> 140 us (0.986)
  Pallas kernels: 9.3 us -> 7.72 us
    pallas_call x9 -> x8, Pallas kernels: 5.43 us -> 3.17 us  [call(): pl.pallas_call(kernel, name=name, out_shape=tuple((jax.ShapeDtypeStruct(s...]
where the time goes in v4:
time: 140 us
  blocking collectives  129 us (92%)
  Pallas kernels  7.72 us (6%)
  local copies, waits for them, and re-layouts  1.73 us (1%)
    all_to_all x10, blocking collectives, exchange(): return lax.all_to_all(pieces, axis, 0, 0, tiled=True)  129 us
    pallas_call x8, Pallas kernels, call(): pl.pallas_call(kernel, name=name, out_shape=tuple((jax.ShapeDtypeStruct(s...  3.17 us
    pallas_call x2, Pallas kernels, scan_call(): pl.pallas_call(kernel, name=name, out_shape=tuple((jax.ShapeDtypeStruct(s...  3.1 us

profile of v4, /device:TPU:2, one launch (start us, length us, event | category | flops | bytes accessed | tf_op | source)
XLA Modules:
  0.0 139.7 jit_solution(8679722775766474023)
XLA Ops:
  0.6 0.0 copy-start.6
  0.6 0.0 copy-start.5
  0.7 0.0 copy-start.4
  0.7 0.0 copy-start.2
  0.7 0.0 copy-start.1
  0.7 0.0 copy-start.8
  0.7 0.0 copy-start.11
  0.7 0.0 copy-start.12
  0.7 0.0 copy-start.13
  0.7 0.0 copy-start.14
  0.7 0.0 copy-start.15
  0.7 0.0 copy-start.16
  0.8 0.0 copy-start.17
  0.8 0.0 copy-start.18
  0.8 0.0 copy-start
  0.8 0.8 copy-done.6
  1.6 0.1 copy-done.5
  1.7 0.1 copy-done.4
  1.8 0.0 copy-done.2
  1.8 0.0 copy-done.1
  1.8 0.0 copy-done.8
  1.8 0.0 copy-done.11
  1.8 0.0 copy-done.12
  1.8 0.0 copy-done.13
  1.8 0.0 copy-done.14
  1.8 0.3 first_project.1
  2.2 0.0 copy-start.9
  2.2 0.0 copy-start.10
  2.2 12.3 %all_to_all.50.refs_0_ = bf16[8,8,384]{2,1,0:T(8,128)(2,1)S(1)} all-to-all(bf16[8,8,384]{2,1,0:T(8,128)(2,1)S(1)} %bitcast.32), channel_id=1, replica_groups=mesh['tp_0'=8,'tp_1'=8,'dp_0'=4,'dp_1'=2] {'dp_0','dp_1'}, dimensions={0} | all-to-all | bytes 98304 | tf_op jit(solution)/shard_map/all_to_all | solution.py:386
  14.5 0.7 copy-done.7
  15.2 0.6 first_states.1
  15.8 25.5 %all_to_all.51.refs_0_.refs_7_ = bf16[64,8,128]{2,1,0:T(8,128)(2,1)S(1)} all-to-all(bf16[64,8,128]{2,1,0:T(8,128)(2,1)S(1)} %get-tuple-element.37), channel_id=1, replica_groups=mesh['tp_0'=8,'tp_1'=8,'dp_0'=4,'dp_1'=2] {'tp_0','tp_1'}, dimensions={0} | all-to-all | bytes 262144 | tf_op jit(solution)/shard_map/all_to_all | solution.py:386
  41.3 0.0 copy-done
  41.3 1.2 first_scan.1
  42.5 7.7 %all_to_all.52.refs_0_ = bf16[8,8,128]{2,1,0:T(8,128)(2,1)S(1)} all-to-all(bf16[8,8,128]{2,1,0:T(8,128)(2,1)S(1)} %get-tuple-element.40), channel_id=1, replica_groups=mesh['tp_0'=8,'tp_1'=8,'dp_0'=4,'dp_1'=2] {'dp_0','dp_1'}, dimensions={0} | all-to-all | bytes 32768 | tf_op jit(solution)/shard_map/all_to_all | solution.py:386
  50.2 0.6 first_finish.1
  50.9 19.0 %all_to_all.53.refs_0_.refs_8_ = bf16[64,16,128]{2,1,0:T(8,128)(2,1)S(1)} all-to-all(bf16[64,16,128]{2,1,0:T(8,128)(2,1)S(1)} %first_finish.1), channel_id=1, replica_groups=mesh['tp_0'=8,'tp_1'=8,'dp_0'=4,'dp_1'=2] {'tp_0','tp_1'}, dimensions={0} | all-to-all | bytes 524288 | tf_op jit(solution)/shard_map/all_to_all | solution.py:386
  69.8 0.5 first_combine.1
  70.3 16.7 %all_to_all.54.refs_0_ = bf16[64,8,128]{2,1,0:T(8,128)(2,1)S(1)} all-to-all(bf16[64,8,128]{2,1,0:T(8,128)(2,1)S(1)} %first_combine.1), channel_id=1, replica_groups=mesh['tp_0'=8,'tp_1'=8,'dp_0'=4,'dp_1'=2] {'tp_0','tp_1'}, dimensions={0} | all-to-all | bytes 262144 | tf_op jit(solution)/shard_map/all_to_all | solution.py:386
  87.0 0.7 second_project.1
  87.8 8.1 %all_to_all.55.refs_0_ = bf16[8,8,640]{2,1,0:T(8,128)(2,1)S(1)} all-to-all(bf16[8,8,640]{2,1,0:T(8,128)(2,1)S(1)} %bitcast.27), channel_id=1, replica_groups=mesh['tp_0'=8,'tp_1'=8,'dp_0'=4,'dp_1'=2] {'dp_0','dp_1'}, dimensions={0} | all-to-all | bytes 163840 | tf_op jit(solution)/shard_map/all_to_all | solution.py:386
  95.8 1.9 %second_scan.1 = (bf16[8,8,128]{2,1,0:T(8,128)(2,1)S(1)}, bf16[8,640]{1,0:T(8,128)(2,1)S(1)}, f32[8,128,128]{2,1,0:T(8,128)S(1)}, f32[2,8,128,128]{3,2,1,0:T(8,128)}) custom-call(bf16[8,8,640]{2,1,0:T(8,128)(2,1)S(1)} %all_to_all.55.refs_0_, f32[40,256]{1,0:T(8,128)S(1)} %get-tuple-element.44.refs_1_, ...), custom_call_target="tpu_custom_call" | custom-call | tf_op jit(solution)/shard_map/second_scan/pallas_call | solution.py:349
  97.8 7.7 %all_to_all.56.refs_0_ = bf16[8,8,128]{2,1,0:T(8,128)(2,1)S(1)} all-to-all(bf16[8,8,128]{2,1,0:T(8,128)(2,1)S(1)} %get-tuple-element.46), channel_id=1, replica_groups=mesh['tp_0'=8,'tp_1'=8,'dp_0'=4,'dp_1'=2] {'dp_0','dp_1'}, dimensions={0} | all-to-all | bytes 32768 | tf_op jit(solution)/shard_map/all_to_all | solution.py:386
  105.5 0.3 second_finish.1
  105.8 10.9 %all_to_all.57.refs_0_ = bf16[8,40,128]{2,1,0:T(8,128)(2,1)S(1)} all-to-all(bf16[8,40,128]{2,1,0:T(8,128)(2,1)S(1)} %second_finish.1), channel_id=1, replica_groups=mesh['tp_0'=8,'tp_1'=8,'dp_0'=4,'dp_1'=2] {'tp_1'}, dimensions={0} | all-to-all | bytes 163840 | tf_op jit(solution)/shard_map/all_to_all | solution.py:386
  116.8 10.8 %all_to_all.58.refs_0_ = bf16[8,32,128]{2,1,0:T(8,128)(2,1)S(1)} all-to-all(bf16[8,32,128]{2,1,0:T(8,128)(2,1)S(1)} %second_scale.1), channel_id=1, replica_groups=mesh['tp_0'=8,'tp_1'=8,'dp_0'=4,'dp_1'=2] {'tp_0'}, dimensions={0} | all-to-all | bytes 131072 | tf_op jit(solution)/shard_map/all_to_all | solution.py:386
  127.5 10.7 %all_to_all.59.refs_0_ = bf16[8,32,128]{2,1,0:T(8,128)(2,1)S(1)} all-to-all(bf16[8,32,128]{2,1,0:T(8,128)(2,1)S(1)} %second_combine.1), channel_id=1, replica_groups=mesh['tp_0'=8,'tp_1'=8,'dp_0'=4,'dp_1'=2] {'tp_1'}, dimensions={0} | all-to-all | bytes 131072 | tf_op jit(solution)/shard_map/all_to_all | solution.py:386
  138.3 1.4 %last.1 = (bf16[64,512]{1,0:T(8,128)(2,1)}, bf16[2,3,8,128]{3,2,1,0:T(8,128)(2,1)}, bf16[2,3,8,32]{3,2,1,0:T(8,128)(2,1)}, bf16[2,3,8,32]{3,2,1,0:T(8,128)(2,1)}, f32[2,8,128,128]{3,2,1,0:T(8,128)}) custom-call(bf16[8,32,128]{2,1,0:T(8,128)(2,1)S(1)} %all_to_all.59.refs_0_, ...), custom_call_target="tpu_custom_call", output_to_operand_aliasing={{4}: (7, {})} | custom-call | tf_op jit(solution)/shard_map/last/pallas_call | solution.py:372
  (12 shorter events, 0.1 us)
Async XLA Ops:
  0.6 1.0 copy-start.6
  0.6 1.0 copy-start.5
  0.7 1.1 copy-start.4
  0.7 1.1 copy-start.2
  0.7 1.1 copy-start.1
  0.7 1.1 copy-start.8
  0.7 1.1 copy-start.11
  0.7 1.1 copy-start.12
  0.7 1.1 copy-start.13
  0.7 1.1 copy-start.14
  0.7 1.1 copy-start.15
  0.7 1.1 copy-start.16
  0.8 1.1 copy-start.17
  0.8 1.1 copy-start.18
  0.8 40.5 %copy-start = (f32[2,8,2,64,128]{4,3,2,1,0:T(8,128)S(1)}, f32[2,8,2,64,128]{4,3,2,1,0:T(8,128)}, u32[]{:S(2)}) copy-start(f32[2,8,2,64,128]{4,3,2,1,0:T(8,128)} %param.37) | copy-start | bytes 3145732
  2.2 12.4 %copy-start.9 = (bf16[2,8,3,32]{3,1,2,0:T(8,128)(2,1)S(1)}, bf16[2,8,3,32]{3,1,2,0:T(8,128)(2,1)}, u32[]{:S(2)}) copy-start(bf16[2,8,3,32]{3,1,2,0:T(8,128)(2,1)} %param.35) | copy-start | bytes 9220
  2.2 12.3 %copy-start.10 = (bf16[2,8,3,32]{3,1,2,0:T(8,128)(2,1)S(1)}, bf16[2,8,3,32]{3,1,2,0:T(8,128)(2,1)}, u32[]{:S(2)}) copy-start(bf16[2,8,3,32]{3,1,2,0:T(8,128)(2,1)} %param.36) | copy-start | bytes 9220
  14.5 0.7 copy-start.7
  41.3 8.9 %copy-start.3 = (bf16[2,128,512]{2,1,0:T(8,128)(2,1)S(1)}, bf16[2,128,512]{2,1,0:T(8,128)(2,1)}, u32[]{:S(2)}) copy-start(bf16[2,128,512]{2,1,0:T(8,128)(2,1)} %refs_2_.7) | copy-start | bytes 786436

commit v5 on v4

--- a/solution.py
+++ b/solution.py
@@ -97,9 +97,9 @@
     return jnp.transpose(got.reshape(512, 128).astype(F32))[:64]
 
 
-def second_project(t, got, gain, gate_w, inner_w, write_w, read_w, step_w, early, middle):
+def second_project(t, got, gain, gate_w, inner_w, write_w, read_w, step_w, early):
     wide = turned_back(got)
-    both = from_groups(early, middle[:, 8:], got)
+    both = from_groups(early[:, :8], early[:, 8:], got)
     early, middle, late = both[:, :128], both[:, 128:256], both[:, 256:]
     blocks = [late[64 * i : 64 * i + 64] for i in range(8)]
     low = iota((64, 128), 1) < 64
@@ -111,8 +111,8 @@
     later = jnp.concatenate(
         [
             side_by_side(early, 0),
+            side_by_side(early, 4),
             side_by_side(middle, 0),
-            side_by_side(middle, 4),
             jnp.concatenate(pairs, axis=1),
         ],
         axis=0,
@@ -176,8 +176,11 @@
     row, col = iota((512, 64), 0), iota((512, 64), 1)
     spread = one_hot((row % 8 >= 4) & (col == channel(row % 8 - 4, row // 32)))
     weights = jnp.concatenate([write_w[1], read_w[1]], axis=0)
-    message = to_groups(lambda j: 0 * j, quarters(weights), lambda j: j) + dot_rows(spread, extras)
-    message = message.astype(BF).reshape(64, 8, 128)
+    blocks = quarters(weights)
+    early = to_groups(lambda j: j // 4, blocks, lambda j: j % 4)
+    late = to_groups(lambda j: 0 * j + 2, blocks, lambda j: j) + dot_rows(spread, extras)
+    message = [m.astype(BF).reshape(64, 8, 128) for m in (early, late)]
+    message = jnp.concatenate(message, axis=1)
     return message, jnp.concatenate([inner, step, retain, gate], axis=0), raw
 
 
@@ -203,7 +206,7 @@
 
 def first_scan(got, parts, recurrent, skip):
     row, col = iota((256, 512), 0), iota((256, 512), 1)
-    extras = dot(one_hot(col == row % 64 * 8 + 4 + row // 64), got.reshape(512, 128))
+    extras = dot(one_hot(col == row % 64 * 8 + 4 + row // 64), got[:, 8:].reshape(512, 128))
     turned = jnp.transpose(extras)[:40]
     write_vec, read_vec = sort_vectors(turned[:8])
     updated, message = scan_step(
@@ -229,18 +232,16 @@
     return jnp.transpose(jnp.concatenate([part, jnp.broadcast_to(squares, (64, 512))], axis=0))
 
 
-def first_finish(got, gain, out_w, write_w, read_w):
+def first_finish(got, gain, out_w):
     turned = partial(0, got, gain, out_w)
     high = rounded(turned)
     lane, row = iota((512, 128), 1), iota((512, 128), 0)
     out = jnp.where((lane < 64) | (row % 8 < 4), turned, turned - high).astype(BF)
-    weights = jnp.concatenate([write_w[1], read_w[1]], axis=0)
-    beside = to_groups(lambda j: 1 + j // 4, quarters(weights), lambda j: j % 4).astype(BF)
-    return (jnp.concatenate([out.reshape(64, 8, 128), beside.reshape(64, 8, 128)], axis=1),)
+    return (out.reshape(64, 8, 128),)
 
 
 def first_combine(got, own, write_w, read_w):
-    some = got[:, :8].astype(F32).reshape(16, 4, 8, 128)
+    some = got.astype(F32).reshape(16, 4, 8, 128)
     some = some[:, 0] + some[:, 1] + some[:, 2] + some[:, 3]
     both = some + jnp.concatenate([some[:, 4:], some[:, :4]], axis=1)
     factor = lax.rsqrt(both / 512 + EPS)
@@ -318,6 +319,13 @@
     out_ref[...] = jnp.zeros((8, 128), F32)
 
 
+def start_copies(source, dest, sems):
+    copies = [pltpu.make_async_copy(source.at[b], dest.at[b], sems.at[b]) for b in range(8)]
+    for copy in copies:
+        copy.start()
+    return copies
+
+
 def scan_call(fn, name, outs, args, recurrent, earlier):
     n_in = len(args)
 
@@ -328,15 +336,15 @@
             dest = refs[n_in + 1 :]
         else:
             dest, whole_ref, sem = refs[n_in + 2 : -2], refs[-2], refs[-1]
-            copy = pltpu.make_async_copy(refs[n_in + 1], whole_ref.at[0], sem)
-            copy.start()
+            copies = start_copies(refs[n_in + 1], whole_ref.at[0], sem)
         results = fn(*values[:-1], state, values[-1])
         for ref, value in zip(dest[:-1], results[:-1]):
             ref[...] = value
         for b in range(8):
             dest[-1][b] = results[-1][b]
         if earlier is not None:
-            copy.wait()
+            for copy in copies:
+                copy.wait()
 
     whole = pl.BlockSpec(memory_space=pltpu.VMEM)
     specs = [whole] * (n_in + 1 + (earlier is not None))
@@ -352,7 +360,7 @@
         out_shape=tuple(jax.ShapeDtypeStruct(s, d) for s, d in outs),
         in_specs=specs,
         out_specs=tuple(out_specs),
-        scratch_shapes=[] if earlier is None else [pltpu.SemaphoreType.DMA],
+        scratch_shapes=[] if earlier is None else [pltpu.SemaphoreType.DMA((8,))],
         compiler_params=pltpu.CompilerParams(vmem_limit_bytes=16 * 1024 * 1024),
     )(*operands)
 
@@ -362,11 +370,11 @@
 
     def kernel(*refs):
         state_ref, dest, whole_ref, sem = refs[n_in], refs[n_in + 2 : -2], refs[-2], refs[-1]
-        copy = pltpu.make_async_copy(state_ref, whole_ref.at[1], sem)
-        copy.start()
+        copies = start_copies(state_ref, whole_ref.at[1], sem)
         for ref, value in zip(dest, last(*[r[...] for r in refs[:n_in]])):
             ref[...] = value
-        copy.wait()
+        for copy in copies:
+            copy.wait()
 
     whole, anywhere = pl.BlockSpec(memory_space=pltpu.VMEM), pl.BlockSpec(memory_space=pl.ANY)
     return pl.pallas_call(
@@ -377,7 +385,7 @@
         in_specs=[whole] * (n_in + 1) + [anywhere],
         out_specs=tuple(whole for _ in outs) + (anywhere,),
         input_output_aliases={n_in + 1: len(outs)},
-        scratch_shapes=[pltpu.SemaphoreType.DMA],
+        scratch_shapes=[pltpu.SemaphoreType.DMA((8,))],
         compiler_params=pltpu.CompilerParams(vmem_limit_bytes=16 * 1024 * 1024),
     )(*args, state, whole_state)
 
@@ -423,6 +431,7 @@
         compiler_params=pltpu.CompilerParams(vmem_limit_bytes=1024 * 1024),
     )()
     small = (conv_inner, conv_write, conv_read, step_bias, decay_log, skip_gain, group_gain)
+    small = (*small, state_inner, state_write, state_read)
     out, own, *small = call(
         lambda t, first, hidden, gain, gate, inner, write, read, step, *small: (
             *first_project(t, hidden, gain, gate, inner, write, read, step),
@@ -437,12 +446,13 @@
         *small,
         placed=True,
     )
-    conv_inner, conv_write, conv_read, step_bias, decay_log, skip_gain, group_gain = small
+    conv_inner, conv_write, conv_read, step_bias, decay_log, skip_gain, group_gain = small[:7]
+    state_inner, state_write, state_read = small[7:]
     got = exchange(out.reshape(8, 8, 384), DP)
     message, parts, raw0 = call(
         first_states,
         "first_states",
-        (((64, 8, 128), BF), ((32, 128), F32), ((8, 384), BF)),
+        (((64, 16, 128), BF), ((32, 128), F32), ((8, 384), BF)),
         got,
         conv_inner,
         conv_write,
@@ -465,11 +475,9 @@
         None,
     )
     got = exchange(message, DP)
-    (out,) = call(
-        first_finish, "first_finish", (((64, 16, 128), BF),), got, group_gain, out_weight, write_weight, read_weight
-    )
-    middle = exchange(out, TP)
-    (out,) = call(first_combine, "first_combine", (((64, 8, 128), BF),), middle, own, write_weight, read_weight)
+    (out,) = call(first_finish, "first_finish", (((64, 8, 128), BF),), got, group_gain, out_weight)
+    got = exchange(out, TP)
+    (out,) = call(first_combine, "first_combine", (((64, 8, 128), BF),), got, own, write_weight, read_weight)
     got = exchange(out, TP)
     out, own = call(
         second_project,
@@ -479,7 +487,6 @@
         norm_gain,
         *weights,
         early,
-        middle,
         placed=True,
     )
     got = exchange(out.reshape(8, 8, 640), DP)

time: 140 us -> 139 us (level)
  no operation moved by 1% of the time
where the time goes in v5:
time: 139 us
  blocking collectives  129 us (93%)
  Pallas kernels  7.85 us (6%)
    all_to_all x10, blocking collectives, exchange(): return lax.all_to_all(pieces, axis, 0, 0, tiled=True)  129 us
    pallas_call x8, Pallas kernels, call(): pl.pallas_call(kernel, name=name, out_shape=tuple((jax.ShapeDtypeStruct(s...  3.31 us
    pallas_call x2, Pallas kernels, scan_call(): pl.pallas_call(kernel, name=name, out_shape=tuple((jax.ShapeDtypeStruct(s...  3.05 us

profile of v5, /device:TPU:2, one launch (start us, length us, event | category | flops | bytes accessed | tf_op | source)
XLA Modules:
  0.0 138.9 jit_solution(1185018620537106103)
XLA Ops:
  0.6 0.0 copy-start.5
  0.6 0.0 copy-start.4
  0.7 0.0 copy-start.3
  0.7 0.0 copy-start.2
  0.7 0.0 copy-start.1
  0.7 0.0 copy-start.7
  0.7 0.0 copy-start.8
  0.7 0.0 copy-start.9
  0.7 0.0 copy-start.10
  0.7 0.0 copy-start.11
  0.7 0.0 copy-start.12
  0.7 0.0 copy-start.13
  0.8 0.0 copy-start.14
  0.8 0.0 copy-start.15
  0.8 0.0 copy-start.16
  0.8 0.0 copy-start.17
  0.8 0.0 copy-start.18
  0.8 0.0 copy-start
  0.8 0.8 copy-done.5
  1.6 0.1 copy-done.4
  1.7 0.1 copy-done.3
  1.8 0.0 copy-done.2
  1.8 0.0 copy-done.1
  1.8 0.0 copy-done.7
  1.8 0.0 copy-done.8
  1.8 0.0 copy-done.9
  1.8 0.0 copy-done.10
  1.8 0.0 copy-done.11
  1.8 0.0 copy-done.12
  1.9 0.3 first_project.1
  2.2 12.3 %all_to_all.50.refs_0_ = bf16[8,8,384]{2,1,0:T(8,128)(2,1)S(1)} all-to-all(bf16[8,8,384]{2,1,0:T(8,128)(2,1)S(1)} %bitcast.23), channel_id=1, replica_groups=mesh['tp_0'=8,'tp_1'=8,'dp_0'=4,'dp_1'=2] {'dp_0','dp_1'}, dimensions={0} | all-to-all | bytes 98304 | tf_op jit(solution)/shard_map/all_to_all | solution.py:394
  14.6 1.1 first_states.1
  15.6 27.6 %all_to_all.51.refs_0_.refs_7_ = bf16[64,16,128]{2,1,0:T(8,128)(2,1)S(1)} all-to-all(bf16[64,16,128]{2,1,0:T(8,128)(2,1)S(1)} %get-tuple-element.43), channel_id=1, replica_groups=mesh['tp_0'=8,'tp_1'=8,'dp_0'=4,'dp_1'=2] {'tp_0','tp_1'}, dimensions={0} | all-to-all | bytes 524288 | tf_op jit(solution)/shard_map/all_to_all | solution.py:394
  43.2 1.2 first_scan.1
  44.4 7.7 %all_to_all.52.refs_0_ = bf16[8,8,128]{2,1,0:T(8,128)(2,1)S(1)} all-to-all(bf16[8,8,128]{2,1,0:T(8,128)(2,1)S(1)} %get-tuple-element.46), channel_id=1, replica_groups=mesh['tp_0'=8,'tp_1'=8,'dp_0'=4,'dp_1'=2] {'dp_0','dp_1'}, dimensions={0} | all-to-all | bytes 32768 | tf_op jit(solution)/shard_map/all_to_all | solution.py:394
  52.2 0.3 first_finish.1
  52.4 16.7 %all_to_all.53.refs_0_ = bf16[64,8,128]{2,1,0:T(8,128)(2,1)S(1)} all-to-all(bf16[64,8,128]{2,1,0:T(8,128)(2,1)S(1)} %first_finish.1), channel_id=1, replica_groups=mesh['tp_0'=8,'tp_1'=8,'dp_0'=4,'dp_1'=2] {'tp_0','tp_1'}, dimensions={0} | all-to-all | bytes 262144 | tf_op jit(solution)/shard_map/all_to_all | solution.py:394
  69.1 0.5 first_combine.1
  69.7 16.6 %all_to_all.54.refs_0_ = bf16[64,8,128]{2,1,0:T(8,128)(2,1)S(1)} all-to-all(bf16[64,8,128]{2,1,0:T(8,128)(2,1)S(1)} %first_combine.1), channel_id=1, replica_groups=mesh['tp_0'=8,'tp_1'=8,'dp_0'=4,'dp_1'=2] {'tp_0','tp_1'}, dimensions={0} | all-to-all | bytes 262144 | tf_op jit(solution)/shard_map/all_to_all | solution.py:394
  86.2 0.7 second_project.1
  86.9 8.1 %all_to_all.55.refs_0_ = bf16[8,8,640]{2,1,0:T(8,128)(2,1)S(1)} all-to-all(bf16[8,8,640]{2,1,0:T(8,128)(2,1)S(1)} %bitcast.22), channel_id=1, replica_groups=mesh['tp_0'=8,'tp_1'=8,'dp_0'=4,'dp_1'=2] {'dp_0','dp_1'}, dimensions={0} | all-to-all | bytes 163840 | tf_op jit(solution)/shard_map/all_to_all | solution.py:394
  95.0 1.9 %second_scan.1 = (bf16[8,8,128]{2,1,0:T(8,128)(2,1)S(1)}, bf16[8,640]{1,0:T(8,128)(2,1)S(1)}, f32[8,128,128]{2,1,0:T(8,128)S(1)}, f32[2,8,128,128]{3,2,1,0:T(8,128)}) custom-call(bf16[8,8,640]{2,1,0:T(8,128)(2,1)S(1)} %all_to_all.55.refs_0_, f32[40,256]{1,0:T(8,128)S(1)} %get-tuple-element.50.refs_1_, ...), custom_call_target="tpu_custom_call" | custom-call | tf_op jit(solution)/shard_map/second_scan/pallas_call | solution.py:357
  96.9 7.7 %all_to_all.56.refs_0_ = bf16[8,8,128]{2,1,0:T(8,128)(2,1)S(1)} all-to-all(bf16[8,8,128]{2,1,0:T(8,128)(2,1)S(1)} %get-tuple-element.52), channel_id=1, replica_groups=mesh['tp_0'=8,'tp_1'=8,'dp_0'=4,'dp_1'=2] {'dp_0','dp_1'}, dimensions={0} | all-to-all | bytes 32768 | tf_op jit(solution)/shard_map/all_to_all | solution.py:394
  104.6 0.3 second_finish.1
  105.0 10.9 %all_to_all.57.refs_0_ = bf16[8,40,128]{2,1,0:T(8,128)(2,1)S(1)} all-to-all(bf16[8,40,128]{2,1,0:T(8,128)(2,1)S(1)} %second_finish.1), channel_id=1, replica_groups=mesh['tp_0'=8,'tp_1'=8,'dp_0'=4,'dp_1'=2] {'tp_1'}, dimensions={0} | all-to-all | bytes 163840 | tf_op jit(solution)/shard_map/all_to_all | solution.py:394
  115.9 10.8 %all_to_all.58.refs_0_ = bf16[8,32,128]{2,1,0:T(8,128)(2,1)S(1)} all-to-all(bf16[8,32,128]{2,1,0:T(8,128)(2,1)S(1)} %second_scale.1), channel_id=1, replica_groups=mesh['tp_0'=8,'tp_1'=8,'dp_0'=4,'dp_1'=2] {'tp_0'}, dimensions={0} | all-to-all | bytes 131072 | tf_op jit(solution)/shard_map/all_to_all | solution.py:394
  126.7 10.8 %all_to_all.59.refs_0_ = bf16[8,32,128]{2,1,0:T(8,128)(2,1)S(1)} all-to-all(bf16[8,32,128]{2,1,0:T(8,128)(2,1)S(1)} %second_combine.1), channel_id=1, replica_groups=mesh['tp_0'=8,'tp_1'=8,'dp_0'=4,'dp_1'=2] {'tp_1'}, dimensions={0} | all-to-all | bytes 131072 | tf_op jit(solution)/shard_map/all_to_all | solution.py:394
  137.5 1.5 %last.1 = (bf16[64,512]{1,0:T(8,128)(2,1)}, bf16[2,3,8,128]{3,2,1,0:T(8,128)(2,1)}, bf16[2,3,8,32]{3,2,1,0:T(8,128)(2,1)}, bf16[2,3,8,32]{3,2,1,0:T(8,128)(2,1)}, f32[2,8,128,128]{3,2,1,0:T(8,128)}) custom-call(bf16[8,32,128]{2,1,0:T(8,128)(2,1)S(1)} %all_to_all.59.refs_0_, ...), custom_call_target="tpu_custom_call", output_to_operand_aliasing={{4}: (7, {})} | custom-call | tf_op jit(solution)/shard_map/last/pallas_call | solution.py:380
  (12 shorter events, 0.1 us)
Async XLA Ops:
  0.6 1.0 copy-start.5
  0.6 1.0 copy-start.4
  0.7 1.1 copy-start.3
  0.7 1.1 copy-start.2
  0.7 1.1 copy-start.1
  0.7 1.1 copy-start.7
  0.7 1.1 copy-start.8
  0.7 1.1 copy-start.9
  0.7 1.1 copy-start.10
  0.7 1.1 copy-start.11
  0.7 1.1 copy-start.12
  0.7 1.1 copy-start.13
  0.8 1.1 copy-start.14
  0.8 1.1 copy-start.15
  0.8 1.1 copy-start.16
  0.8 1.1 copy-start.17
  0.8 1.1 copy-start.18
  0.8 42.4 %copy-start = (f32[2,8,2,64,128]{4,3,2,1,0:T(8,128)S(1)}, f32[2,8,2,64,128]{4,3,2,1,0:T(8,128)}, u32[]{:S(2)}) copy-start(f32[2,8,2,64,128]{4,3,2,1,0:T(8,128)} %param.37) | copy-start | bytes 3145732
  43.2 8.9 %copy-start.6 = (bf16[2,128,512]{2,1,0:T(8,128)(2,1)S(1)}, bf16[2,128,512]{2,1,0:T(8,128)(2,1)}, u32[]{:S(2)}) copy-start(bf16[2,128,512]{2,1,0:T(8,128)(2,1)} %refs_2_.7) | copy-start | bytes 786436

commit v6 on v5

--- a/solution.py
+++ b/solution.py
@@ -65,6 +65,18 @@
 
 def side_by_side(rows, first):
     return jnp.concatenate([rows[64 * j : 64 * j + 64] for j in range(first, first + 4)], axis=1)
+
+
+def spread(first, write_w, read_w):
+    weights = jnp.concatenate([write_w[1], read_w[1]], axis=0)
+    rolled = jnp.concatenate([weights[:, 64:], weights[:, :64]], axis=1)
+    odd, even = quarters(weights), quarters(rolled)
+    halves = [odd[i // 2] if i % 2 else even[(i // 2 + 3) % 4] for i in range(8)]
+    early = to_groups(lambda j: j // 4, odd, lambda j: j % 4)
+    late = to_groups(lambda j: 0 * j + 2, odd, lambda j: j)
+    message = jnp.concatenate([m.astype(BF).reshape(64, 8, 128) for m in (early, late)], axis=1)
+    beside = to_groups(lambda j: 0 * j + 3, halves, lambda j: j)
+    return message, beside.astype(BF).reshape(64, 8, 128)
 
 
 def project(t, wide, gain, gate_w, inner_w, write_w, read_w, step_w, extra):
@@ -157,7 +169,7 @@
     return jnp.concatenate([state[1:], fresh[None]], axis=0)
 
 
-def first_states(got, conv_inner, conv_write, conv_read, state_inner, state_write, state_read, bias, decay, write_w, read_w):
+def first_states(got, conv_inner, conv_write, conv_read, state_inner, state_write, state_read, bias, decay, early):
     raw = arrive(got)
     inner, step, retain, gate = local_parts(raw, 0, conv_inner, state_inner, bias, decay)
     vec_state = jnp.concatenate([state_write, state_read], axis=3).astype(F32)
@@ -174,13 +186,9 @@
         axis=0,
     ).astype(BF)
     row, col = iota((512, 64), 0), iota((512, 64), 1)
-    spread = one_hot((row % 8 >= 4) & (col == channel(row % 8 - 4, row // 32)))
-    weights = jnp.concatenate([write_w[1], read_w[1]], axis=0)
-    blocks = quarters(weights)
-    early = to_groups(lambda j: j // 4, blocks, lambda j: j % 4)
-    late = to_groups(lambda j: 0 * j + 2, blocks, lambda j: j) + dot_rows(spread, extras)
-    message = [m.astype(BF).reshape(64, 8, 128) for m in (early, late)]
-    message = jnp.concatenate(message, axis=1)
+    here = one_hot((row % 8 >= 4) & (col == channel(row % 8 - 4, row // 32)))
+    late = dot_rows(here, extras).reshape(64, 8, 128) + early[:, 8:].astype(F32)
+    message = jnp.concatenate([early[:, :8], late.astype(BF)], axis=1)
     return message, jnp.concatenate([inner, step, retain, gate], axis=0), raw
 
 
@@ -192,11 +200,12 @@
 
 
 def scan_step(recurrent, inner, step, retain, gate, write_vec, read_vec, skip):
-    turned = jnp.transpose(jnp.concatenate([step * inner, retain, jnp.zeros((112, 128), F32)], axis=0))
+    turned = jnp.transpose(jnp.concatenate([step * inner, jnp.zeros((120, 128), F32)], axis=0))
     lane = iota((128, 128), 1)
     updated, reads = [], jnp.zeros((128, 128), F32)
     for b in range(8):
-        new = turned[:, 8 + b : 9 + b] * recurrent[b] + turned[:, b : b + 1] * write_vec[b : b + 1]
+        kept = [jnp.broadcast_to(retain[b : b + 1, c : c + 1], (64, 128)) for c in (0, 64)]
+        new = jnp.concatenate(kept, axis=0) * recurrent[b] + turned[:, b : b + 1] * write_vec[b : b + 1]
         updated.append(new)
         reads = jnp.where(lane == b, jnp.sum(new * read_vec[b : b + 1], axis=1, keepdims=True), reads)
     readout = jnp.transpose(reads)[:8] + by_head(jnp.broadcast_to(skip, (8, 2))) * inner
@@ -240,20 +249,15 @@
     return (out.reshape(64, 8, 128),)
 
 
-def first_combine(got, own, write_w, read_w):
+def first_combine(got, own, beside):
     some = got.astype(F32).reshape(16, 4, 8, 128)
     some = some[:, 0] + some[:, 1] + some[:, 2] + some[:, 3]
     both = some + jnp.concatenate([some[:, 4:], some[:, :4]], axis=1)
     factor = lax.rsqrt(both / 512 + EPS)
     factor = jnp.concatenate([factor[:, :, 64:], factor[:, :, :64]], axis=2)
     new = own + jnp.sum(some * factor, axis=0)
-    weights = jnp.concatenate([write_w[1], read_w[1]], axis=0)
-    rolled = jnp.concatenate([weights[:, 64:], weights[:, :64]], axis=1)
-    odd, even = quarters(weights), quarters(rolled)
-    blocks = [odd[i // 2] if i % 2 else even[(i // 2 + 3) % 4] for i in range(8)]
-    beside = to_groups(lambda j: 0 * j + 3, blocks, lambda j: j).reshape(64, 8, 128)
     low = iota((64, 8, 128), 2) < 64
-    return (jnp.where(low, jnp.broadcast_to(new[None], (64, 8, 128)), beside).astype(BF),)
+    return (jnp.where(low, jnp.broadcast_to(new[None], (64, 8, 128)), beside.astype(F32)).astype(BF),)
 
 
 def second_finish(got, gain, out_w):
@@ -430,6 +434,9 @@
         cost_estimate=pl.CostEstimate(flops=20000000000, bytes_accessed=0, transcendentals=0),
         compiler_params=pltpu.CompilerParams(vmem_limit_bytes=1024 * 1024),
     )()
+    early, beside = call(
+        spread, "spread", (((64, 16, 128), BF), ((64, 8, 128), BF)), first, write_weight, read_weight
+    )
     small = (conv_inner, conv_write, conv_read, step_bias, decay_log, skip_gain, group_gain)
     small = (*small, state_inner, state_write, state_read)
     out, own, *small = call(
@@ -439,7 +446,7 @@
         ),
         "first_project",
         (((64, 384), BF), ((8, 128), F32)) + tuple((a.shape, a.dtype) for a in small),
-        first,
+        beside,
         hidden,
         norm_gain,
         *weights,
@@ -462,8 +469,7 @@
         state_read,
         step_bias,
         decay_log,
-        write_weight,
-        read_weight,
+        early,
     )
     early = exchange(message, TP)
     message, turned, updated = scan_call(
@@ -477,7 +483,7 @@
     got = exchange(message, DP)
     (out,) = call(first_finish, "first_finish", (((64, 8, 128), BF),), got, group_gain, out_weight)
     got = exchange(out, TP)
-    (out,) = call(first_combine, "first_combine", (((64, 8, 128), BF),), got, own, write_weight, read_weight)
+    (out,) = call(first_combine, "first_combine", (((64, 8, 128), BF),), got, own, beside)
     got = exchange(out, TP)
     out, own = call(
         second_project,

time: 139 us -> 140 us (level)
    pallas_call x8 -> x9, Pallas kernels: 3.31 us -> 3.48 us  [call(): pl.pallas_call(kernel, name=name, out_shape=tuple((jax.ShapeDtypeStruct(s...]
where the time goes in v6:
time: 140 us; the launch traced here: 139 us
  blocking collectives  129 us (92%)
  Pallas kernels  7.63 us (5%)
    all_to_all x10, blocking collectives, exchange(): return lax.all_to_all(pieces, axis, 0, 0, tiled=True)  129 us
    pallas_call x9, Pallas kernels, call(): pl.pallas_call(kernel, name=name, out_shape=tuple((jax.ShapeDtypeStruct(s...  3.48 us

profile of v6, /device:TPU:2, one launch (start us, length us, event | category | flops | bytes accessed | tf_op | source)
XLA Modules:
  0.0 139.1 jit_solution(9320718930782210490)
XLA Ops:
  0.6 0.0 copy-start.6
  0.6 0.0 copy-start.5
  0.7 0.0 copy-start.1
  0.7 0.0 copy-start.2
  0.7 0.0 copy-start.3
  0.7 0.0 copy-start.13
  0.7 0.0 copy-start.14
  0.7 0.0 copy-start.16
  0.7 0.0 copy-start.17
  0.7 0.0 copy-start.18
  0.7 0.7 copy-done.6
  1.5 0.0 copy-done.5
  1.5 1.1 spread.1
  2.6 0.0 copy-start.8
  2.6 0.0 copy-start.12
  2.6 0.0 copy-start.15
  2.6 0.0 copy-done.1
  2.7 0.0 copy-done.2
  2.7 0.0 copy-done.3
  2.7 0.0 copy-done.13
  2.7 0.0 copy-done.14
  2.7 0.0 copy-done.16
  2.7 0.0 copy-done.17
  2.7 0.0 copy-done.18
  2.7 0.0 copy-done.7
  2.7 0.0 copy-done.9
  2.8 0.5 copy-done.8
  3.3 0.0 copy-done.12
  3.3 0.0 copy-done.15
  3.3 0.3 first_project.1
  3.7 12.3 %all_to_all.50.refs_0_ = bf16[8,8,384]{2,1,0:T(8,128)(2,1)S(1)} all-to-all(bf16[8,8,384]{2,1,0:T(8,128)(2,1)S(1)} %bitcast.21), channel_id=1, replica_groups=mesh['tp_0'=8,'tp_1'=8,'dp_0'=4,'dp_1'=2] {'dp_0','dp_1'}, dimensions={0} | all-to-all | bytes 98304 | tf_op jit(solution)/shard_map/all_to_all | solution.py:398
  16.0 0.5 first_states.1
  16.5 27.6 %all_to_all.51.refs_0_.refs_7_ = bf16[64,16,128]{2,1,0:T(8,128)(2,1)S(1)} all-to-all(bf16[64,16,128]{2,1,0:T(8,128)(2,1)S(1)} %get-tuple-element.47), channel_id=1, replica_groups=mesh['tp_0'=8,'tp_1'=8,'dp_0'=4,'dp_1'=2] {'tp_0','tp_1'}, dimensions={0} | all-to-all | bytes 524288 | tf_op jit(solution)/shard_map/all_to_all | solution.py:398
  44.2 1.1 first_scan.1
  45.2 7.7 %all_to_all.52.refs_0_ = bf16[8,8,128]{2,1,0:T(8,128)(2,1)S(1)} all-to-all(bf16[8,8,128]{2,1,0:T(8,128)(2,1)S(1)} %get-tuple-element.50), channel_id=1, replica_groups=mesh['tp_0'=8,'tp_1'=8,'dp_0'=4,'dp_1'=2] {'dp_0','dp_1'}, dimensions={0} | all-to-all | bytes 32768 | tf_op jit(solution)/shard_map/all_to_all | solution.py:398
  52.9 0.3 first_finish.1
  53.2 16.7 %all_to_all.53.refs_0_ = bf16[64,8,128]{2,1,0:T(8,128)(2,1)S(1)} all-to-all(bf16[64,8,128]{2,1,0:T(8,128)(2,1)S(1)} %first_finish.1), channel_id=1, replica_groups=mesh['tp_0'=8,'tp_1'=8,'dp_0'=4,'dp_1'=2] {'tp_0','tp_1'}, dimensions={0} | all-to-all | bytes 262144 | tf_op jit(solution)/shard_map/all_to_all | solution.py:398
  69.9 0.1 first_combine.1
  70.1 16.6 %all_to_all.54.refs_0_ = bf16[64,8,128]{2,1,0:T(8,128)(2,1)S(1)} all-to-all(bf16[64,8,128]{2,1,0:T(8,128)(2,1)S(1)} %first_combine.1), channel_id=1, replica_groups=mesh['tp_0'=8,'tp_1'=8,'dp_0'=4,'dp_1'=2] {'tp_0','tp_1'}, dimensions={0} | all-to-all | bytes 262144 | tf_op jit(solution)/shard_map/all_to_all | solution.py:398
  86.6 0.7 second_project.1
  87.4 8.1 %all_to_all.55.refs_0_ = bf16[8,8,640]{2,1,0:T(8,128)(2,1)S(1)} all-to-all(bf16[8,8,640]{2,1,0:T(8,128)(2,1)S(1)} %bitcast.20), channel_id=1, replica_groups=mesh['tp_0'=8,'tp_1'=8,'dp_0'=4,'dp_1'=2] {'dp_0','dp_1'}, dimensions={0} | all-to-all | bytes 163840 | tf_op jit(solution)/shard_map/all_to_all | solution.py:398
  95.4 1.6 %second_scan.1 = (bf16[8,8,128]{2,1,0:T(8,128)(2,1)S(1)}, bf16[8,640]{1,0:T(8,128)(2,1)S(1)}, f32[8,128,128]{2,1,0:T(8,128)S(1)}, f32[2,8,128,128]{3,2,1,0:T(8,128)}) custom-call(bf16[8,8,640]{2,1,0:T(8,128)(2,1)S(1)} %all_to_all.55.refs_0_, f32[40,256]{1,0:T(8,128)S(1)} %get-tuple-element.54.refs_1_, ...), custom_call_target="tpu_custom_call" | custom-call | tf_op jit(solution)/shard_map/second_scan/pallas_call | solution.py:361
  97.1 7.7 %all_to_all.56.refs_0_ = bf16[8,8,128]{2,1,0:T(8,128)(2,1)S(1)} all-to-all(bf16[8,8,128]{2,1,0:T(8,128)(2,1)S(1)} %get-tuple-element.56), channel_id=1, replica_groups=mesh['tp_0'=8,'tp_1'=8,'dp_0'=4,'dp_1'=2] {'dp_0','dp_1'}, dimensions={0} | all-to-all | bytes 32768 | tf_op jit(solution)/shard_map/all_to_all | solution.py:398
  104.8 0.3 second_finish.1
  105.1 10.9 %all_to_all.57.refs_0_ = bf16[8,40,128]{2,1,0:T(8,128)(2,1)S(1)} all-to-all(bf16[8,40,128]{2,1,0:T(8,128)(2,1)S(1)} %second_finish.1), channel_id=1, replica_groups=mesh['tp_0'=8,'tp_1'=8,'dp_0'=4,'dp_1'=2] {'tp_1'}, dimensions={0} | all-to-all | bytes 163840 | tf_op jit(solution)/shard_map/all_to_all | solution.py:398
  116.1 10.8 %all_to_all.58.refs_0_ = bf16[8,32,128]{2,1,0:T(8,128)(2,1)S(1)} all-to-all(bf16[8,32,128]{2,1,0:T(8,128)(2,1)S(1)} %second_scale.1), channel_id=1, replica_groups=mesh['tp_0'=8,'tp_1'=8,'dp_0'=4,'dp_1'=2] {'tp_0'}, dimensions={0} | all-to-all | bytes 131072 | tf_op jit(solution)/shard_map/all_to_all | solution.py:398
  126.8 10.8 %all_to_all.59.refs_0_ = bf16[8,32,128]{2,1,0:T(8,128)(2,1)S(1)} all-to-all(bf16[8,32,128]{2,1,0:T(8,128)(2,1)S(1)} %second_combine.1), channel_id=1, replica_groups=mesh['tp_0'=8,'tp_1'=8,'dp_0'=4,'dp_1'=2] {'tp_1'}, dimensions={0} | all-to-all | bytes 131072 | tf_op jit(solution)/shard_map/all_to_all | solution.py:398
  137.6 1.5 %last.1 = (bf16[64,512]{1,0:T(8,128)(2,1)}, bf16[2,3,8,128]{3,2,1,0:T(8,128)(2,1)}, bf16[2,3,8,32]{3,2,1,0:T(8,128)(2,1)}, bf16[2,3,8,32]{3,2,1,0:T(8,128)(2,1)}, f32[2,8,128,128]{3,2,1,0:T(8,128)}) custom-call(bf16[8,32,128]{2,1,0:T(8,128)(2,1)S(1)} %all_to_all.59.refs_0_, ...), custom_call_target="tpu_custom_call", output_to_operand_aliasing={{4}: (7, {})} | custom-call | tf_op jit(solution)/shard_map/last/pallas_call | solution.py:384
  (13 shorter events, 0.1 us)
Async XLA Ops:
  0.6 0.8 copy-start.6
  0.6 0.9 copy-start.5
  0.7 2.0 %copy-start.1 = (bf16[2,512,128]{2,1,0:T(8,128)(2,1)S(1)}, bf16[2,512,128]{2,1,0:T(8,128)(2,1)}, u32[]{:S(2)}) copy-start(bf16[2,512,128]{2,1,0:T(8,128)(2,1)} %refs_2_.6) | copy-start | bytes 786436
  0.7 2.0 %copy-start.2 = (bf16[2,512,128]{2,1,0:T(8,128)(2,1)S(1)}, bf16[2,512,128]{2,1,0:T(8,128)(2,1)}, u32[]{:S(2)}) copy-start(bf16[2,512,128]{2,1,0:T(8,128)(2,1)} %refs_3_.3) | copy-start | bytes 786436
  0.7 2.0 %copy-start.3 = (bf16[2,512,128]{2,1,0:T(8,128)(2,1)S(1)}, bf16[2,512,128]{2,1,0:T(8,128)(2,1)}, u32[]{:S(2)}) copy-start(bf16[2,512,128]{2,1,0:T(8,128)(2,1)} %refs_6_.1) | copy-start | bytes 786436
  0.7 2.0 %copy-start.13 = (bf16[2,4,32]{2,1,0:T(4,128)(2,1)S(1)}, bf16[2,4,32]{2,1,0:T(4,128)(2,1)}, u32[]{:S(2)}) copy-start(bf16[2,4,32]{2,1,0:T(4,128)(2,1)} %refs_9_.1) | copy-start | bytes 1540
  0.7 2.0 %copy-start.14 = (bf16[2,4,32]{2,1,0:T(4,128)(2,1)S(1)}, bf16[2,4,32]{2,1,0:T(4,128)(2,1)}, u32[]{:S(2)}) copy-start(bf16[2,4,32]{2,1,0:T(4,128)(2,1)} %refs_10_.1) | copy-start | bytes 1540
  0.7 2.0 %copy-start.16 = (f32[2,2]{1,0:T(2,128)S(1)}, f32[2,2]{1,0:T(2,128)}, u32[]{:S(2)}) copy-start(f32[2,2]{1,0:T(2,128)} %refs_12_.1) | copy-start | bytes 52
  0.7 2.0 %copy-start.17 = (f32[2,2]{1,0:T(2,128)S(1)}, f32[2,2]{1,0:T(2,128)}, u32[]{:S(2)}) copy-start(f32[2,2]{1,0:T(2,128)} %refs_13_.1) | copy-start | bytes 52
  0.7 2.0 %copy-start.18 = (f32[2,128]{1,0:T(2,128)S(1)}, f32[2,128]{1,0:T(2,128)}, u32[]{:S(2)}) copy-start(f32[2,128]{1,0:T(2,128)} %refs_14_.1) | copy-start | bytes 3076
  1.5 1.2 copy-start.7
  1.5 1.2 copy-start.9
  1.5 1.2 copy-start.10
  1.5 1.2 copy-start.11
  2.6 0.7 copy-start.8
  2.6 0.7 copy-start.12
  2.6 0.7 copy-start.15
  3.3 40.8 %copy-start = (f32[2,8,2,64,128]{4,3,2,1,0:T(8,128)S(1)}, f32[2,8,2,64,128]{4,3,2,1,0:T(8,128)}, u32[]{:S(2)}) copy-start(f32[2,8,2,64,128]{4,3,2,1,0:T(8,128)} %param.37) | copy-start | bytes 3145732
  44.2 8.8 %copy-start.4 = (bf16[2,128,512]{2,1,0:T(8,128)(2,1)S(1)}, bf16[2,128,512]{2,1,0:T(8,128)(2,1)}, u32[]{:S(2)}) copy-start(bf16[2,128,512]{2,1,0:T(8,128)(2,1)} %refs_2_.7) | copy-start | bytes 786436

commit v7 on v6

--- a/solution.py
+++ b/solution.py
@@ -45,12 +45,10 @@
 
 
 def to_groups(entry, blocks, pick):
-    row, col = iota((512, 64), 0), iota((512, 64), 1)
-    here = col == channel(entry(row % 8), row // 32)
-    total = jnp.zeros((512, 128), F32)
-    for b, block in enumerate(blocks):
-        total = total + dot(one_hot(here & (pick(row % 8) == b)), block)
-    return total
+    width = 64 * len(blocks)
+    row, col = iota((512, width), 0), iota((512, width), 1)
+    here = (col % 64 == channel(entry(row % 8), row // 32)) & (col // 64 == pick(row % 8))
+    return dot(one_hot(here), jnp.concatenate(blocks, axis=0))
 
 
 def quarters(weights):
@@ -434,27 +432,30 @@
         cost_estimate=pl.CostEstimate(flops=20000000000, bytes_accessed=0, transcendentals=0),
         compiler_params=pltpu.CompilerParams(vmem_limit_bytes=1024 * 1024),
     )()
-    early, beside = call(
-        spread, "spread", (((64, 16, 128), BF), ((64, 8, 128), BF)), first, write_weight, read_weight
-    )
     small = (conv_inner, conv_write, conv_read, step_bias, decay_log, skip_gain, group_gain)
-    small = (*small, state_inner, state_write, state_read)
-    out, own, *small = call(
-        lambda t, first, hidden, gain, gate, inner, write, read, step, *small: (
-            *first_project(t, hidden, gain, gate, inner, write, read, step),
-            *small,
-        ),
+    small = (*small, state_inner, state_write, state_read, norm_gain)
+    early, beside, *small = call(
+        lambda first, write, read, *small: (*spread(first, write, read), *small),
+        "spread",
+        (((64, 16, 128), BF), ((64, 8, 128), BF)) + tuple((a.shape, a.dtype) for a in small),
+        first,
+        write_weight,
+        read_weight,
+        *small,
+    )
+    norm_gain = small[10]
+    out, own = call(
+        lambda t, beside, *rest: first_project(t, *rest),
         "first_project",
-        (((64, 384), BF), ((8, 128), F32)) + tuple((a.shape, a.dtype) for a in small),
+        (((64, 384), BF), ((8, 128), F32)),
         beside,
         hidden,
         norm_gain,
         *weights,
-        *small,
         placed=True,
     )
     conv_inner, conv_write, conv_read, step_bias, decay_log, skip_gain, group_gain = small[:7]
-    state_inner, state_write, state_read = small[7:]
+    state_inner, state_write, state_read = small[7:10]
     got = exchange(out.reshape(8, 8, 384), DP)
     message, parts, raw0 = call(
         first_states,

time: 140 us -> 139 us (level)
  no operation moved by 1% of the time
where the time goes in v7:
time: 139 us; the launch traced here: 138 us
  blocking collectives  129 us (93%)
  Pallas kernels  7.29 us (5%)
    all_to_all x10, blocking collectives, exchange(): return lax.all_to_all(pieces, axis, 0, 0, tiled=True)  129 us
    pallas_call x9, Pallas kernels, call(): pl.pallas_call(kernel, name=name, out_shape=tuple((jax.ShapeDtypeStruct(s...  3.14 us

profile of v7, /device:TPU:2, one launch (start us, length us, event | category | flops | bytes accessed | tf_op | source)
XLA Modules:
  0.0 138.3 jit_solution(17581468941754333022)
XLA Ops:
  0.6 0.0 copy-start.6
  0.6 0.0 copy-start.5
  0.7 0.0 copy-start.8
  0.7 0.0 copy-start.9
  0.7 0.0 copy-start.10
  0.7 0.0 copy-start.13
  0.7 0.0 copy-start.14
  0.7 0.0 copy-start.16
  0.7 0.0 copy-start.17
  0.7 0.0 copy-start.18
  0.7 0.0 copy-start.1
  0.7 0.0 copy-start.2
  0.8 0.0 copy-start.3
  0.8 0.0 copy-start.11
  0.8 0.0 copy-start.12
  0.8 0.0 copy-start.15
  0.8 0.7 copy-done.6
  1.5 0.0 copy-done.5
  1.5 0.0 copy-done.8
  1.5 0.0 copy-done.9
  1.5 0.0 copy-done.10
  1.5 0.0 copy-done.13
  1.5 0.0 copy-done.14
  1.6 0.0 copy-done.11
  1.6 0.0 copy-done.12
  1.6 0.0 copy-done.15
  1.6 0.8 spread.1
  2.4 0.1 copy-done.7
  2.5 0.3 first_project.1
  2.9 12.3 %all_to_all.50.refs_0_ = bf16[8,8,384]{2,1,0:T(8,128)(2,1)S(1)} all-to-all(bf16[8,8,384]{2,1,0:T(8,128)(2,1)S(1)} %bitcast.21), channel_id=1, replica_groups=mesh['tp_0'=8,'tp_1'=8,'dp_0'=4,'dp_1'=2] {'dp_0','dp_1'}, dimensions={0} | all-to-all | bytes 98304 | tf_op jit(solution)/shard_map/all_to_all | solution.py:396
  15.2 0.5 first_states.1
  15.8 27.6 %all_to_all.51.refs_0_.refs_7_ = bf16[64,16,128]{2,1,0:T(8,128)(2,1)S(1)} all-to-all(bf16[64,16,128]{2,1,0:T(8,128)(2,1)S(1)} %get-tuple-element.49), channel_id=1, replica_groups=mesh['tp_0'=8,'tp_1'=8,'dp_0'=4,'dp_1'=2] {'tp_0','tp_1'}, dimensions={0} | all-to-all | bytes 524288 | tf_op jit(solution)/shard_map/all_to_all | solution.py:396
  43.4 1.1 first_scan.1
  44.4 7.7 %all_to_all.52.refs_0_ = bf16[8,8,128]{2,1,0:T(8,128)(2,1)S(1)} all-to-all(bf16[8,8,128]{2,1,0:T(8,128)(2,1)S(1)} %get-tuple-element.52), channel_id=1, replica_groups=mesh['tp_0'=8,'tp_1'=8,'dp_0'=4,'dp_1'=2] {'dp_0','dp_1'}, dimensions={0} | all-to-all | bytes 32768 | tf_op jit(solution)/shard_map/all_to_all | solution.py:396
  52.1 0.0 copy-done.4
  52.1 0.3 first_finish.1
  52.4 16.7 %all_to_all.53.refs_0_ = bf16[64,8,128]{2,1,0:T(8,128)(2,1)S(1)} all-to-all(bf16[64,8,128]{2,1,0:T(8,128)(2,1)S(1)} %first_finish.1), channel_id=1, replica_groups=mesh['tp_0'=8,'tp_1'=8,'dp_0'=4,'dp_1'=2] {'tp_0','tp_1'}, dimensions={0} | all-to-all | bytes 262144 | tf_op jit(solution)/shard_map/all_to_all | solution.py:396
  69.1 0.1 first_combine.1
  69.3 16.6 %all_to_all.54.refs_0_ = bf16[64,8,128]{2,1,0:T(8,128)(2,1)S(1)} all-to-all(bf16[64,8,128]{2,1,0:T(8,128)(2,1)S(1)} %first_combine.1), channel_id=1, replica_groups=mesh['tp_0'=8,'tp_1'=8,'dp_0'=4,'dp_1'=2] {'tp_0','tp_1'}, dimensions={0} | all-to-all | bytes 262144 | tf_op jit(solution)/shard_map/all_to_all | solution.py:396
  85.8 0.7 second_project.1
  86.6 8.1 %all_to_all.55.refs_0_ = bf16[8,8,640]{2,1,0:T(8,128)(2,1)S(1)} all-to-all(bf16[8,8,640]{2,1,0:T(8,128)(2,1)S(1)} %bitcast.20), channel_id=1, replica_groups=mesh['tp_0'=8,'tp_1'=8,'dp_0'=4,'dp_1'=2] {'dp_0','dp_1'}, dimensions={0} | all-to-all | bytes 163840 | tf_op jit(solution)/shard_map/all_to_all | solution.py:396
  94.6 1.6 %second_scan.1 = (bf16[8,8,128]{2,1,0:T(8,128)(2,1)S(1)}, bf16[8,640]{1,0:T(8,128)(2,1)S(1)}, f32[8,128,128]{2,1,0:T(8,128)S(1)}, f32[2,8,128,128]{3,2,1,0:T(8,128)}) custom-call(bf16[8,8,640]{2,1,0:T(8,128)(2,1)S(1)} %all_to_all.55.refs_0_, f32[40,256]{1,0:T(8,128)S(1)} %get-tuple-element.56.refs_1_, ...), custom_call_target="tpu_custom_call" | custom-call | tf_op jit(solution)/shard_map/second_scan/pallas_call | solution.py:359
  96.3 7.7 %all_to_all.56.refs_0_ = bf16[8,8,128]{2,1,0:T(8,128)(2,1)S(1)} all-to-all(bf16[8,8,128]{2,1,0:T(8,128)(2,1)S(1)} %get-tuple-element.58), channel_id=1, replica_groups=mesh['tp_0'=8,'tp_1'=8,'dp_0'=4,'dp_1'=2] {'dp_0','dp_1'}, dimensions={0} | all-to-all | bytes 32768 | tf_op jit(solution)/shard_map/all_to_all | solution.py:396
  104.0 0.3 second_finish.1
  104.3 10.9 %all_to_all.57.refs_0_ = bf16[8,40,128]{2,1,0:T(8,128)(2,1)S(1)} all-to-all(bf16[8,40,128]{2,1,0:T(8,128)(2,1)S(1)} %second_finish.1), channel_id=1, replica_groups=mesh['tp_0'=8,'tp_1'=8,'dp_0'=4,'dp_1'=2] {'tp_1'}, dimensions={0} | all-to-all | bytes 163840 | tf_op jit(solution)/shard_map/all_to_all | solution.py:396
  115.3 10.8 %all_to_all.58.refs_0_ = bf16[8,32,128]{2,1,0:T(8,128)(2,1)S(1)} all-to-all(bf16[8,32,128]{2,1,0:T(8,128)(2,1)S(1)} %second_scale.1), channel_id=1, replica_groups=mesh['tp_0'=8,'tp_1'=8,'dp_0'=4,'dp_1'=2] {'tp_0'}, dimensions={0} | all-to-all | bytes 131072 | tf_op jit(solution)/shard_map/all_to_all | solution.py:396
  126.0 10.8 %all_to_all.59.refs_0_ = bf16[8,32,128]{2,1,0:T(8,128)(2,1)S(1)} all-to-all(bf16[8,32,128]{2,1,0:T(8,128)(2,1)S(1)} %second_combine.1), channel_id=1, replica_groups=mesh['tp_0'=8,'tp_1'=8,'dp_0'=4,'dp_1'=2] {'tp_1'}, dimensions={0} | all-to-all | bytes 131072 | tf_op jit(solution)/shard_map/all_to_all | solution.py:396
  136.8 1.5 %last.1 = (bf16[64,512]{1,0:T(8,128)(2,1)}, bf16[2,3,8,128]{3,2,1,0:T(8,128)(2,1)}, bf16[2,3,8,32]{3,2,1,0:T(8,128)(2,1)}, bf16[2,3,8,32]{3,2,1,0:T(8,128)(2,1)}, f32[2,8,128,128]{3,2,1,0:T(8,128)}) custom-call(bf16[8,32,128]{2,1,0:T(8,128)(2,1)S(1)} %all_to_all.59.refs_0_, ...), custom_call_target="tpu_custom_call", output_to_operand_aliasing={{4}: (7, {})} | custom-call | tf_op jit(solution)/shard_map/last/pallas_call | solution.py:382
  (13 shorter events, 0.1 us)
Async XLA Ops:
  0.6 0.8 copy-start.6
  0.6 0.9 copy-start.5
  0.7 0.9 copy-start.8
  0.7 0.8 copy-start.9
  0.7 0.8 copy-start.10
  0.7 0.8 copy-start.13
  0.7 0.8 copy-start.14
  0.7 0.8 copy-start.16
  0.7 0.8 copy-start.17
  0.7 0.8 copy-start.18
  0.7 1.7 %copy-start.1 = (bf16[2,512,128]{2,1,0:T(8,128)(2,1)S(1)}, bf16[2,512,128]{2,1,0:T(8,128)(2,1)}, u32[]{:S(2)}) copy-start(bf16[2,512,128]{2,1,0:T(8,128)(2,1)} %refs_2_.4) | copy-start | bytes 786436
  0.7 1.7 %copy-start.2 = (bf16[2,512,128]{2,1,0:T(8,128)(2,1)S(1)}, bf16[2,512,128]{2,1,0:T(8,128)(2,1)}, u32[]{:S(2)}) copy-start(bf16[2,512,128]{2,1,0:T(8,128)(2,1)} %refs_3_.5) | copy-start | bytes 786436
  0.8 1.7 %copy-start.3 = (bf16[2,512,128]{2,1,0:T(8,128)(2,1)S(1)}, bf16[2,512,128]{2,1,0:T(8,128)(2,1)}, u32[]{:S(2)}) copy-start(bf16[2,512,128]{2,1,0:T(8,128)(2,1)} %refs_6_.3) | copy-start | bytes 786436
  0.8 0.8 copy-start.11
  0.8 0.8 copy-start.12
  0.8 0.8 copy-start.15
  1.6 0.9 copy-start.7
  2.5 40.8 %copy-start = (f32[2,8,2,64,128]{4,3,2,1,0:T(8,128)S(1)}, f32[2,8,2,64,128]{4,3,2,1,0:T(8,128)}, u32[]{:S(2)}) copy-start(f32[2,8,2,64,128]{4,3,2,1,0:T(8,128)} %param.37) | copy-start | bytes 3145732
  43.4 8.8 %copy-start.4 = (bf16[2,128,512]{2,1,0:T(8,128)(2,1)S(1)}, bf16[2,128,512]{2,1,0:T(8,128)(2,1)}, u32[]{:S(2)}) copy-start(bf16[2,128,512]{2,1,0:T(8,128)(2,1)} %refs_2_.5) | copy-start | bytes 786436

commit v8 on v7

--- a/solution.py
+++ b/solution.py
@@ -321,8 +321,8 @@
     out_ref[...] = jnp.zeros((8, 128), F32)
 
 
-def start_copies(source, dest, sems):
-    copies = [pltpu.make_async_copy(source.at[b], dest.at[b], sems.at[b]) for b in range(8)]
+def start_copies(source, dest, sems, rows=range(8)):
+    copies = [pltpu.make_async_copy(source.at[b], dest.at[b], sems.at[b]) for b in rows]
     for copy in copies:
         copy.start()
     return copies
@@ -337,8 +337,8 @@
         if earlier is None:
             dest = refs[n_in + 1 :]
         else:
-            dest, whole_ref, sem = refs[n_in + 2 : -2], refs[-2], refs[-1]
-            copies = start_copies(refs[n_in + 1], whole_ref.at[0], sem)
+            dest, whole_ref, sem = refs[n_in + 3 : -2], refs[-2], refs[-1]
+            copies = start_copies(refs[n_in + 1], whole_ref.at[0], sem, range(4, 8))
         results = fn(*values[:-1], state, values[-1])
         for ref, value in zip(dest[:-1], results[:-1]):
             ref[...] = value
@@ -349,8 +349,11 @@
                 copy.wait()
 
     whole = pl.BlockSpec(memory_space=pltpu.VMEM)
-    specs = [whole] * (n_in + 1 + (earlier is not None))
-    operands = (*args, recurrent) + (() if earlier is None else (earlier,))
+    specs = [whole] * (n_in + 1)
+    operands = (*args, recurrent)
+    if earlier is not None:
+        specs += [whole, pl.BlockSpec(memory_space=pl.ANY)]
+        operands += earlier
     outs = (*outs, ((8, 128, 128), F32))
     out_specs = [whole] * len(outs)
     if earlier is not None:
@@ -362,9 +365,35 @@
         out_shape=tuple(jax.ShapeDtypeStruct(s, d) for s, d in outs),
         in_specs=specs,
         out_specs=tuple(out_specs),
+        input_output_aliases={} if earlier is None else {n_in + 2: len(outs) - 1},
         scratch_shapes=[] if earlier is None else [pltpu.SemaphoreType.DMA((8,))],
         compiler_params=pltpu.CompilerParams(vmem_limit_bytes=16 * 1024 * 1024),
     )(*operands)
+
+
+def second_project_call(outs, args, state):
+    n_in = len(args)
+
+    def kernel(*refs):
+        dest, whole_ref, sem = refs[n_in + 1 : -2], refs[-2], refs[-1]
+        copies = start_copies(refs[n_in], whole_ref.at[0], sem, range(4))
+        t = lax.axis_index(Z) * 8 + lax.axis_index(Y)
+        for ref, value in zip(dest, second_project(t, *[r[...] for r in refs[:n_in]])):
+            ref[...] = value
+        for copy in copies:
+            copy.wait()
+
+    whole = pl.BlockSpec(memory_space=pltpu.VMEM)
+    return pl.pallas_call(
+        kernel,
+        name="second_project",
+        out_shape=tuple(jax.ShapeDtypeStruct(s, d) for s, d in outs)
+        + (jax.ShapeDtypeStruct((2, 8, 128, 128), F32),),
+        in_specs=[whole] * (n_in + 1),
+        out_specs=tuple(whole for _ in outs) + (pl.BlockSpec(memory_space=pl.ANY),),
+        scratch_shapes=[pltpu.SemaphoreType.DMA((8,))],
+        compiler_params=pltpu.CompilerParams(vmem_limit_bytes=16 * 1024 * 1024),
+    )(*args, state)
 
 
 def last_call(outs, args, state, whole_state):
@@ -486,15 +515,8 @@
     got = exchange(out, TP)
     (out,) = call(first_combine, "first_combine", (((64, 8, 128), BF),), got, own, beside)
     got = exchange(out, TP)
-    out, own = call(
-        second_project,
-        "second_project",
-        (((64, 640), BF), ((32, 128), F32)),
-        got,
-        norm_gain,
-        *weights,
-        early,
-        placed=True,
+    out, own, whole_state = second_project_call(
+        (((64, 640), BF), ((32, 128), F32)), (got, norm_gain, *weights, early), updated
     )
     got = exchange(out.reshape(8, 8, 640), DP)
     message, raw1, second, updated = scan_call(
@@ -503,7 +525,7 @@
         (((8, 8, 128), BF), ((8, 640), BF)),
         (got, turned, conv_inner, state_inner, step_bias, decay_log, skip_gain),
         recurrent,
-        updated,
+        (updated, whole_state),
     )
     got = exchange(message, DP)
     (out,) = call(second_finish, "second_finish", (((8, 40, 128), BF),), got, group_gain, out_weight)

time: 139 us -> 139 us (level)
    pallas_call x9 -> x8, Pallas kernels: 3.14 us -> 2.4 us  [call(): pl.pallas_call(kernel, name=name, out_shape=tuple((jax.ShapeDtypeStruct(s...]
where the time goes in v8:
time: 139 us
  blocking collectives  129 us (93%)
  Pallas kernels  7.68 us (6%)
    all_to_all x10, blocking collectives, exchange(): return lax.all_to_all(pieces, axis, 0, 0, tiled=True)  129 us

profile of v8, /device:TPU:2, one launch (start us, length us, event | category | flops | bytes accessed | tf_op | source)
XLA Modules:
  0.0 138.7 jit_solution(17138641185604898271)
XLA Ops:
  0.6 0.0 copy-start.6
  0.6 0.0 copy-start.5
  0.7 0.0 copy-start.8
  0.7 0.0 copy-start.9
  0.7 0.0 copy-start.10
  0.7 0.0 copy-start.13
  0.7 0.0 copy-start.14
  0.7 0.0 copy-start.16
  0.7 0.0 copy-start.17
  0.7 0.0 copy-start.18
  0.7 0.0 copy-start.1
  0.7 0.0 copy-start.2
  0.8 0.0 copy-start.3
  0.8 0.0 copy-start.11
  0.8 0.0 copy-start.12
  0.8 0.0 copy-start.15
  0.8 0.7 copy-done.6
  1.5 0.0 copy-done.5
  1.5 0.0 copy-done.8
  1.5 0.0 copy-done.9
  1.5 0.0 copy-done.10
  1.5 0.0 copy-done.13
  1.6 0.0 copy-done.11
  1.6 0.0 copy-done.12
  1.6 0.0 copy-done.15
  1.6 0.8 spread.1
  2.4 0.1 copy-done.7
  2.5 0.3 first_project.1
  2.9 12.3 %all_to_all.50.refs_0_ = bf16[8,8,384]{2,1,0:T(8,128)(2,1)S(1)} all-to-all(bf16[8,8,384]{2,1,0:T(8,128)(2,1)S(1)} %bitcast.21), channel_id=1, replica_groups=mesh['tp_0'=8,'tp_1'=8,'dp_0'=4,'dp_1'=2] {'dp_0','dp_1'}, dimensions={0} | all-to-all | bytes 98304 | tf_op jit(solution)/shard_map/all_to_all | solution.py:425
  15.2 0.5 first_states.1
  15.8 27.6 %all_to_all.51.refs_0_.refs_7_ = bf16[64,16,128]{2,1,0:T(8,128)(2,1)S(1)} all-to-all(bf16[64,16,128]{2,1,0:T(8,128)(2,1)S(1)} %get-tuple-element.50), channel_id=1, replica_groups=mesh['tp_0'=8,'tp_1'=8,'dp_0'=4,'dp_1'=2] {'tp_0','tp_1'}, dimensions={0} | all-to-all | bytes 524288 | tf_op jit(solution)/shard_map/all_to_all | solution.py:425
  43.4 0.0 copy-done
  43.4 1.1 first_scan.1
  44.4 7.7 %all_to_all.52.refs_0_ = bf16[8,8,128]{2,1,0:T(8,128)(2,1)S(1)} all-to-all(bf16[8,8,128]{2,1,0:T(8,128)(2,1)S(1)} %get-tuple-element.53), channel_id=1, replica_groups=mesh['tp_0'=8,'tp_1'=8,'dp_0'=4,'dp_1'=2] {'dp_0','dp_1'}, dimensions={0} | all-to-all | bytes 32768 | tf_op jit(solution)/shard_map/all_to_all | solution.py:425
  52.1 0.0 copy-done.4
  52.1 0.3 first_finish.1
  52.4 16.7 %all_to_all.53.refs_0_ = bf16[64,8,128]{2,1,0:T(8,128)(2,1)S(1)} all-to-all(bf16[64,8,128]{2,1,0:T(8,128)(2,1)S(1)} %first_finish.1), channel_id=1, replica_groups=mesh['tp_0'=8,'tp_1'=8,'dp_0'=4,'dp_1'=2] {'tp_0','tp_1'}, dimensions={0} | all-to-all | bytes 262144 | tf_op jit(solution)/shard_map/all_to_all | solution.py:425
  69.1 0.1 first_combine.1
  69.3 16.6 %all_to_all.54.refs_0_ = bf16[64,8,128]{2,1,0:T(8,128)(2,1)S(1)} all-to-all(bf16[64,8,128]{2,1,0:T(8,128)(2,1)S(1)} %first_combine.1), channel_id=1, replica_groups=mesh['tp_0'=8,'tp_1'=8,'dp_0'=4,'dp_1'=2] {'tp_0','tp_1'}, dimensions={0} | all-to-all | bytes 262144 | tf_op jit(solution)/shard_map/all_to_all | solution.py:425
  85.8 1.1 second_project.1
  87.0 8.1 %all_to_all.55.refs_0_ = bf16[8,8,640]{2,1,0:T(8,128)(2,1)S(1)} all-to-all(bf16[8,8,640]{2,1,0:T(8,128)(2,1)S(1)} %bitcast.20), channel_id=1, replica_groups=mesh['tp_0'=8,'tp_1'=8,'dp_0'=4,'dp_1'=2] {'dp_0','dp_1'}, dimensions={0} | all-to-all | bytes 163840 | tf_op jit(solution)/shard_map/all_to_all | solution.py:425
  95.0 1.6 %second_scan.1 = (bf16[8,8,128]{2,1,0:T(8,128)(2,1)S(1)}, bf16[8,640]{1,0:T(8,128)(2,1)S(1)}, f32[8,128,128]{2,1,0:T(8,128)S(1)}, f32[2,8,128,128]{3,2,1,0:T(8,128)}) custom-call(bf16[8,8,640]{2,1,0:T(8,128)(2,1)S(1)} %all_to_all.55.refs_0_, f32[40,256]{1,0:T(8,128)S(1)} %get-tuple-element.58.refs_1_, ...), custom_call_target="tpu_custom_call", output_to_operand_aliasing={{3}: (9, {})} | custom-call | tf_op jit(solution)/shard_map/second_scan/pallas_call | solution.py:362
  96.7 7.7 %all_to_all.56.refs_0_ = bf16[8,8,128]{2,1,0:T(8,128)(2,1)S(1)} all-to-all(bf16[8,8,128]{2,1,0:T(8,128)(2,1)S(1)} %get-tuple-element.60), channel_id=1, replica_groups=mesh['tp_0'=8,'tp_1'=8,'dp_0'=4,'dp_1'=2] {'dp_0','dp_1'}, dimensions={0} | all-to-all | bytes 32768 | tf_op jit(solution)/shard_map/all_to_all | solution.py:425
  104.4 0.3 second_finish.1
  104.7 10.9 %all_to_all.57.refs_0_ = bf16[8,40,128]{2,1,0:T(8,128)(2,1)S(1)} all-to-all(bf16[8,40,128]{2,1,0:T(8,128)(2,1)S(1)} %second_finish.1), channel_id=1, replica_groups=mesh['tp_0'=8,'tp_1'=8,'dp_0'=4,'dp_1'=2] {'tp_1'}, dimensions={0} | all-to-all | bytes 163840 | tf_op jit(solution)/shard_map/all_to_all | solution.py:425
  115.7 10.8 %all_to_all.58.refs_0_ = bf16[8,32,128]{2,1,0:T(8,128)(2,1)S(1)} all-to-all(bf16[8,32,128]{2,1,0:T(8,128)(2,1)S(1)} %second_scale.1), channel_id=1, replica_groups=mesh['tp_0'=8,'tp_1'=8,'dp_0'=4,'dp_1'=2] {'tp_0'}, dimensions={0} | all-to-all | bytes 131072 | tf_op jit(solution)/shard_map/all_to_all | solution.py:425
  126.4 10.7 %all_to_all.59.refs_0_ = bf16[8,32,128]{2,1,0:T(8,128)(2,1)S(1)} all-to-all(bf16[8,32,128]{2,1,0:T(8,128)(2,1)S(1)} %second_combine.1), channel_id=1, replica_groups=mesh['tp_0'=8,'tp_1'=8,'dp_0'=4,'dp_1'=2] {'tp_1'}, dimensions={0} | all-to-all | bytes 131072 | tf_op jit(solution)/shard_map/all_to_all | solution.py:425
  137.2 1.5 %last.1 = (bf16[64,512]{1,0:T(8,128)(2,1)}, bf16[2,3,8,128]{3,2,1,0:T(8,128)(2,1)}, bf16[2,3,8,32]{3,2,1,0:T(8,128)(2,1)}, bf16[2,3,8,32]{3,2,1,0:T(8,128)(2,1)}, f32[2,8,128,128]{3,2,1,0:T(8,128)}) custom-call(bf16[8,32,128]{2,1,0:T(8,128)(2,1)S(1)} %all_to_all.59.refs_0_, ...), custom_call_target="tpu_custom_call", output_to_operand_aliasing={{4}: (7, {})} | custom-call | tf_op jit(solution)/shard_map/last/pallas_call | solution.py:411
  (13 shorter events, 0.1 us)
Async XLA Ops:
  0.6 0.8 copy-start.6
  0.6 0.9 copy-start.5
  0.7 0.9 copy-start.8
  0.7 0.8 copy-start.9
  0.7 0.8 copy-start.10
  0.7 0.8 copy-start.13
  0.7 0.8 copy-start.14
  0.7 0.8 copy-start.16
  0.7 0.8 copy-start.17
  0.7 0.8 copy-start.18
  0.7 1.7 %copy-start.1 = (bf16[2,512,128]{2,1,0:T(8,128)(2,1)S(1)}, bf16[2,512,128]{2,1,0:T(8,128)(2,1)}, u32[]{:S(2)}) copy-start(bf16[2,512,128]{2,1,0:T(8,128)(2,1)} %refs_2_.4) | copy-start | bytes 786436
  0.7 1.7 %copy-start.2 = (bf16[2,512,128]{2,1,0:T(8,128)(2,1)S(1)}, bf16[2,512,128]{2,1,0:T(8,128)(2,1)}, u32[]{:S(2)}) copy-start(bf16[2,512,128]{2,1,0:T(8,128)(2,1)} %refs_3_.5) | copy-start | bytes 786436
  0.8 1.7 %copy-start.3 = (bf16[2,512,128]{2,1,0:T(8,128)(2,1)S(1)}, bf16[2,512,128]{2,1,0:T(8,128)(2,1)}, u32[]{:S(2)}) copy-start(bf16[2,512,128]{2,1,0:T(8,128)(2,1)} %refs_6_.3) | copy-start | bytes 786436
  0.8 0.8 copy-start.11
  0.8 0.8 copy-start.12
  0.8 0.8 copy-start.15
  1.6 0.9 copy-start.7
  2.5 40.8 %copy-start = (f32[2,8,2,64,128]{4,3,2,1,0:T(8,128)S(1)}, f32[2,8,2,64,128]{4,3,2,1,0:T(8,128)}, u32[]{:S(2)}) copy-start(f32[2,8,2,64,128]{4,3,2,1,0:T(8,128)} %param.37) | copy-start | bytes 3145732
  43.4 8.8 %copy-start.4 = (bf16[2,128,512]{2,1,0:T(8,128)(2,1)S(1)}, bf16[2,128,512]{2,1,0:T(8,128)(2,1)}, u32[]{:S(2)}) copy-start(bf16[2,128,512]{2,1,0:T(8,128)(2,1)} %refs_2_.5) | copy-start | bytes 786436
